TPU v7x, 256 devices: a whole 4x4x8 slice. The times are simulated.
256 devices in a mesh: ep: 64 (over z, y, core), tp: 4 (over x).
Axes of the slice: x: 4, y: 4, z: 8, core: 2. Of those that a mesh axis runs over, the one named last changes fastest.
Arguments:
- tokens: bfloat16 [16384, 2048], P('ep'), may hold values from -6 to 6
- expert_ids: int32 [16384, 2], P('ep'), may hold values from 0 to 63, all different within a row; in each aligned block of 256 rows (0 to 255, 256 to 511, ...) at most 24 rows name the same one
- route_weight: float32 [16384, 2], P('ep'), may hold values from 0.1 to 1
- norm_gain: float32 [2048], replicated, may hold values from 0.1 to 1.9
- expert_gate: bfloat16 [64, 2048, 2048], P('ep', None, 'tp'), may hold values from -4 to 4
- expert_up: bfloat16 [64, 2048, 2048], P('ep', None, 'tp'), may hold values from -4 to 4
- expert_down: bfloat16 [64, 2048, 2048], P('ep', 'tp'), may hold values from -0.03125 to 0.03125
Outputs:
- combined: bfloat16 [16384, 2048], P('ep', 'tp')
Inputs may be any that keep to these rules, and one draw needn't show every extreme that they name: `expert_ids`: each row names 2 different experts. In each aligned block of 256 rows (the rows of one index of ep) no expert is named by more than 24 rows, and in some block one expert is named by exactly 24 rows.
All inputs are finite; a program needn't handle non-finite values.
Results may differ from a plain program's by a relative error of at most 0.012.
Values may be sent and summed in bfloat16 or wider, within the bound.
No kernel may reach another device: no remote copies, remote signals or barrier semaphores. Data moves between devices by JAX's collectives and lax.ppermute only.
A program may use at most 128 MiB of HBM per device.

v0:
```python
import jax
import jax.numpy as jnp
from jax import lax
from jax.sharding import PartitionSpec as P

NORM_EPS = 1e-06
CLAMP_LIMIT = 7.0
SWISH_SCALE = 1.702


def normalize(tokens, norm_gain):
    values = tokens.astype(jnp.float32)
    scaled = values * lax.rsqrt(jnp.mean(values * values, axis=-1, keepdims=True) + NORM_EPS)
    return (scaled * norm_gain).astype(jnp.bfloat16)


def activate(gate_sum, up_sum):
    gate_cut = jnp.minimum(gate_sum, CLAMP_LIMIT)
    up_cut = jnp.clip(up_sum, -CLAMP_LIMIT, CLAMP_LIMIT)
    return ((up_cut + 1.0) * gate_cut * jax.nn.sigmoid(SWISH_SCALE * gate_cut)).astype(jnp.bfloat16)


def shards(tokens, expert_ids, route_weight, norm_gain, expert_gate, expert_up, expert_down):
    groups = lax.axis_size("ep")
    tp_count = lax.axis_size("tp")
    member_count = expert_gate.shape[0]
    experts = groups * member_count
    tok_count, model_width = tokens.shape
    top_count = expert_ids.shape[1]
    capacity = min(tok_count, 3 * tok_count * top_count // experts)
    quarter = model_width // tp_count
    normed = normalize(tokens, norm_gain)
    flat_ids = expert_ids.reshape(-1)
    onehot = (flat_ids[:, None] == jnp.arange(experts, dtype=jnp.int32)[None, :]).astype(jnp.int32)
    slot_index = jnp.sum(jnp.cumsum(onehot, axis=0) * onehot, axis=1) - 1
    position = flat_ids * capacity + slot_index
    token_index = jnp.arange(flat_ids.shape[0], dtype=jnp.int32) // top_count
    row_table = jnp.full((experts * capacity,), tok_count, jnp.int32).at[position].set(token_index)
    padded = jnp.concatenate([normed, jnp.zeros((1, model_width), jnp.bfloat16)], axis=0)
    offset = lax.axis_index("tp") * quarter
    source_rows = lax.dynamic_slice_in_dim(padded, offset, quarter, 1)
    send_rows = source_rows[row_table].reshape(groups, member_count, capacity, quarter)
    received = lax.all_to_all(send_rows, "ep", split_axis=0, concat_axis=0, tiled=True)
    slot_count = received.shape[2]
    shard_piece = lax.all_gather(received, "tp", axis=3, tiled=True)
    span_size = shard_piece.shape[3]
    member = 0
    row_block = shard_piece[:, member].reshape(-1, span_size)
    gate_rows = expert_gate[member]
    up_rows = expert_up[member]
    gate_list = [jnp.dot(row_block, gate_rows, preferred_element_type=jnp.float32)]
    up_list = [jnp.dot(row_block, up_rows, preferred_element_type=jnp.float32)]
    gate_sum = jnp.stack(gate_list)
    up_sum = jnp.stack(up_list)
    activated = activate(gate_sum, up_sum)
    member = 0
    weight_rows = expert_down[member]
    product = lax.dot_general(
        weight_rows, activated[member], (((0,), (1,)), ((), ())), preferred_element_type=jnp.float32
    )
    term_list = [product.reshape(quarter * lax.axis_size("tp"), groups, slot_count)]
    summed = lax.psum_scatter(
        jnp.stack(term_list, axis=2).astype(jnp.bfloat16), "tp", scatter_dimension=0, tiled=True
    )
    returned = lax.all_to_all(
        summed.reshape(quarter, experts * capacity), "ep", split_axis=1, concat_axis=1, tiled=True
    )
    picked = jnp.take(returned, position, axis=1).reshape(quarter, tok_count, top_count)
    weighted = jnp.sum(picked.astype(jnp.float32) * route_weight[None, :, :], axis=2)
    return weighted.T.astype(jnp.bfloat16)


def solution(mesh):
    return jax.shard_map(
        shards,
        mesh=mesh,
        in_specs=(
            P("ep", None),
            P("ep", None),
            P("ep", None),
            P(),
            P("ep", None, "tp"),
            P("ep", None, "tp"),
            P("ep", "tp", None),
        ),
        out_specs=P("ep", "tp"),
        check_vma=False,
    )
```

profile of v0, /device:TPU:1, one launch (start us, length us, event | category | flops | bytes accessed | tf_op | source)
XLA Modules:
  0.0 289.8 jit_solution(16499533995587385464)
XLA Ops:
  6.5 1.0 copy.21
  7.5 0.1 eq.26
  7.7 0.1 reshape.111
  7.8 0.7 broadcast_multiply_fusion
  8.5 1.2 reduce-window.6
  9.7 0.2 slice_reduce_fusion
  10.0 0.1 fusion.13
  10.1 0.1 copy.26
  10.3 0.1 mul.76
  10.4 2.5 scatter_custom_fusion
  12.9 1.5 fusion.4
  14.4 1.0 fusion.6
  15.5 5.4 %gather_fusion = bf16[1536,512]{1,0:T(8,128)(2,1)} fusion(bf16[257,512]{1,0:T(8,128)(2,1)S(1)} %pad_dynamic-slice_fusion, s32[2048]{0:T(1024)S(1)} %pad_clamp_fusion), kind=kCustom, calls=%fused_computation | custom fusion | bytes 3151872 | tf_op jit(solution)/shard_map/gather | solution.py:42
  20.9 52.3 %all_to_all.17 = bf16[64,1,24,512]{3,2,1,0:T(8,128)(2,1)} all-to-all(bf16[64,1,24,512]{3,2,1,0:T(8,128)(2,1)} %bitcast.46), channel_id=1, replica_groups=mesh['ep'=64,'tp'=4] {'ep'}, dimensions={0} | all-to-all | bytes 3145728 | tf_op jit(solution)/shard_map/all_to_all | solution.py:43
  73.2 0.0 all-gather.2.cloned.1.call-update
  73.2 0.0 reduce-scatter.2.cloned.1.call-start
  73.3 65.1 %all-gather.2.cloned.1.call-done = bf16[64,1,24,2048]{3,2,1,0:T(8,128)(2,1)} async-done(((bf16[64,1,24,512]{3,2,1,0:T(8,128)(2,1)}), bf16[64,1,24,2048]{3,2,1,0:T(8,128)(2,1)}) %all-gather.2.cloned.1.call-update) | async-done | bytes 6291472 | tf_op jit(solution)/shard_map/all_gather | solution.py:45
  138.4 8.5 %convolution_minimum_fusion = f32[1536,512]{1,0:T(8,128)} fusion(bf16[1536,2048]{1,0:T(8,128)(2,1)} %bitcast.52, bf16[1,2048,512]{2,1,0:T(8,128)(2,1)} %param.11), kind=kOutput, calls=%fused_computation.5 | convolution fusion | flops 3222011904 | bytes 11534336 | tf_op jit(solution)/shard_map/dot_general | solution.py:51
  146.9 11.9 %convolution_convert_fusion = bf16[1536,2048]{1,0:T(8,128)(2,1)} fusion(bf16[1,512,2048]{2,1,0:T(8,128)(2,1)S(1)} %copy-done, f32[1536,512]{1,0:T(8,128)} %convolution_minimum_fusion, bf16[1536,2048]{1,0:T(8,128)(2,1)} %bitcast.53, bf16[1,2048,512]{2,1,0:T(8,128)(2,1)} %param.12), kind=kOutput, calls=%fused_computation.3 | convolution fusion | flops 6452674560 | bytes 19922944 | tf_op jit(solution)/shard_map/dot_general | solution.py:58
  158.8 0.0 reduce-scatter.2.cloned.1.call-update
  158.8 0.0 copy-start.2
  158.8 0.0 copy-start.3
  158.9 67.5 %reduce-scatter.2.cloned.1.call-done = bf16[512,64,1,24]{0,3,1,2:T(8,128)(2,1)} async-done(((bf16[2048,64,1,24]{0,3,1,2:T(8,128)(2,1)}), bf16[512,64,1,24]{0,3,1,2:T(8,128)(2,1)}) %reduce-scatter.2.cloned.1.call-update) | async-done | bytes 1572880 | tf_op jit(solution)/shard_map/reduce_scatter | solution.py:62
  226.3 10.9 %all-to-all-start.1 = ((bf16[512,64,24]{0,2,1:T(8,128)(2,1)}), bf16[512,64,24]{0,2,1:T(8,128)(2,1)}, u32[]{:S(2)}, u32[]{:S(2)}) async-start(bf16[512,64,24]{0,2,1:T(8,128)(2,1)} %bitcast.48), calls=%async_computation.2 | async-start | bytes 3145728 | tf_op jit(solution)/shard_map/all_to_all | solution.py:65
  237.2 0.1 sub.15
  237.4 0.1 copy.24
  237.5 0.2 copy.25
  237.7 0.1 copy.28
  237.8 38.4 %all-to-all-done.1 = bf16[512,64,24]{0,2,1:T(8,128)(2,1)} async-done(((bf16[512,64,24]{0,2,1:T(8,128)(2,1)}), bf16[512,64,24]{0,2,1:T(8,128)(2,1)}, u32[]{:S(2)}, u32[]{:S(2)}) %all-to-all-start.1) | async-done | bytes 1572896 | tf_op jit(solution)/shard_map/all_to_all | solution.py:65
  276.2 3.6 %gather_fusion.1 = bf16[512,512]{1,0:T(8,128)(2,1)S(1)} fusion(bf16[512,1536]{0,1:T(8,128)(2,1)} %bitcast.12, s32[1024]{0:T(1024)S(1)} %pad_clamp_fusion.1), kind=kCustom, calls=%fused_computation.1 | custom fusion | bytes 1050624 | tf_op jit(solution)/shard_map/jit(_take)/gather | solution.py:68
  279.8 0.2 gather.11
  280.0 2.9 %multiply_reduce_fusion = bf16[512,256]{0,1:T(8,128)(2,1)} fusion(bf16[512,256,2]{0,2,1:T(2,128)(2,1)S(1)} %gather.11, pred[256,2]{1,0:T(8,128)(4,1)S(1)} %copy.25, f32[256,2]{1,0:T(8,128)S(1)} %copy.28), kind=kLoop, calls=%fused_computation.19 | loop fusion | flops 917504 | bytes 788992 | tf_op jit(solution)/shard_map/reduce_sum | solution.py:69
  (19 shorter events, 0.2 us)
Async XLA Ops:
  6.5 140.4 %copy-start = (bf16[1,512,2048]{2,1,0:T(8,128)(2,1)S(1)}, bf16[1,512,2048]{2,1,0:T(8,128)(2,1)}, u32[]{:S(2)}) copy-start(bf16[1,512,2048]{2,1,0:T(8,128)(2,1)} %param.13) | copy-start | bytes 6291460
  6.5 7.9 %copy-start.1 = (bf16[256,2048]{1,0:T(8,128)(2,1)S(1)}, bf16[256,2048]{1,0:T(8,128)(2,1)}, u32[]{:S(2)}) copy-start(bf16[256,2048]{1,0:T(8,128)(2,1)} %param.7) | copy-start | bytes 3145732
  6.5 131.9 %all-gather.2.cloned.1.call-start = ((), (), s32[]{:S(2)}) async-start(), calls=%async_computation.3 | async-start | bytes 7864320 | tf_op jit(solution)/shard_map/all_gather | solution.py:45
  73.2 153.1 %reduce-scatter.2.cloned.1.call-start = ((), (), s32[]{:S(2)}) async-start(), calls=%async_computation.4 | async-start | bytes 7864320 | tf_op jit(solution)/shard_map/reduce_scatter | solution.py:62
  158.8 78.6 %copy-start.2 = (s32[256,2]{0,1:T(2,128)S(1)}, s32[256,2]{0,1:T(2,128)}, u32[]{:S(2)}) copy-start(s32[256,2]{0,1:T(2,128)} %param.8) | copy-start | bytes 6148
  158.8 78.8 %copy-start.3 = (f32[256,2]{0,1:T(2,128)S(1)}, f32[256,2]{0,1:T(2,128)}, u32[]{:S(2)}) copy-start(f32[256,2]{0,1:T(2,128)} %param.9) | copy-start | bytes 6148
  226.3 49.9 %all-to-all-start.1 = ((bf16[512,64,24]{0,2,1:T(8,128)(2,1)}), bf16[512,64,24]{0,2,1:T(8,128)(2,1)}, u32[]{:S(2)}, u32[]{:S(2)}) async-start(bf16[512,64,24]{0,2,1:T(8,128)(2,1)} %bitcast.48), calls=%async_computation.2 | async-start | bytes 3145728 | tf_op jit(solution)/shard_map/all_to_all | solution.py:65
Sparse Core Ops, SparseCore 0:
  73.4 65.0 all-gather.1
  159.0 67.3 reduce-scatter.1
where the time goes:
time: 290 us
  waiting for transfers between devices  171 us (59%)
  blocking collectives  52.3 us (18%)
  matrix products  20.4 us (7%)
  local copies, waits for them, and re-layouts  14 us (5%)
  between operations  13.6 us (5%)
  starting transfers between devices  11 us (4%)
  other arithmetic  7.57 us (3%)
    reduce_scatter x1, waiting for transfers between devices, shards(): lax.psum_scatter(jnp.stack(term_list, axis=2).astype(jnp.bfloat16), 'tp',...  67.5 us
    all_gather x1, waiting for transfers between devices, shards(): shard_piece = lax.all_gather(received, 'tp', axis=3, tiled=True)  65.1 us
    all_to_all x1, blocking collectives, shards(): lax.all_to_all(send_rows, 'ep', split_axis=0, concat_axis=0, tiled=True)  52.3 us
    all_to_all x1, waiting for transfers between devices, shards(): lax.all_to_all(summed.reshape(quarter, experts * capacity), 'ep', split_a...  38.4 us
    dot_general x1, matrix products, shards(): lax.dot_general(weight_rows, activated[member], (((0,), (1,)), ((), ())),...  11.9 us
    all_to_all x1, starting transfers between devices, shards(): lax.all_to_all(summed.reshape(quarter, experts * capacity), 'ep', split_a...  10.9 us
    dot_general x1, matrix products, shards(): jnp.dot(row_block, gate_rows, preferred_element_type=jnp.float32)  8.52 us
  transfers between devices with their start and end apart: 3, of which 3 were waited for; matrix products, arithmetic and copies ran while one was open for 0% of the time, Pallas kernels for 0%

commit v1 on v0

v1 whole, which is shorter than its diff:
```python
import jax
import jax.numpy as jnp
from jax import lax
from jax.experimental import pallas as pl
from jax.experimental.pallas import tpu as pltpu
from jax.sharding import PartitionSpec as P


NORM_EPS = 1e-06
CLAMP_LIMIT = 7.0
SWISH_SCALE = 1.702
SLOTS = 8
VMEM_BYTES = 20 << 20
INTERPRET = False


def activate(gate_sum, up_sum):
    gate_cut = jnp.minimum(gate_sum, CLAMP_LIMIT)
    up_cut = jnp.clip(up_sum, -CLAMP_LIMIT, CLAMP_LIMIT)
    return ((up_cut + 1.0) * gate_cut * jax.nn.sigmoid(SWISH_SCALE * gate_cut)).astype(jnp.bfloat16)


def dot(a, b):
    return jnp.dot(a, b, preferred_element_type=jnp.float32)


def first_body(own, near_a, near_b, gate_w, up_w, gate_out, up_out):
    rows, quarter = own.shape
    step = rows // 2
    for top in range(0, rows, step):
        at = slice(top, top + step)
        for w, out in ((gate_w, gate_out), (up_w, up_out)):
            total = dot(own[at, :], w[:quarter, :])
            total = total + dot(near_a[at, :], w[quarter : 2 * quarter, :])
            out[at, :] = total + dot(near_b[at, :], w[2 * quarter :, :])


def last_body(gate_sum, up_sum, far_a, far_b, gate_w, up_w, down_far, down_near, *outs):
    across_a, across_b, for_a, for_b, kept = outs
    half, quarter = far_a.shape
    for part, (far, across) in enumerate(((far_a, across_a), (far_b, across_b))):
        at = slice(part * half, (part + 1) * half)
        rows = far[...]
        gate = gate_sum[at, :] + dot(rows, gate_w[...])
        up = up_sum[at, :] + dot(rows, up_w[...])
        active = activate(gate, up)
        across[...] = dot(active, down_far[...]).astype(jnp.bfloat16)
        for k, out in enumerate((for_a, for_b, kept)):
            block = down_near[:, k * quarter : (k + 1) * quarter]
            out[at, :] = dot(active, block).astype(jnp.bfloat16)


def first_call(own, near_a, near_b, gate_w, up_w):
    rows, hidden = own.shape[0], gate_w.shape[1]
    shape = jax.ShapeDtypeStruct((rows, hidden), jnp.float32)
    return pl.pallas_call(
        first_body,
        out_shape=(shape, shape),
        compiler_params=pltpu.CompilerParams(vmem_limit_bytes=VMEM_BYTES),
        cost_estimate=pl.CostEstimate(
            flops=4 * rows * gate_w.shape[0] * hidden, bytes_accessed=8 << 20, transcendentals=0
        ),
        interpret=INTERPRET,
        name="first",
    )(own, near_a, near_b, gate_w, up_w)


def last_call(gate_sum, up_sum, far_a, far_b, gate_w, up_w, down_far, down_near):
    rows, hidden = gate_sum.shape
    half, quarter = far_a.shape
    small = jax.ShapeDtypeStruct((half, quarter), jnp.bfloat16)
    full = jax.ShapeDtypeStruct((rows, quarter), jnp.bfloat16)
    return pl.pallas_call(
        last_body,
        out_shape=(small, small, full, full, full),
        compiler_params=pltpu.CompilerParams(vmem_limit_bytes=VMEM_BYTES),
        cost_estimate=pl.CostEstimate(
            flops=12 * rows * quarter * hidden, bytes_accessed=8 << 20, transcendentals=rows * hidden
        ),
        interpret=INTERPRET,
        name="last",
    )(gate_sum, up_sum, far_a, far_b, gate_w, up_w, down_far, down_near)


def merge_body(for_a, for_b, via_a, via_b, sum_a, sum_b):
    half = via_a.shape[0]
    f32 = jnp.float32
    sum_a[:half, :] = for_a[:half, :]
    sum_a[half:, :] = (for_a[half:, :].astype(f32) + via_b[...].astype(f32)).astype(jnp.bfloat16)
    sum_b[:half, :] = (for_b[:half, :].astype(f32) + via_a[...].astype(f32)).astype(jnp.bfloat16)
    sum_b[half:, :] = for_b[half:, :]


def merge_call(for_a, for_b, via_a, via_b):
    shape = jax.ShapeDtypeStruct(for_a.shape, for_a.dtype)
    return pl.pallas_call(
        merge_body,
        out_shape=(shape, shape),
        compiler_params=pltpu.CompilerParams(vmem_limit_bytes=8 << 20),
        cost_estimate=pl.CostEstimate(flops=1 << 20, bytes_accessed=3 << 20, transcendentals=0),
        interpret=INTERPRET,
        name="merge",
    )(for_a, for_b, via_a, via_b)


def layer(tokens, expert_ids, route_weight, norm_gain, expert_gate, expert_up, expert_down):
    groups = lax.axis_size("ep")
    tp_count = lax.axis_size("tp")
    tok_count, width = tokens.shape
    top_count = expert_ids.shape[1]
    capacity = min(tok_count, 3 * tok_count * top_count // groups)
    quarter = width // tp_count
    bf16 = jnp.bfloat16
    me = lax.axis_index("tp")
    mate_a = me + 1 - 2 * (me % 2)
    mate_b = tp_count - 1 - me
    opposite = (me + 2) % tp_count
    even = [(i, i ^ 1) for i in range(tp_count)]
    odd = [(i, tp_count - 1 - i) for i in range(tp_count)]

    values = tokens.astype(jnp.float32)
    scale = lax.rsqrt(jnp.mean(values * values, axis=-1, keepdims=True) + NORM_EPS)
    own_values = lax.dynamic_slice_in_dim(tokens, me * quarter, quarter, 1).astype(jnp.float32)
    own_gain = lax.dynamic_slice_in_dim(norm_gain, me * quarter, quarter, 0)
    normed = (own_values * scale * own_gain).astype(bf16)

    experts = jnp.arange(groups, dtype=jnp.int32)[:, None]
    ids = expert_ids.T
    weights = route_weight.T
    named = [ids[k][None, :] == experts for k in range(top_count)]
    member = named[0]
    for k in range(1, top_count):
        member = member | named[k]
    earlier = (
        jnp.arange(tok_count, dtype=jnp.int32)[:, None] < jnp.arange(tok_count, dtype=jnp.int32)[None, :]
    ).astype(bf16)
    rank = dot(member.astype(bf16), earlier).astype(jnp.int32)
    rank = jnp.where(member, rank, -1)
    weight = sum(jnp.where(named[k], weights[k][None, :], 0.0) for k in range(top_count))
    weight_high = lax.reduce_precision(weight, 8, 7)
    weight_low = weight - weight_high

    gate_w, up_w, down_w = expert_gate[0], expert_up[0], expert_down[0]

    def rows_of(w, blocks):
        return jnp.concatenate([lax.dynamic_slice_in_dim(w, b * quarter, quarter, 0) for b in blocks], axis=0)

    def cols_of(w, blocks):
        return jnp.concatenate([lax.dynamic_slice_in_dim(w, b * quarter, quarter, 1) for b in blocks], axis=1)

    near_blocks = (me, mate_a, mate_b)
    gate_near, up_near = rows_of(gate_w, near_blocks), rows_of(up_w, near_blocks)
    gate_far, up_far = rows_of(gate_w, (opposite,)), rows_of(up_w, (opposite,))
    down_far, down_near = cols_of(down_w, (opposite,)), cols_of(down_w, (mate_a, mate_b, me))

    chosen_of, sends = [], []
    for first in range(0, capacity, SLOTS):
        slots = first + jnp.arange(SLOTS, dtype=jnp.int32)
        chosen = (rank[:, None, :] == slots[None, :, None]).reshape(groups * SLOTS, tok_count)
        chosen_of.append(chosen)
        sends.append(dot(chosen.astype(bf16), normed).astype(bf16).reshape(groups, SLOTS, quarter))

    combined = jnp.zeros((tok_count, quarter), jnp.float32)
    for chunk, first in enumerate(range(0, capacity, SLOTS)):

        def exchange(x):
            return lax.all_to_all(x, "ep", split_axis=0, concat_axis=0, tiled=True)

        def shift(x, name):
            return lax.ppermute(x, "tp", even if name[1] == "r" else odd)

        chosen, send = chosen_of[chunk], sends[chunk]
        rows = groups * SLOTS
        half = rows // 2
        own = exchange(send).reshape(rows, quarter)
        if chunk == 0:
            own, sends, gate_near, up_near, gate_far, up_far, down_far, down_near = lax.optimization_barrier(
                (own, sends, gate_near, up_near, gate_far, up_far, down_far, down_near)
            )
        near_a = shift(own, "nr")
        near_b = shift(own, "nl")
        far_a = shift(near_b[:half], "fr")
        far_b = shift(near_a[half:], "fl")
        gate_sum, up_sum = first_call(own, near_a, near_b, gate_near, up_near)
        across_a, across_b, for_a, for_b, kept = last_call(
            gate_sum, up_sum, far_a, far_b, gate_far, up_far, down_far, down_near
        )
        f32 = jnp.float32
        via_a = shift(across_a, "ar")
        via_b = shift(across_b, "al")
        for_a, for_b = merge_call(for_a, for_b, via_a, via_b)
        got_a = shift(for_a, "br")
        got_b = shift(for_b, "bl")
        total = kept.astype(f32) + got_a.astype(f32) + got_b.astype(f32)
        result = total.astype(bf16).reshape(groups, SLOTS, quarter)
        returned = exchange(result).reshape(rows, quarter)
        for part in (weight_high, weight_low):
            table = jnp.where(chosen.reshape(groups, SLOTS, tok_count), part[:, None, :], 0.0)
            table = table.reshape(rows, tok_count).astype(bf16)
            combined = combined + lax.dot_general(
                table, returned, (((0,), (0,)), ((), ())), preferred_element_type=jnp.float32
            )
    return combined.astype(bf16)


def solution(mesh):
    return jax.shard_map(
        layer,
        mesh=mesh,
        in_specs=(
            P("ep", None),
            P("ep", None),
            P("ep", None),
            P(),
            P("ep", None, "tp"),
            P("ep", None, "tp"),
            P("ep", "tp", None),
        ),
        out_specs=P("ep", "tp"),
        check_vma=False,
    )
```

time: 290 us -> 230 us (0.79)
  waiting for transfers between devices: 171 us -> 85.6 us
  starting transfers between devices: 11 us -> 84.7 us
  blocking collectives: 52.3 us -> 0 us
  Pallas kernels: 0 us -> 19.5 us
  between operations: 13.6 us -> 0.46 us
  matrix products: 20.4 us -> 9.86 us
  local copies, waits for them, and re-layouts: 14 us -> 21.5 us
    reduce_scatter x1 -> x0, waiting for transfers between devices: 67.5 us -> none  [shards(): lax.psum_scatter(jnp.stack(term_list, axis=2).astype(jnp.bfloat16), 'tp',...]
    all_gather x1 -> x0, waiting for transfers between devices: 65.1 us -> none  [shards(): shard_piece = lax.all_gather(received, 'tp', axis=3, tiled=True)]
    all_to_all x1 -> x0, blocking collectives: 52.3 us -> none  [shards(): lax.all_to_all(send_rows, 'ep', split_axis=0, concat_axis=0, tiled=True)]
    all_to_all x1 -> x6, starting transfers between devices: 10.9 us -> 63.1 us  [exchange(): return lax.all_to_all(x, 'ep', split_axis=0, concat_axis=0, tiled=True)]
    ppermute x0 -> x24, waiting for transfers between devices: none -> 28.9 us  [shift(): return lax.ppermute(x, 'tp', even if name[1] == 'r' else odd)]
    ppermute x0 -> x24, starting transfers between devices: none -> 21.6 us  [shift(): return lax.ppermute(x, 'tp', even if name[1] == 'r' else odd)]
    pallas_call x0 -> x9, Pallas kernels: none -> 19.5 us  [the longest x3 9.33 us: first_call(): pl.pallas_call(first_body, out_shape=(shape, shape), compiler_params=pltp...]
    all_to_all x1 -> x6, waiting for transfers between devices: 38.4 us -> 56.7 us  [exchange(): return lax.all_to_all(x, 'ep', split_axis=0, concat_axis=0, tiled=True)]
  transfers between devices with their start and end apart: 3 -> 30, of which waited for: 3 -> 10; matrix products, arithmetic and copies ran while one was open for 0% -> 8% of each run, Pallas kernels for 0% -> 9%
where the time goes in v1:
time: 230 us; the launch traced here: 229 us
  waiting for transfers between devices  85.6 us (37%)
  starting transfers between devices  84.7 us (37%)
  local copies, waits for them, and re-layouts  21.5 us (9%)
  Pallas kernels  19.5 us (8%)
  matrix products  9.86 us (4%)
  other arithmetic  7.39 us (3%)
    all_to_all x6, starting transfers between devices, exchange(): return lax.all_to_all(x, 'ep', split_axis=0, concat_axis=0, tiled=True)  63.1 us
    all_to_all x6, waiting for transfers between devices, exchange(): return lax.all_to_all(x, 'ep', split_axis=0, concat_axis=0, tiled=True)  56.7 us
    ppermute x24, waiting for transfers between devices, shift(): return lax.ppermute(x, 'tp', even if name[1] == 'r' else odd)  28.9 us
    ppermute x24, starting transfers between devices, shift(): return lax.ppermute(x, 'tp', even if name[1] == 'r' else odd)  21.6 us
    unnamed x58, local copies, waits for them, and re-layouts  11.7 us
    pallas_call x3, Pallas kernels, first_call(): pl.pallas_call(first_body, out_shape=(shape, shape), compiler_params=pltp...  9.33 us
    pallas_call x3, Pallas kernels, last_call(): pl.pallas_call(last_body, out_shape=(small, small, full, full, full), com...  7.8 us
    dot_general x6, matrix products, layer(): lax.dot_general(table, returned, (((0,), (0,)), ((), ())), preferred_elem...  5.12 us
  transfers between devices with their start and end apart: 30, of which 10 were waited for; matrix products, arithmetic and copies ran while one was open for 8% of the time, Pallas kernels for 9%

profile of v1, /device:TPU:1, one launch (start us, length us, event | category | flops | bytes accessed | tf_op | source)
XLA Modules:
  0.0 229.0 jit_solution(8363267555008108047)
XLA Ops:
  0.0 1.6 multiply_reduce_fusion
  3.5 2.2 fusion
  5.7 13.3 %all-to-all-start = ((bf16[64,8,512]{2,1,0:T(8,128)(2,1)}), bf16[64,8,512]{2,1,0:T(8,128)(2,1)}, u32[]{:S(2)}, u32[]{:S(2)}) async-start(bf16[64,8,512]{2,1,0:T(8,128)(2,1)} %fusion), calls=%async_computation | async-start | bytes 1048576 | tf_op jit(solution)/shard_map/all_to_all | solution.py:167
  27.0 9.6 %all-to-all-done = bf16[64,8,512]{2,1,0:T(8,128)(2,1)} async-done(((bf16[64,8,512]{2,1,0:T(8,128)(2,1)}), bf16[64,8,512]{2,1,0:T(8,128)(2,1)}, u32[]{:S(2)}, u32[]{:S(2)}) %all-to-all-start) | async-done | bytes 524320 | tf_op jit(solution)/shard_map/all_to_all | solution.py:167
  36.6 5.9 %all-to-all-start.4 = ((bf16[64,8,512]{2,1,0:T(8,128)(2,1)}), bf16[64,8,512]{2,1,0:T(8,128)(2,1)}, u32[]{:S(2)}, u32[]{:S(2)}) async-start(bf16[64,8,512]{2,1,0:T(8,128)(2,1)} %fusion.2), calls=%async_computation.4 | async-start | bytes 1048576 | tf_op jit(solution)/shard_map/all_to_all | solution.py:167
  42.5 2.6 %collective-permute-start.1 = (bf16[512,512]{1,0:T(8,128)(2,1)}, bf16[512,512]{1,0:T(8,128)(2,1)}, u32[]{:S(2)}, u32[]{:S(2)}) collective-permute-start(bf16[512,512]{1,0:T(8,128)(2,1)} %bitcast.8.own), channel_id=1, source_target_pairs={{0,3},{1,2},{2,1},{3,0},{4,7},{5,6},{6,5},{7,4},{8,11},{9,10},{10,... | collective-permute-start | bytes 1572872 | tf_op jit(solution)/shard_map/ppermute | solution.py:170
  45.1 15.0 %all-to-all-done.4 = bf16[64,8,512]{2,1,0:T(8,128)(2,1)} async-done(((bf16[64,8,512]{2,1,0:T(8,128)(2,1)}), bf16[64,8,512]{2,1,0:T(8,128)(2,1)}, u32[]{:S(2)}, u32[]{:S(2)}) %all-to-all-start.4) | async-done | bytes 524320 | tf_op jit(solution)/shard_map/all_to_all | solution.py:167
  60.1 5.9 %all-to-all-start.2 = ((bf16[64,8,512]{2,1,0:T(8,128)(2,1)}), bf16[64,8,512]{2,1,0:T(8,128)(2,1)}, u32[]{:S(2)}, u32[]{:S(2)}) async-start(bf16[64,8,512]{2,1,0:T(8,128)(2,1)} %fusion.1), calls=%async_computation.2 | async-start | bytes 1048576 | tf_op jit(solution)/shard_map/all_to_all | solution.py:167
  69.2 1.9 collective-permute-start.3
  73.4 3.3 %first.3 = (f32[512,512]{1,0:T(8,128)S(1)}, f32[512,512]{1,0:T(8,128)S(1)}) custom-call(bf16[512,512]{1,0:T(8,128)(2,1)} %bitcast.8.own, bf16[512,512]{1,0:T(8,128)(2,1)} %collective-permute-done.near_a, bf16[512,512]{1,0:T(8,128)(2,1)} %collective-permute-done.1.near_b, bf16[1536,512]{1,0:T(8,128)(2,1)S(1)} %pad_maximum_fusion.gate_w, ...), custom_call_target="tpu_custom_call" | custom-call | flops 1610612736 | bytes 8388608 | tf_op jit(solution)/shard_map/first/pallas_call | solution.py:56
  77.7 2.1 last.3
  80.6 1.8 collective-permute-start.5
  82.4 6.4 %collective-permute-done.17.near_b = bf16[512,512]{1,0:T(8,128)(2,1)S(1)} collective-permute-done((bf16[512,512]{1,0:T(8,128)(2,1)}, bf16[512,512]{1,0:T(8,128)(2,1)S(1)}, u32[]{:S(2)}, u32[]{:S(2)}) %collective-permute-start.17) | collective-permute-done | bytes 524320 | tf_op jit(solution)/shard_map/ppermute | solution.py:170
  89.6 5.1 %collective-permute-done.4.via_a = bf16[256,512]{1,0:T(8,128)(2,1)S(1)} collective-permute-done((bf16[256,512]{1,0:T(8,128)(2,1)S(1)}, bf16[256,512]{1,0:T(8,128)(2,1)S(1)}, u32[]{:S(2)}, u32[]{:S(2)}) %collective-permute-start.4) | collective-permute-done | bytes 262176 | tf_op jit(solution)/shard_map/ppermute | solution.py:170
  96.2 1.8 collective-permute-start.7
  100.4 1.8 collective-permute-start.9
  105.7 2.9 %first.5 = (f32[512,512]{1,0:T(8,128)S(1)}, f32[512,512]{1,0:T(8,128)S(1)}) custom-call(bf16[512,512]{1,0:T(8,128)(2,1)} %bitcast.30.own, bf16[512,512]{1,0:T(8,128)(2,1)S(1)} %copy-done.23, bf16[512,512]{1,0:T(8,128)(2,1)S(1)} %copy-done.21, bf16[1536,512]{1,0:T(8,128)(2,1)S(1)} %pad_maximum_fusion.gate_w, bf16[1536,512]{1,0:T(8,128)(2,1)S(1)} %copy-done.1), custom_call_target="tpu_custom_call" | custom-call | flops 1610612736 | bytes 8388608 | tf_op jit(solution)/shard_map/first/pallas_call | solution.py:56
  108.6 4.3 %collective-permute-done.19.far_b = bf16[256,512]{1,0:T(8,128)(2,1)} collective-permute-done((bf16[256,512]{1,0:T(8,128)(2,1)}, bf16[256,512]{1,0:T(8,128)(2,1)}, u32[]{:S(2)}, u32[]{:S(2)}) %collective-permute-start.19) | collective-permute-done | bytes 262176 | tf_op jit(solution)/shard_map/ppermute | solution.py:170
  112.9 3.7 %last.5 = (bf16[256,512]{1,0:T(8,128)(2,1)}, bf16[256,512]{1,0:T(8,128)(2,1)}, bf16[512,512]{1,0:T(8,128)(2,1)S(1)}, bf16[512,512]{1,0:T(8,128)(2,1)S(1)}, bf16[512,512]{1,0:T(8,128)(2,1)S(1)}) custom-call(f32[512,512]{1,0:T(8,128)S(1)} %get-tuple-element.68.gate_sum, f32[512,512]{1,0:T(8,128)S(1)} %get-tuple-element.69.up_sum, ...), custom_call_target="tpu_custom_call" | custom-call | flops 1610612736 | bytes 8388608 | tf_op jit(solution)/shard_map/last/pallas_call | solution.py:73
  119.0 1.8 collective-permute-start.21
  120.9 2.2 fusion.14
  123.1 20.0 %all-to-all-start.1 = ((bf16[64,8,512]{2,1,0:T(8,128)(2,1)}), bf16[64,8,512]{2,1,0:T(8,128)(2,1)}, u32[]{:S(2)}, u32[]{:S(2)}) async-start(bf16[64,8,512]{2,1,0:T(8,128)(2,1)} %fusion.14), calls=%async_computation.1 | async-start | bytes 1048576 | tf_op jit(solution)/shard_map/all_to_all | solution.py:167
  150.4 1.8 collective-permute-start.23
  152.2 3.1 %first.4 = (f32[512,512]{1,0:T(8,128)S(1)}, f32[512,512]{1,0:T(8,128)S(1)}) custom-call(bf16[512,512]{1,0:T(8,128)(2,1)} %bitcast.26.own, bf16[512,512]{1,0:T(8,128)(2,1)} %collective-permute-done.8.near_a, bf16[512,512]{1,0:T(8,128)(2,1)} %collective-permute-done.9.near_b, bf16[1536,512]{1,0:T(8,128)(2,1)S(1)} %pad_maximum_fusion.gate_w, ...), custom_call_target="tpu_custom_call" | custom-call | flops 1610612736 | bytes 8388608 | tf_op jit(solution)/shard_map/first/pallas_call | solution.py:56
  155.4 2.1 last.4
  159.0 9.0 %collective-permute-done.12.via_a = bf16[256,512]{1,0:T(8,128)(2,1)S(1)} collective-permute-done((bf16[256,512]{1,0:T(8,128)(2,1)S(1)}, bf16[256,512]{1,0:T(8,128)(2,1)S(1)}, u32[]{:S(2)}, u32[]{:S(2)}) %collective-permute-start.12) | collective-permute-done | bytes 262176 | tf_op jit(solution)/shard_map/ppermute | solution.py:170
  167.9 3.2 %collective-permute-done.13.via_b = bf16[256,512]{1,0:T(8,128)(2,1)S(1)} collective-permute-done((bf16[256,512]{1,0:T(8,128)(2,1)S(1)}, bf16[256,512]{1,0:T(8,128)(2,1)S(1)}, u32[]{:S(2)}, u32[]{:S(2)}) %collective-permute-start.13) | collective-permute-done | bytes 262176 | tf_op jit(solution)/shard_map/ppermute | solution.py:170
  172.6 12.4 %all-to-all-start.5 = ((bf16[64,8,512]{2,1,0:T(8,128)(2,1)}), bf16[64,8,512]{2,1,0:T(8,128)(2,1)S(1)}, u32[]{:S(2)}, u32[]{:S(2)}) async-start(bf16[64,8,512]{2,1,0:T(8,128)(2,1)} %fusion.16), calls=%async_computation.5 | async-start | bytes 1048576 | tf_op jit(solution)/shard_map/all_to_all | solution.py:167
  187.5 15.2 %all-to-all-done.5 = bf16[64,8,512]{2,1,0:T(8,128)(2,1)S(1)} async-done(((bf16[64,8,512]{2,1,0:T(8,128)(2,1)}), bf16[64,8,512]{2,1,0:T(8,128)(2,1)S(1)}, u32[]{:S(2)}, u32[]{:S(2)}) %all-to-all-start.5) | async-done | bytes 524320 | tf_op jit(solution)/shard_map/all_to_all | solution.py:167
  202.7 5.7 %all-to-all-start.3 = ((bf16[64,8,512]{2,1,0:T(8,128)(2,1)}), bf16[64,8,512]{2,1,0:T(8,128)(2,1)S(1)}, u32[]{:S(2)}, u32[]{:S(2)}) async-start(bf16[64,8,512]{2,1,0:T(8,128)(2,1)} %fusion.15), calls=%async_computation.3 | async-start | bytes 1048576 | tf_op jit(solution)/shard_map/all_to_all | solution.py:167
  209.2 16.9 %all-to-all-done.3 = bf16[64,8,512]{2,1,0:T(8,128)(2,1)S(1)} async-done(((bf16[64,8,512]{2,1,0:T(8,128)(2,1)}), bf16[64,8,512]{2,1,0:T(8,128)(2,1)S(1)}, u32[]{:S(2)}, u32[]{:S(2)}) %all-to-all-start.3) | async-done | bytes 524320 | tf_op jit(solution)/shard_map/all_to_all | solution.py:167
  226.9 2.1 fusion.8
  (133 shorter events, 42.0 us)
Async XLA Ops:
  0.0 19.3 %copy-start.24 = (bf16[256,2048]{1,0:T(8,128)(2,1)S(1)}, bf16[256,2048]{1,0:T(8,128)(2,1)}, u32[]{:S(2)}) copy-start(bf16[256,2048]{1,0:T(8,128)(2,1)} %param.7) | copy-start | bytes 3145732
  1.6 20.1 %copy-start.27 = (bf16[1,2048,512]{2,1,0:T(8,128)(2,1)S(1)}, bf16[1,2048,512]{2,1,0:T(8,128)(2,1)}, u32[]{:S(2)}) copy-start(bf16[1,2048,512]{2,1,0:T(8,128)(2,1)} %param.11) | copy-start | bytes 6291460
  5.7 30.9 %all-to-all-start = ((bf16[64,8,512]{2,1,0:T(8,128)(2,1)}), bf16[64,8,512]{2,1,0:T(8,128)(2,1)}, u32[]{:S(2)}, u32[]{:S(2)}) async-start(bf16[64,8,512]{2,1,0:T(8,128)(2,1)} %fusion), calls=%async_computation | async-start | bytes 1048576 | tf_op jit(solution)/shard_map/all_to_all | solution.py:167
  36.6 23.5 %all-to-all-start.4 = ((bf16[64,8,512]{2,1,0:T(8,128)(2,1)}), bf16[64,8,512]{2,1,0:T(8,128)(2,1)}, u32[]{:S(2)}, u32[]{:S(2)}) async-start(bf16[64,8,512]{2,1,0:T(8,128)(2,1)} %fusion.2), calls=%async_computation.4 | async-start | bytes 1048576 | tf_op jit(solution)/shard_map/all_to_all | solution.py:167
  42.5 23.5 %collective-permute-start.1 = (bf16[512,512]{1,0:T(8,128)(2,1)}, bf16[512,512]{1,0:T(8,128)(2,1)}, u32[]{:S(2)}, u32[]{:S(2)}) collective-permute-start(bf16[512,512]{1,0:T(8,128)(2,1)} %bitcast.8.own), channel_id=1, source_target_pairs={{0,3},{1,2},{2,1},{3,0},{4,7},{5,6},{6,5},{7,4},{8,11},{9,10},{10,... | collective-permute-start | bytes 1572872 | tf_op jit(solution)/shard_map/ppermute | solution.py:170
  45.1 23.2 %collective-permute-start = (bf16[512,512]{1,0:T(8,128)(2,1)}, bf16[512,512]{1,0:T(8,128)(2,1)}, u32[]{:S(2)}, u32[]{:S(2)}) collective-permute-start(bf16[512,512]{1,0:T(8,128)(2,1)} %bitcast.8.own), channel_id=1, source_target_pairs={{0,1},{1,0},{2,3},{3,2},{4,5},{5,4},{6,7},{7,6},{8,9},{9,8},{10,11... | collective-permute-start | bytes 1572872 | tf_op jit(solution)/shard_map/ppermute | solution.py:170
  60.1 40.3 %all-to-all-start.2 = ((bf16[64,8,512]{2,1,0:T(8,128)(2,1)}), bf16[64,8,512]{2,1,0:T(8,128)(2,1)}, u32[]{:S(2)}, u32[]{:S(2)}) async-start(bf16[64,8,512]{2,1,0:T(8,128)(2,1)} %fusion.1), calls=%async_computation.2 | async-start | bytes 1048576 | tf_op jit(solution)/shard_map/all_to_all | solution.py:167
  67.0 9.8 %collective-permute-start.2 = (bf16[256,512]{1,0:T(8,128)(2,1)S(1)}, bf16[256,512]{1,0:T(8,128)(2,1)S(1)}, u32[]{:S(2)}, u32[]{:S(2)}) collective-permute-start(bf16[256,512]{1,0:T(8,128)(2,1)S(1)} %slice.44), channel_id=1, source_target_pairs={{0,1},{1,0},{2,3},{3,2},{4,5},{5,4},{6,7},{7,6},{8,9},{9,8},{10,11... | collective-permute-start | bytes 786440 | tf_op jit(solution)/shard_map/ppermute | solution.py:170
  69.2 8.5 %collective-permute-start.3 = (bf16[256,512]{1,0:T(8,128)(2,1)S(1)}, bf16[256,512]{1,0:T(8,128)(2,1)S(1)}, u32[]{:S(2)}, u32[]{:S(2)}) collective-permute-start(bf16[256,512]{1,0:T(8,128)(2,1)S(1)} %slice.45), channel_id=1, source_target_pairs={{0,3},{1,2},{2,1},{3,0},{4,7},{5,6},{6,5},{7,4},{8,11},{9,10},{10,... | collective-permute-start | bytes 786440 | tf_op jit(solution)/shard_map/ppermute | solution.py:170
  71.1 17.7 %collective-permute-start.17 = (bf16[512,512]{1,0:T(8,128)(2,1)}, bf16[512,512]{1,0:T(8,128)(2,1)S(1)}, u32[]{:S(2)}, u32[]{:S(2)}) collective-permute-start(bf16[512,512]{1,0:T(8,128)(2,1)} %bitcast.30.own), channel_id=1, source_target_pairs={{0,3},{1,2},{2,1},{3,0},{4,7},{5,6},{6,5},{7,4},{8,11},{9,10},{10,... | collective-permute-start | bytes 1572872 | tf_op jit(solution)/shard_map/ppermute | solution.py:170
  76.7 21.3 %collective-permute-start.16 = (bf16[512,512]{1,0:T(8,128)(2,1)}, bf16[512,512]{1,0:T(8,128)(2,1)S(1)}, u32[]{:S(2)}, u32[]{:S(2)}) collective-permute-start(bf16[512,512]{1,0:T(8,128)(2,1)} %bitcast.30.own), channel_id=1, source_target_pairs={{0,1},{1,0},{2,3},{3,2},{4,5},{5,4},{6,7},{7,6},{8,9},{9,8},{10,11... | collective-permute-start | bytes 1572872 | tf_op jit(solution)/shard_map/ppermute | solution.py:170
  79.8 14.9 %collective-permute-start.4 = (bf16[256,512]{1,0:T(8,128)(2,1)S(1)}, bf16[256,512]{1,0:T(8,128)(2,1)S(1)}, u32[]{:S(2)}, u32[]{:S(2)}) collective-permute-start(bf16[256,512]{1,0:T(8,128)(2,1)S(1)} %get-tuple-element.53), channel_id=1, source_target_pairs={{0,1},{1,0},{2,3},{3,2},{4,5},{5,4},{6,7},{7,6},{8,9},{9,8},{10,11... | collective-permute-start | bytes 786440 | tf_op jit(solution)/shard_map/ppermute | solution.py:170
  80.6 14.1 %collective-permute-start.5 = (bf16[256,512]{1,0:T(8,128)(2,1)S(1)}, bf16[256,512]{1,0:T(8,128)(2,1)S(1)}, u32[]{:S(2)}, u32[]{:S(2)}) collective-permute-start(bf16[256,512]{1,0:T(8,128)(2,1)S(1)} %get-tuple-element.54), channel_id=1, source_target_pairs={{0,3},{1,2},{2,1},{3,0},{4,7},{5,6},{6,5},{7,4},{8,11},{9,10},{10,... | collective-permute-start | bytes 786440 | tf_op jit(solution)/shard_map/ppermute | solution.py:170
  89.6 12.6 %collective-permute-start.18 = (bf16[256,512]{1,0:T(8,128)(2,1)}, bf16[256,512]{1,0:T(8,128)(2,1)S(1)}, u32[]{:S(2)}, u32[]{:S(2)}) collective-permute-start(bf16[256,512]{1,0:T(8,128)(2,1)} %slice.48), channel_id=1, source_target_pairs={{0,1},{1,0},{2,3},{3,2},{4,5},{5,4},{6,7},{7,6},{8,9},{9,8},{10,11... | collective-permute-start | bytes 786440 | tf_op jit(solution)/shard_map/ppermute | solution.py:170
  95.9 23.2 %collective-permute-start.6 = (bf16[512,512]{1,0:T(8,128)(2,1)}, bf16[512,512]{1,0:T(8,128)(2,1)}, u32[]{:S(2)}, u32[]{:S(2)}) collective-permute-start(bf16[512,512]{1,0:T(8,128)(2,1)} %get-tuple-element.55), channel_id=1, source_target_pairs={{0,1},{1,0},{2,3},{3,2},{4,5},{5,4},{6,7},{7,6},{8,9},{9,8},{10,11... | collective-permute-start | bytes 1572872 | tf_op jit(solution)/shard_map/ppermute | solution.py:170
  96.2 24.7 %collective-permute-start.7 = (bf16[512,512]{1,0:T(8,128)(2,1)}, bf16[512,512]{1,0:T(8,128)(2,1)}, u32[]{:S(2)}, u32[]{:S(2)}) collective-permute-start(bf16[512,512]{1,0:T(8,128)(2,1)} %get-tuple-element.56), channel_id=1, source_target_pairs={{0,3},{1,2},{2,1},{3,0},{4,7},{5,6},{6,5},{7,4},{8,11},{9,10},{10,... | collective-permute-start | bytes 1572872 | tf_op jit(solution)/shard_map/ppermute | solution.py:170
  99.5 13.4 %collective-permute-start.19 = (bf16[256,512]{1,0:T(8,128)(2,1)}, bf16[256,512]{1,0:T(8,128)(2,1)}, u32[]{:S(2)}, u32[]{:S(2)}) collective-permute-start(bf16[256,512]{1,0:T(8,128)(2,1)} %slice.49), channel_id=1, source_target_pairs={{0,3},{1,2},{2,1},{3,0},{4,7},{5,6},{6,5},{7,4},{8,11},{9,10},{10,... | collective-permute-start | bytes 786440 | tf_op jit(solution)/shard_map/ppermute | solution.py:170
  100.4 42.8 %collective-permute-start.9 = (bf16[512,512]{1,0:T(8,128)(2,1)}, bf16[512,512]{1,0:T(8,128)(2,1)}, u32[]{:S(2)}, u32[]{:S(2)}) collective-permute-start(bf16[512,512]{1,0:T(8,128)(2,1)} %bitcast.26.own), channel_id=1, source_target_pairs={{0,3},{1,2},{2,1},{3,0},{4,7},{5,6},{6,5},{7,4},{8,11},{9,10},{10,... | collective-permute-start | bytes 1572872 | tf_op jit(solution)/shard_map/ppermute | solution.py:170
  102.2 42.5 %collective-permute-start.8 = (bf16[512,512]{1,0:T(8,128)(2,1)}, bf16[512,512]{1,0:T(8,128)(2,1)}, u32[]{:S(2)}, u32[]{:S(2)}) collective-permute-start(bf16[512,512]{1,0:T(8,128)(2,1)} %bitcast.26.own), channel_id=1, source_target_pairs={{0,1},{1,0},{2,3},{3,2},{4,5},{5,4},{6,7},{7,6},{8,9},{9,8},{10,11... | collective-permute-start | bytes 1572872 | tf_op jit(solution)/shard_map/ppermute | solution.py:170
  119.0 27.6 %collective-permute-start.20 = (bf16[256,512]{1,0:T(8,128)(2,1)}, bf16[256,512]{1,0:T(8,128)(2,1)S(1)}, u32[]{:S(2)}, u32[]{:S(2)}) collective-permute-start(bf16[256,512]{1,0:T(8,128)(2,1)} %get-tuple-element.73), channel_id=1, source_target_pairs={{0,1},{1,0},{2,3},{3,2},{4,5},{5,4},{6,7},{7,6},{8,9},{9,8},{10,11... | collective-permute-start | bytes 786440 | tf_op jit(solution)/shard_map/ppermute | solution.py:170
  119.0 27.6 %collective-permute-start.21 = (bf16[256,512]{1,0:T(8,128)(2,1)}, bf16[256,512]{1,0:T(8,128)(2,1)}, u32[]{:S(2)}, u32[]{:S(2)}) collective-permute-start(bf16[256,512]{1,0:T(8,128)(2,1)} %get-tuple-element.74), channel_id=1, source_target_pairs={{0,3},{1,2},{2,1},{3,0},{4,7},{5,6},{6,5},{7,4},{8,11},{9,10},{10,... | collective-permute-start | bytes 786440 | tf_op jit(solution)/shard_map/ppermute | solution.py:170
  123.1 49.5 %all-to-all-start.1 = ((bf16[64,8,512]{2,1,0:T(8,128)(2,1)}), bf16[64,8,512]{2,1,0:T(8,128)(2,1)}, u32[]{:S(2)}, u32[]{:S(2)}) async-start(bf16[64,8,512]{2,1,0:T(8,128)(2,1)} %fusion.14), calls=%async_computation.1 | async-start | bytes 1048576 | tf_op jit(solution)/shard_map/all_to_all | solution.py:167
  144.2 11.1 %collective-permute-start.10 = (bf16[256,512]{1,0:T(8,128)(2,1)S(1)}, bf16[256,512]{1,0:T(8,128)(2,1)S(1)}, u32[]{:S(2)}, u32[]{:S(2)}) collective-permute-start(bf16[256,512]{1,0:T(8,128)(2,1)S(1)} %slice.46), channel_id=1, source_target_pairs={{0,1},{1,0},{2,3},{3,2},{4,5},{5,4},{6,7},{7,6},{8,9},{9,8},{10,11... | collective-permute-start | bytes 786440 | tf_op jit(solution)/shard_map/ppermute | solution.py:170
  145.7 9.6 %collective-permute-start.11 = (bf16[256,512]{1,0:T(8,128)(2,1)S(1)}, bf16[256,512]{1,0:T(8,128)(2,1)S(1)}, u32[]{:S(2)}, u32[]{:S(2)}) collective-permute-start(bf16[256,512]{1,0:T(8,128)(2,1)S(1)} %slice.47), channel_id=1, source_target_pairs={{0,3},{1,2},{2,1},{3,0},{4,7},{5,6},{6,5},{7,4},{8,11},{9,10},{10,... | collective-permute-start | bytes 786440 | tf_op jit(solution)/shard_map/ppermute | solution.py:170
  149.8 21.8 %collective-permute-start.22 = (bf16[512,512]{1,0:T(8,128)(2,1)S(1)}, bf16[512,512]{1,0:T(8,128)(2,1)S(1)}, u32[]{:S(2)}, u32[]{:S(2)}) collective-permute-start(bf16[512,512]{1,0:T(8,128)(2,1)S(1)} %get-tuple-element.75), channel_id=1, source_target_pairs={{0,1},{1,0},{2,3},{3,2},{4,5},{5,4},{6,7},{7,6},{8,9},{9,8},{10,11... | collective-permute-start | bytes 1572872 | tf_op jit(solution)/shard_map/ppermute | solution.py:170
  150.4 21.3 %collective-permute-start.23 = (bf16[512,512]{1,0:T(8,128)(2,1)S(1)}, bf16[512,512]{1,0:T(8,128)(2,1)S(1)}, u32[]{:S(2)}, u32[]{:S(2)}) collective-permute-start(bf16[512,512]{1,0:T(8,128)(2,1)S(1)} %get-tuple-element.76), channel_id=1, source_target_pairs={{0,3},{1,2},{2,1},{3,0},{4,7},{5,6},{6,5},{7,4},{8,11},{9,10},{10,... | collective-permute-start | bytes 1572872 | tf_op jit(solution)/shard_map/ppermute | solution.py:170
  157.5 10.5 %collective-permute-start.12 = (bf16[256,512]{1,0:T(8,128)(2,1)S(1)}, bf16[256,512]{1,0:T(8,128)(2,1)S(1)}, u32[]{:S(2)}, u32[]{:S(2)}) collective-permute-start(bf16[256,512]{1,0:T(8,128)(2,1)S(1)} %get-tuple-element.63), channel_id=1, source_target_pairs={{0,1},{1,0},{2,3},{3,2},{4,5},{5,4},{6,7},{7,6},{8,9},{9,8},{10,11... | collective-permute-start | bytes 786440 | tf_op jit(solution)/shard_map/ppermute | solution.py:170
  158.0 13.2 %collective-permute-start.13 = (bf16[256,512]{1,0:T(8,128)(2,1)S(1)}, bf16[256,512]{1,0:T(8,128)(2,1)S(1)}, u32[]{:S(2)}, u32[]{:S(2)}) collective-permute-start(bf16[256,512]{1,0:T(8,128)(2,1)S(1)} %get-tuple-element.64), channel_id=1, source_target_pairs={{0,3},{1,2},{2,1},{3,0},{4,7},{5,6},{6,5},{7,4},{8,11},{9,10},{10,... | collective-permute-start | bytes 786440 | tf_op jit(solution)/shard_map/ppermute | solution.py:170
  171.3 13.8 %collective-permute-start.14 = (bf16[512,512]{1,0:T(8,128)(2,1)S(1)}, bf16[512,512]{1,0:T(8,128)(2,1)S(1)}, u32[]{:S(2)}, u32[]{:S(2)}) collective-permute-start(bf16[512,512]{1,0:T(8,128)(2,1)S(1)} %get-tuple-element.65), channel_id=1, source_target_pairs={{0,1},{1,0},{2,3},{3,2},{4,5},{5,4},{6,7},{7,6},{8,9},{9,8},{10,11... | collective-permute-start | bytes 1572872 | tf_op jit(solution)/shard_map/ppermute | solution.py:170
  171.4 13.7 %collective-permute-start.15 = (bf16[512,512]{1,0:T(8,128)(2,1)S(1)}, bf16[512,512]{1,0:T(8,128)(2,1)S(1)}, u32[]{:S(2)}, u32[]{:S(2)}) collective-permute-start(bf16[512,512]{1,0:T(8,128)(2,1)S(1)} %get-tuple-element.66), channel_id=1, source_target_pairs={{0,3},{1,2},{2,1},{3,0},{4,7},{5,6},{6,5},{7,4},{8,11},{9,10},{10,... | collective-permute-start | bytes 1572872 | tf_op jit(solution)/shard_map/ppermute | solution.py:170
  172.6 30.1 %all-to-all-start.5 = ((bf16[64,8,512]{2,1,0:T(8,128)(2,1)}), bf16[64,8,512]{2,1,0:T(8,128)(2,1)S(1)}, u32[]{:S(2)}, u32[]{:S(2)}) async-start(bf16[64,8,512]{2,1,0:T(8,128)(2,1)} %fusion.16), calls=%async_computation.5 | async-start | bytes 1048576 | tf_op jit(solution)/shard_map/all_to_all | solution.py:167
  202.7 23.4 %all-to-all-start.3 = ((bf16[64,8,512]{2,1,0:T(8,128)(2,1)}), bf16[64,8,512]{2,1,0:T(8,128)(2,1)S(1)}, u32[]{:S(2)}, u32[]{:S(2)}) async-start(bf16[64,8,512]{2,1,0:T(8,128)(2,1)} %fusion.15), calls=%async_computation.3 | async-start | bytes 1048576 | tf_op jit(solution)/shard_map/all_to_all | solution.py:167
  (27 other events, 134.2 us)

commit v2 on v1

--- a/solution.py
+++ b/solution.py
@@ -36,18 +36,40 @@
 
 
 def last_body(gate_sum, up_sum, far_a, far_b, gate_w, up_w, down_far, down_near, *outs):
-    across_a, across_b, for_a, for_b, kept = outs
+    sent_a, sent_b, rest_a, rest_b, kept = outs
     half, quarter = far_a.shape
-    for part, (far, across) in enumerate(((far_a, across_a), (far_b, across_b))):
-        at = slice(part * half, (part + 1) * half)
+    low, high = slice(0, half), slice(half, 2 * half)
+    for at, far, places in (
+        (low, far_a, ((sent_a, low), (sent_a, high), (rest_b, low), (kept, low))),
+        (high, far_b, ((sent_b, low), (rest_a, low), (sent_b, high), (kept, high))),
+    ):
         rows = far[...]
         gate = gate_sum[at, :] + dot(rows, gate_w[...])
         up = up_sum[at, :] + dot(rows, up_w[...])
         active = activate(gate, up)
-        across[...] = dot(active, down_far[...]).astype(jnp.bfloat16)
-        for k, out in enumerate((for_a, for_b, kept)):
-            block = down_near[:, k * quarter : (k + 1) * quarter]
-            out[at, :] = dot(active, block).astype(jnp.bfloat16)
+        for k, (out, place) in enumerate(places):
+            block = down_far[...] if k == 0 else down_near[:, (k - 1) * quarter : k * quarter]
+            out[place, :] = dot(active, block).astype(jnp.bfloat16)
+
+
+def total_body(kept, got_a, got_b, late_a, late_b, out):
+    half = late_a.shape[0]
+    f32 = jnp.float32
+    top = kept[:half, :].astype(f32) + got_a[half:, :].astype(f32) + late_b[...].astype(f32)
+    out[:half, :] = top.astype(jnp.bfloat16)
+    bottom = kept[half:, :].astype(f32) + late_a[...].astype(f32) + got_b[half:, :].astype(f32)
+    out[half:, :] = bottom.astype(jnp.bfloat16)
+
+
+def total_call(kept, got_a, got_b, late_a, late_b):
+    return pl.pallas_call(
+        total_body,
+        out_shape=jax.ShapeDtypeStruct(kept.shape, kept.dtype),
+        compiler_params=pltpu.CompilerParams(vmem_limit_bytes=8 << 20),
+        cost_estimate=pl.CostEstimate(flops=1 << 20, bytes_accessed=3 << 20, transcendentals=0),
+        interpret=INTERPRET,
+        name="total",
+    )(kept, got_a, got_b, late_a, late_b)
 
 
 def first_call(own, near_a, near_b, gate_w, up_w):
@@ -72,7 +94,7 @@
     full = jax.ShapeDtypeStruct((rows, quarter), jnp.bfloat16)
     return pl.pallas_call(
         last_body,
-        out_shape=(small, small, full, full, full),
+        out_shape=(full, full, small, small, full),
         compiler_params=pltpu.CompilerParams(vmem_limit_bytes=VMEM_BYTES),
         cost_estimate=pl.CostEstimate(
             flops=12 * rows * quarter * hidden, bytes_accessed=8 << 20, transcendentals=rows * hidden
@@ -80,27 +102,6 @@
         interpret=INTERPRET,
         name="last",
     )(gate_sum, up_sum, far_a, far_b, gate_w, up_w, down_far, down_near)
-
-
-def merge_body(for_a, for_b, via_a, via_b, sum_a, sum_b):
-    half = via_a.shape[0]
-    f32 = jnp.float32
-    sum_a[:half, :] = for_a[:half, :]
-    sum_a[half:, :] = (for_a[half:, :].astype(f32) + via_b[...].astype(f32)).astype(jnp.bfloat16)
-    sum_b[:half, :] = (for_b[:half, :].astype(f32) + via_a[...].astype(f32)).astype(jnp.bfloat16)
-    sum_b[half:, :] = for_b[half:, :]
-
-
-def merge_call(for_a, for_b, via_a, via_b):
-    shape = jax.ShapeDtypeStruct(for_a.shape, for_a.dtype)
-    return pl.pallas_call(
-        merge_body,
-        out_shape=(shape, shape),
-        compiler_params=pltpu.CompilerParams(vmem_limit_bytes=8 << 20),
-        cost_estimate=pl.CostEstimate(flops=1 << 20, bytes_accessed=3 << 20, transcendentals=0),
-        interpret=INTERPRET,
-        name="merge",
-    )(for_a, for_b, via_a, via_b)
 
 
 def layer(tokens, expert_ids, route_weight, norm_gain, expert_gate, expert_up, expert_down):
@@ -153,12 +154,19 @@
     gate_far, up_far = rows_of(gate_w, (opposite,)), rows_of(up_w, (opposite,))
     down_far, down_near = cols_of(down_w, (opposite,)), cols_of(down_w, (mate_a, mate_b, me))
 
-    chosen_of, sends = [], []
+    tables, sends = [], []
     for first in range(0, capacity, SLOTS):
         slots = first + jnp.arange(SLOTS, dtype=jnp.int32)
-        chosen = (rank[:, None, :] == slots[None, :, None]).reshape(groups * SLOTS, tok_count)
-        chosen_of.append(chosen)
-        sends.append(dot(chosen.astype(bf16), normed).astype(bf16).reshape(groups, SLOTS, quarter))
+        chosen = rank[:, None, :] == slots[None, :, None]
+        rows = groups * SLOTS
+        tables.append(
+            [jnp.where(chosen, p[:, None, :], 0.0).reshape(rows, tok_count).astype(bf16) for p in (weight_high, weight_low)]
+        )
+
+    for first, last in ((0, SLOTS), (SLOTS, capacity)):
+        slots = jnp.arange(first, last, dtype=jnp.int32)
+        chosen = (rank[:, None, :] == slots[None, :, None]).reshape(groups * (last - first), tok_count)
+        sends.append(dot(chosen.astype(bf16), normed).astype(bf16))
 
     combined = jnp.zeros((tok_count, quarter), jnp.float32)
     for chunk, first in enumerate(range(0, capacity, SLOTS)):
@@ -169,37 +177,38 @@
         def shift(x, name):
             return lax.ppermute(x, "tp", even if name[1] == "r" else odd)
 
-        chosen, send = chosen_of[chunk], sends[chunk]
-        rows = groups * SLOTS
         half = rows // 2
-        own = exchange(send).reshape(rows, quarter)
         if chunk == 0:
-            own, sends, gate_near, up_near, gate_far, up_far, down_far, down_near = lax.optimization_barrier(
-                (own, sends, gate_near, up_near, gate_far, up_far, down_far, down_near)
+            own = exchange(sends[0].reshape(groups, SLOTS, quarter)).reshape(rows, quarter)
+            own, sends, tables, gate_near, up_near, gate_far, up_far, down_far, down_near = lax.optimization_barrier(
+                (own, sends, tables, gate_near, up_near, gate_far, up_far, down_far, down_near)
             )
+        elif chunk == 1:
+            rest = exchange(sends[1].reshape(groups, capacity - SLOTS, quarter))
+        if chunk:
+            own = rest[:, first - SLOTS : first].reshape(rows, quarter)
         near_a = shift(own, "nr")
         near_b = shift(own, "nl")
         far_a = shift(near_b[:half], "fr")
         far_b = shift(near_a[half:], "fl")
         gate_sum, up_sum = first_call(own, near_a, near_b, gate_near, up_near)
-        across_a, across_b, for_a, for_b, kept = last_call(
+        sent_a, sent_b, rest_a, rest_b, kept = last_call(
             gate_sum, up_sum, far_a, far_b, gate_far, up_far, down_far, down_near
         )
         f32 = jnp.float32
-        via_a = shift(across_a, "ar")
-        via_b = shift(across_b, "al")
-        for_a, for_b = merge_call(for_a, for_b, via_a, via_b)
-        got_a = shift(for_a, "br")
-        got_b = shift(for_b, "bl")
-        total = kept.astype(f32) + got_a.astype(f32) + got_b.astype(f32)
-        result = total.astype(bf16).reshape(groups, SLOTS, quarter)
+        got_a = shift(sent_a, "ar")
+        got_b = shift(sent_b, "al")
+        late_a = shift((rest_a.astype(f32) + got_b[:half].astype(f32)).astype(bf16), "br")
+        late_b = shift((rest_b.astype(f32) + got_a[:half].astype(f32)).astype(bf16), "bl")
+        result = total_call(kept, got_a, got_b, late_a, late_b).reshape(groups, SLOTS, quarter)
         returned = exchange(result).reshape(rows, quarter)
-        for part in (weight_high, weight_low):
-            table = jnp.where(chosen.reshape(groups, SLOTS, tok_count), part[:, None, :], 0.0)
-            table = table.reshape(rows, tok_count).astype(bf16)
-            combined = combined + lax.dot_general(
-                table, returned, (((0,), (0,)), ((), ())), preferred_element_type=jnp.float32
-            )
+        table_high, table_low = tables[chunk]
+        added = lax.dot_general(table_high, returned, (((0,), (0,)), ((), ())), preferred_element_type=jnp.float32)
+        combined = combined + added
+        added = lax.dot_general(table_low, returned, (((0,), (0,)), ((), ())), preferred_element_type=jnp.float32)
+        combined = combined + added
+        if first + SLOTS < capacity:
+            combined = lax.optimization_barrier(combined)
     return combined.astype(bf16)
 
 

time: 230 us -> 232 us (level)
  waiting for transfers between devices: 85.6 us -> 91.5 us
  local copies, waits for them, and re-layouts: 21.5 us -> 18.7 us
    ppermute x24, waiting for transfers between devices: 28.9 us -> 66.3 us  [shift(): return lax.ppermute(x, 'tp', even if name[1] == 'r' else odd)]
    all_to_all x6 -> x5, waiting for transfers between devices: 56.7 us -> 25.2 us  [exchange(): return lax.all_to_all(x, 'ep', split_axis=0, concat_axis=0, tiled=True)]
    all_to_all x6 -> x5, starting transfers between devices: 63.1 us -> 57.5 us  [exchange(): return lax.all_to_all(x, 'ep', split_axis=0, concat_axis=0, tiled=True)]
    reshape x3 -> x0, other arithmetic: 4.27 us -> none  [layer(): result = total.astype(bf16).reshape(groups, SLOTS, quarter)]
    ppermute x24, starting transfers between devices: 21.6 us -> 25.5 us  [shift(): return lax.ppermute(x, 'tp', even if name[1] == 'r' else odd)]
    convert_element_type x0 -> x7, other arithmetic: none -> 3.69 us  [the longest x1 1.4 us: layer(): jnp.where(chosen, p[:, None, :], 0.0).reshape(rows, tok_count).astype(bf16)]
    unnamed x58 -> x54, local copies, waits for them, and re-layouts: 11.7 us -> 8.81 us
    pallas_call x6, Pallas kernels: 10.2 us -> 12.9 us  [the longest x3 8.74 us: last_call(): pl.pallas_call(last_body, out_shape=(full, full, small, small, full), com...]
  transfers between devices with their start and end apart: 30 -> 29, of which waited for: 10 -> 15; matrix products, arithmetic and copies ran while one was open for 8% -> 8% of each run, Pallas kernels for 9% -> 9%
where the time goes in v2:
time: 232 us; the launch traced here: 231 us
  waiting for transfers between devices  91.5 us (39%)
  starting transfers between devices  83 us (36%)
  Pallas kernels  20.8 us (9%)
  local copies, waits for them, and re-layouts  18.7 us (8%)
  matrix products  9.57 us (4%)
  other arithmetic  6.97 us (3%)
    ppermute x24, waiting for transfers between devices, shift(): return lax.ppermute(x, 'tp', even if name[1] == 'r' else odd)  66.3 us
    all_to_all x5, starting transfers between devices, exchange(): return lax.all_to_all(x, 'ep', split_axis=0, concat_axis=0, tiled=True)  57.5 us
    ppermute x24, starting transfers between devices, shift(): return lax.ppermute(x, 'tp', even if name[1] == 'r' else odd)  25.5 us
    all_to_all x5, waiting for transfers between devices, exchange(): return lax.all_to_all(x, 'ep', split_axis=0, concat_axis=0, tiled=True)  25.2 us
    unnamed x54, local copies, waits for them, and re-layouts  8.81 us
    pallas_call x3, Pallas kernels, last_call(): pl.pallas_call(last_body, out_shape=(full, full, small, small, full), com...  8.74 us
    pallas_call x3, Pallas kernels, first_call(): pl.pallas_call(first_body, out_shape=(shape, shape), compiler_params=pltp...  7.87 us
    dot_general x3, matrix products, dot(): return jnp.dot(a, b, preferred_element_type=jnp.float32)  4.82 us
  transfers between devices with their start and end apart: 29, of which 15 were waited for; matrix products, arithmetic and copies ran while one was open for 8% of the time, Pallas kernels for 9%

profile of v2, /device:TPU:1, one launch (start us, length us, event | category | flops | bytes accessed | tf_op | source)
XLA Modules:
  0.0 231.0 jit_solution(11662658426277491722)
XLA Ops:
  3.3 2.1 convolution_convert_fusion.1
  5.5 13.3 %all-to-all-start = ((bf16[64,8,512]{2,1,0:T(8,128)(2,1)}), bf16[64,8,512]{2,1,0:T(8,128)(2,1)}, u32[]{:S(2)}, u32[]{:S(2)}) async-start(bf16[64,8,512]{2,1,0:T(8,128)(2,1)} %bitcast.4), calls=%async_computation | async-start | bytes 1048576 | tf_op jit(solution)/shard_map/all_to_all | solution.py:175
  19.4 2.5 %convolution_convert_fusion = bf16[1024,512]{1,0:T(8,128)(2,1)} fusion(pred[1024,256]{1,0:T(32,128)(4,1)S(1)} %bitcast_compare_fusion, f32[512]{0:T(512)S(1)} %dynamic_slice.67, f32[256]{0:T(256)S(1)} %add_rsqrt_fusion, bf16[256,2048]{1,0:T(8,128)(2,1)} %param.7, s32[]{:T(128)S(6)} %select_n.84), kind=kOutput, calls=%fused_computation.4 | convolution fusion | flops 269484032 | bytes 1575940 | tf_op jit(solution)/shard_map/dot_general | solution.py:24
  28.7 7.7 %all-to-all-done = bf16[64,8,512]{2,1,0:T(8,128)(2,1)} async-done(((bf16[64,8,512]{2,1,0:T(8,128)(2,1)}), bf16[64,8,512]{2,1,0:T(8,128)(2,1)}, u32[]{:S(2)}, u32[]{:S(2)}) %all-to-all-start) | async-done | bytes 524320 | tf_op jit(solution)/shard_map/all_to_all | solution.py:175
  36.4 5.9 %all-to-all-start.2 = ((bf16[64,16,512]{2,1,0:T(8,128)(2,1)}), bf16[64,16,512]{2,1,0:T(8,128)(2,1)}, u32[]{:S(2)}, u32[]{:S(2)}) async-start(bf16[64,16,512]{2,1,0:T(8,128)(2,1)} %bitcast.113), calls=%async_computation.2 | async-start | bytes 2097152 | tf_op jit(solution)/shard_map/all_to_all | solution.py:175
  42.3 2.6 %collective-permute-start.1 = (bf16[512,512]{1,0:T(8,128)(2,1)}, bf16[512,512]{1,0:T(8,128)(2,1)S(1)}, u32[]{:S(2)}, u32[]{:S(2)}) collective-permute-start(bf16[512,512]{1,0:T(8,128)(2,1)} %bitcast.5.own), channel_id=1, source_target_pairs={{0,3},{1,2},{2,1},{3,0},{4,7},{5,6},{6,5},{7,4},{8,11},{9,10},{10,... | collective-permute-start | bytes 1572872 | tf_op jit(solution)/shard_map/ppermute | solution.py:178
  44.9 12.0 %collective-permute-done.1.near_b = bf16[512,512]{1,0:T(8,128)(2,1)S(1)} collective-permute-done((bf16[512,512]{1,0:T(8,128)(2,1)}, bf16[512,512]{1,0:T(8,128)(2,1)S(1)}, u32[]{:S(2)}, u32[]{:S(2)}) %collective-permute-start.1) | collective-permute-done | bytes 524320 | tf_op jit(solution)/shard_map/ppermute | solution.py:178
  58.6 2.2 collective-permute-start.3
  62.2 2.8 %first.3 = (f32[512,512]{1,0:T(8,128)S(1)}, f32[512,512]{1,0:T(8,128)S(1)}) custom-call(bf16[512,512]{1,0:T(8,128)(2,1)} %bitcast.5.own, bf16[512,512]{1,0:T(8,128)(2,1)S(1)} %collective-permute-done.near_a, bf16[512,512]{1,0:T(8,128)(2,1)S(1)} %collective-permute-done.1.near_b, bf16[1536,512]{1,0:T(8,128)(2,1)S(1)} %pad_maximum_fusion.gate_w, ...), custom_call_target="tpu_custom_call" | custom-call | flops 1610612736 | bytes 8388608 | tf_op jit(solution)/shard_map/first/pallas_call | solution.py:78
  67.1 3.3 %all-to-all-done.2 = bf16[64,16,512]{2,1,0:T(8,128)(2,1)} async-done(((bf16[64,16,512]{2,1,0:T(8,128)(2,1)}), bf16[64,16,512]{2,1,0:T(8,128)(2,1)}, u32[]{:S(2)}, u32[]{:S(2)}) %all-to-all-start.2) | async-done | bytes 1048608 | tf_op jit(solution)/shard_map/all_to_all | solution.py:175
  70.4 2.2 slice_bitcast_fusion
  72.6 2.5 %collective-permute-start.9 = (bf16[512,512]{1,0:T(8,128)(2,1)S(1)}, bf16[512,512]{1,0:T(8,128)(2,1)S(1)}, u32[]{:S(2)}, u32[]{:S(2)}) collective-permute-start(bf16[512,512]{1,0:T(8,128)(2,1)S(1)} %get-tuple-element.88.own), channel_id=1, source_target_pairs={{0,3},{1,2},{2,1},{3,0},{4,7},{5,6},{6,5},{7,4},{8,11},{9,10},{10,... | collective-permute-start | bytes 1572872 | tf_op jit(solution)/shard_map/ppermute | solution.py:178
  77.5 3.1 %last.3 = (bf16[512,512]{1,0:T(8,128)(2,1)S(1)}, bf16[512,512]{1,0:T(8,128)(2,1)S(1)}, bf16[256,512]{1,0:T(8,128)(2,1)S(1)}, bf16[256,512]{1,0:T(8,128)(2,1)S(1)}, bf16[512,512]{1,0:T(8,128)(2,1)S(1)}) custom-call(f32[512,512]{1,0:T(8,128)S(1)} %copy-done.14, f32[512,512]{1,0:T(8,128)S(1)} %copy-done.16, bf16[256,512]{1,0:T(8,128)(2,1)S(1)} %collective-permute-done.2.far_a, ...), custom_call_target="tpu_custom_call" | custom-call | flops 1610612736 | bytes 8388608 | tf_op jit(solution)/shard_map/last/pallas_call | solution.py:95
  82.4 3.7 %collective-permute-done.9.near_b = bf16[512,512]{1,0:T(8,128)(2,1)S(1)} collective-permute-done((bf16[512,512]{1,0:T(8,128)(2,1)S(1)}, bf16[512,512]{1,0:T(8,128)(2,1)S(1)}, u32[]{:S(2)}, u32[]{:S(2)}) %collective-permute-start.9) | collective-permute-done | bytes 524320 | tf_op jit(solution)/shard_map/ppermute | solution.py:178
  88.8 9.5 %collective-permute-done.4.got_a = bf16[512,512]{1,0:T(8,128)(2,1)S(1)} collective-permute-done((bf16[512,512]{1,0:T(8,128)(2,1)S(1)}, bf16[512,512]{1,0:T(8,128)(2,1)S(1)}, u32[]{:S(2)}, u32[]{:S(2)}) %collective-permute-start.4) | collective-permute-done | bytes 524320 | tf_op jit(solution)/shard_map/ppermute | solution.py:178
  98.7 2.5 %collective-permute-start.17 = (bf16[512,512]{1,0:T(8,128)(2,1)}, bf16[512,512]{1,0:T(8,128)(2,1)}, u32[]{:S(2)}, u32[]{:S(2)}) collective-permute-start(bf16[512,512]{1,0:T(8,128)(2,1)} %get-tuple-element.87.own), channel_id=1, source_target_pairs={{0,3},{1,2},{2,1},{3,0},{4,7},{5,6},{6,5},{7,4},{8,11},{9,10},{10,... | collective-permute-start | bytes 1572872 | tf_op jit(solution)/shard_map/ppermute | solution.py:178
  101.2 1.8 first.4
  104.0 2.8 %last.4 = (bf16[512,512]{1,0:T(8,128)(2,1)}, bf16[512,512]{1,0:T(8,128)(2,1)}, bf16[256,512]{1,0:T(8,128)(2,1)S(1)}, bf16[256,512]{1,0:T(8,128)(2,1)S(1)}, bf16[512,512]{1,0:T(8,128)(2,1)S(1)}) custom-call(f32[512,512]{1,0:T(8,128)S(1)} %get-tuple-element.58.gate_sum, f32[512,512]{1,0:T(8,128)S(1)} %get-tuple-element.59.up_sum, ...), custom_call_target="tpu_custom_call" | custom-call | flops 1610612736 | bytes 8388608 | tf_op jit(solution)/shard_map/last/pallas_call | solution.py:95
  108.5 2.6 %collective-permute-start.13 = (bf16[512,512]{1,0:T(8,128)(2,1)}, bf16[512,512]{1,0:T(8,128)(2,1)}, u32[]{:S(2)}, u32[]{:S(2)}) collective-permute-start(bf16[512,512]{1,0:T(8,128)(2,1)} %get-tuple-element.62), channel_id=1, source_target_pairs={{0,3},{1,2},{2,1},{3,0},{4,7},{5,6},{6,5},{7,4},{8,11},{9,10},{10,... | collective-permute-start | bytes 1572872 | tf_op jit(solution)/shard_map/ppermute | solution.py:178
  111.1 19.7 %collective-permute-done.6.late_a = bf16[256,512]{1,0:T(8,128)(2,1)S(1)} collective-permute-done((bf16[256,512]{1,0:T(8,128)(2,1)S(1)}, bf16[256,512]{1,0:T(8,128)(2,1)S(1)}, u32[]{:S(2)}, u32[]{:S(2)}) %collective-permute-start.6) | collective-permute-done | bytes 262176 | tf_op jit(solution)/shard_map/ppermute | solution.py:178
  131.7 11.3 %all-to-all-start.1 = ((bf16[64,8,512]{2,1,0:T(8,128)(2,1)}), bf16[64,8,512]{2,1,0:T(8,128)(2,1)}, u32[]{:S(2)}, u32[]{:S(2)}) async-start(bf16[64,8,512]{2,1,0:T(8,128)(2,1)} %bitcast.24), calls=%async_computation.1 | async-start | bytes 1048576 | tf_op jit(solution)/shard_map/all_to_all | solution.py:175
  147.0 3.3 %first.5 = (f32[512,512]{1,0:T(8,128)S(1)}, f32[512,512]{1,0:T(8,128)S(1)}) custom-call(bf16[512,512]{1,0:T(8,128)(2,1)} %get-tuple-element.87.own, bf16[512,512]{1,0:T(8,128)(2,1)} %collective-permute-done.16.near_a, bf16[512,512]{1,0:T(8,128)(2,1)} %collective-permute-done.17.near_b, bf16[1536,512]{1,0:T(8,128)(2,1)S(1)} %pad_maximum_fusion.gate_w, ...), custom_call_target="tpu_custom_call" | custom-call | flops 1610612736 | bytes 8388608 | tf_op jit(solution)/shard_map/first/pallas_call | solution.py:78
  151.4 2.4 %collective-permute-start.15 = (bf16[256,512]{1,0:T(8,128)(2,1)S(1)}, bf16[256,512]{1,0:T(8,128)(2,1)S(1)}, u32[]{:S(2)}, u32[]{:S(2)}) collective-permute-start(bf16[256,512]{1,0:T(8,128)(2,1)S(1)} %add_convert_fusion.2), channel_id=1, source_target_pairs={{0,3},{1,2},{2,1},{3,0},{4,7},{5,6},{6,5},{7,4},{8,11},{9,10},{10,... | collective-permute-start | bytes 786440 | tf_op jit(solution)/shard_map/ppermute | solution.py:178
  155.3 2.8 %last.5 = (bf16[512,512]{1,0:T(8,128)(2,1)}, bf16[512,512]{1,0:T(8,128)(2,1)S(1)}, bf16[256,512]{1,0:T(8,128)(2,1)S(1)}, bf16[256,512]{1,0:T(8,128)(2,1)S(1)}, bf16[512,512]{1,0:T(8,128)(2,1)S(1)}) custom-call(f32[512,512]{1,0:T(8,128)S(1)} %get-tuple-element.67.gate_sum, f32[512,512]{1,0:T(8,128)S(1)} %get-tuple-element.68.up_sum, ...), custom_call_target="tpu_custom_call" | custom-call | flops 1610612736 | bytes 8388608 | tf_op jit(solution)/shard_map/last/pallas_call | solution.py:95
  159.5 2.0 collective-permute-done.14.late_a
  161.6 2.2 total.4
  163.7 13.8 %all-to-all-start.3 = ((bf16[64,8,512]{2,1,0:T(8,128)(2,1)}), bf16[64,8,512]{2,1,0:T(8,128)(2,1)S(1)}, u32[]{:S(2)}, u32[]{:S(2)}) async-start(bf16[64,8,512]{2,1,0:T(8,128)(2,1)} %bitcast.28), calls=%async_computation.3 | async-start | bytes 1048576 | tf_op jit(solution)/shard_map/all_to_all | solution.py:175
  178.1 2.4 %collective-permute-start.23 = (bf16[256,512]{1,0:T(8,128)(2,1)S(1)}, bf16[256,512]{1,0:T(8,128)(2,1)S(1)}, u32[]{:S(2)}, u32[]{:S(2)}) collective-permute-start(bf16[256,512]{1,0:T(8,128)(2,1)S(1)} %add_convert_fusion), channel_id=1, source_target_pairs={{0,3},{1,2},{2,1},{3,0},{4,7},{5,6},{6,5},{7,4},{8,11},{9,10},{10,... | collective-permute-start | bytes 786440 | tf_op jit(solution)/shard_map/ppermute | solution.py:178
  180.5 11.4 %collective-permute-done.21.got_b = bf16[512,512]{1,0:T(8,128)(2,1)S(1)} collective-permute-done((bf16[512,512]{1,0:T(8,128)(2,1)S(1)}, bf16[512,512]{1,0:T(8,128)(2,1)S(1)}, u32[]{:S(2)}, u32[]{:S(2)}) %collective-permute-start.21) | collective-permute-done | bytes 524320 | tf_op jit(solution)/shard_map/ppermute | solution.py:178
  192.1 5.4 %collective-permute-done.23.late_b = bf16[256,512]{1,0:T(8,128)(2,1)S(1)} collective-permute-done((bf16[256,512]{1,0:T(8,128)(2,1)S(1)}, bf16[256,512]{1,0:T(8,128)(2,1)S(1)}, u32[]{:S(2)}, u32[]{:S(2)}) %collective-permute-start.23) | collective-permute-done | bytes 262176 | tf_op jit(solution)/shard_map/ppermute | solution.py:178
  198.7 13.2 %all-to-all-start.4 = ((bf16[64,8,512]{2,1,0:T(8,128)(2,1)}), bf16[64,8,512]{2,1,0:T(8,128)(2,1)S(1)}, u32[]{:S(2)}, u32[]{:S(2)}) async-start(bf16[64,8,512]{2,1,0:T(8,128)(2,1)} %bitcast.31), calls=%async_computation.4 | async-start | bytes 1048576 | tf_op jit(solution)/shard_map/all_to_all | solution.py:175
  215.4 14.2 %all-to-all-done.4 = bf16[64,8,512]{2,1,0:T(8,128)(2,1)S(1)} async-done(((bf16[64,8,512]{2,1,0:T(8,128)(2,1)}), bf16[64,8,512]{2,1,0:T(8,128)(2,1)S(1)}, u32[]{:S(2)}, u32[]{:S(2)}) %all-to-all-start.4) | async-done | bytes 524320 | tf_op jit(solution)/shard_map/all_to_all | solution.py:175
  (135 shorter events, 41.4 us)
Async XLA Ops:
  5.5 30.9 %all-to-all-start = ((bf16[64,8,512]{2,1,0:T(8,128)(2,1)}), bf16[64,8,512]{2,1,0:T(8,128)(2,1)}, u32[]{:S(2)}, u32[]{:S(2)}) async-start(bf16[64,8,512]{2,1,0:T(8,128)(2,1)} %bitcast.4), calls=%async_computation | async-start | bytes 1048576 | tf_op jit(solution)/shard_map/all_to_all | solution.py:175
  36.4 34.0 %all-to-all-start.2 = ((bf16[64,16,512]{2,1,0:T(8,128)(2,1)}), bf16[64,16,512]{2,1,0:T(8,128)(2,1)}, u32[]{:S(2)}, u32[]{:S(2)}) async-start(bf16[64,16,512]{2,1,0:T(8,128)(2,1)} %bitcast.113), calls=%async_computation.2 | async-start | bytes 2097152 | tf_op jit(solution)/shard_map/all_to_all | solution.py:175
  42.3 14.6 %collective-permute-start.1 = (bf16[512,512]{1,0:T(8,128)(2,1)}, bf16[512,512]{1,0:T(8,128)(2,1)S(1)}, u32[]{:S(2)}, u32[]{:S(2)}) collective-permute-start(bf16[512,512]{1,0:T(8,128)(2,1)} %bitcast.5.own), channel_id=1, source_target_pairs={{0,3},{1,2},{2,1},{3,0},{4,7},{5,6},{6,5},{7,4},{8,11},{9,10},{10,... | collective-permute-start | bytes 1572872 | tf_op jit(solution)/shard_map/ppermute | solution.py:178
  44.9 13.0 %collective-permute-start = (bf16[512,512]{1,0:T(8,128)(2,1)}, bf16[512,512]{1,0:T(8,128)(2,1)S(1)}, u32[]{:S(2)}, u32[]{:S(2)}) collective-permute-start(bf16[512,512]{1,0:T(8,128)(2,1)} %bitcast.5.own), channel_id=1, source_target_pairs={{0,1},{1,0},{2,3},{3,2},{4,5},{5,4},{6,7},{7,6},{8,9},{9,8},{10,11... | collective-permute-start | bytes 1572872 | tf_op jit(solution)/shard_map/ppermute | solution.py:178
  57.6 17.5 %collective-permute-start.2 = (bf16[256,512]{1,0:T(8,128)(2,1)}, bf16[256,512]{1,0:T(8,128)(2,1)S(1)}, u32[]{:S(2)}, u32[]{:S(2)}) collective-permute-start(bf16[256,512]{1,0:T(8,128)(2,1)} %slice.76), channel_id=1, source_target_pairs={{0,1},{1,0},{2,3},{3,2},{4,5},{5,4},{6,7},{7,6},{8,9},{9,8},{10,11... | collective-permute-start | bytes 786440 | tf_op jit(solution)/shard_map/ppermute | solution.py:178
  58.6 16.5 %collective-permute-start.3 = (bf16[256,512]{1,0:T(8,128)(2,1)}, bf16[256,512]{1,0:T(8,128)(2,1)}, u32[]{:S(2)}, u32[]{:S(2)}) collective-permute-start(bf16[256,512]{1,0:T(8,128)(2,1)} %slice.77), channel_id=1, source_target_pairs={{0,3},{1,2},{2,1},{3,0},{4,7},{5,6},{6,5},{7,4},{8,11},{9,10},{10,... | collective-permute-start | bytes 786440 | tf_op jit(solution)/shard_map/ppermute | solution.py:178
  72.6 13.5 %collective-permute-start.9 = (bf16[512,512]{1,0:T(8,128)(2,1)S(1)}, bf16[512,512]{1,0:T(8,128)(2,1)S(1)}, u32[]{:S(2)}, u32[]{:S(2)}) collective-permute-start(bf16[512,512]{1,0:T(8,128)(2,1)S(1)} %get-tuple-element.88.own), channel_id=1, source_target_pairs={{0,3},{1,2},{2,1},{3,0},{4,7},{5,6},{6,5},{7,4},{8,11},{9,10},{10,... | collective-permute-start | bytes 1572872 | tf_op jit(solution)/shard_map/ppermute | solution.py:178
  75.1 12.1 %collective-permute-start.8 = (bf16[512,512]{1,0:T(8,128)(2,1)S(1)}, bf16[512,512]{1,0:T(8,128)(2,1)S(1)}, u32[]{:S(2)}, u32[]{:S(2)}) collective-permute-start(bf16[512,512]{1,0:T(8,128)(2,1)S(1)} %get-tuple-element.88.own), channel_id=1, source_target_pairs={{0,1},{1,0},{2,3},{3,2},{4,5},{5,4},{6,7},{7,6},{8,9},{9,8},{10,11... | collective-permute-start | bytes 1572872 | tf_op jit(solution)/shard_map/ppermute | solution.py:178
  77.5 23.6 %copy-start.1 = (bf16[1536,512]{1,0:T(8,128)(2,1)S(1)}, bf16[1536,512]{1,0:T(8,128)(2,1)}, u32[]{:S(2)}) copy-start(bf16[1536,512]{1,0:T(8,128)(2,1)} %pad_maximum_fusion.1.up_w) | copy-start | bytes 4718596
  80.7 17.6 %collective-permute-start.4 = (bf16[512,512]{1,0:T(8,128)(2,1)S(1)}, bf16[512,512]{1,0:T(8,128)(2,1)S(1)}, u32[]{:S(2)}, u32[]{:S(2)}) collective-permute-start(bf16[512,512]{1,0:T(8,128)(2,1)S(1)} %get-tuple-element.51), channel_id=1, source_target_pairs={{0,1},{1,0},{2,3},{3,2},{4,5},{5,4},{6,7},{7,6},{8,9},{9,8},{10,11... | collective-permute-start | bytes 1572872 | tf_op jit(solution)/shard_map/ppermute | solution.py:178
  82.2 26.0 %collective-permute-start.5 = (bf16[512,512]{1,0:T(8,128)(2,1)S(1)}, bf16[512,512]{1,0:T(8,128)(2,1)S(1)}, u32[]{:S(2)}, u32[]{:S(2)}) collective-permute-start(bf16[512,512]{1,0:T(8,128)(2,1)S(1)} %get-tuple-element.52), channel_id=1, source_target_pairs={{0,3},{1,2},{2,1},{3,0},{4,7},{5,6},{6,5},{7,4},{8,11},{9,10},{10,... | collective-permute-start | bytes 1572872 | tf_op jit(solution)/shard_map/ppermute | solution.py:178
  86.1 17.8 %collective-permute-start.10 = (bf16[256,512]{1,0:T(8,128)(2,1)S(1)}, bf16[256,512]{1,0:T(8,128)(2,1)S(1)}, u32[]{:S(2)}, u32[]{:S(2)}) collective-permute-start(bf16[256,512]{1,0:T(8,128)(2,1)S(1)} %slice.81), channel_id=1, source_target_pairs={{0,1},{1,0},{2,3},{3,2},{4,5},{5,4},{6,7},{7,6},{8,9},{9,8},{10,11... | collective-permute-start | bytes 786440 | tf_op jit(solution)/shard_map/ppermute | solution.py:178
  87.1 16.9 %collective-permute-start.11 = (bf16[256,512]{1,0:T(8,128)(2,1)S(1)}, bf16[256,512]{1,0:T(8,128)(2,1)S(1)}, u32[]{:S(2)}, u32[]{:S(2)}) collective-permute-start(bf16[256,512]{1,0:T(8,128)(2,1)S(1)} %slice.82), channel_id=1, source_target_pairs={{0,3},{1,2},{2,1},{3,0},{4,7},{5,6},{6,5},{7,4},{8,11},{9,10},{10,... | collective-permute-start | bytes 786440 | tf_op jit(solution)/shard_map/ppermute | solution.py:178
  98.4 10.1 %collective-permute-start.7 = (bf16[256,512]{1,0:T(8,128)(2,1)S(1)}, bf16[256,512]{1,0:T(8,128)(2,1)S(1)}, u32[]{:S(2)}, u32[]{:S(2)}) collective-permute-start(bf16[256,512]{1,0:T(8,128)(2,1)S(1)} %add_convert_fusion.4), channel_id=1, source_target_pairs={{0,3},{1,2},{2,1},{3,0},{4,7},{5,6},{6,5},{7,4},{8,11},{9,10},{10,... | collective-permute-start | bytes 786440 | tf_op jit(solution)/shard_map/ppermute | solution.py:178
  98.7 44.3 %collective-permute-start.17 = (bf16[512,512]{1,0:T(8,128)(2,1)}, bf16[512,512]{1,0:T(8,128)(2,1)}, u32[]{:S(2)}, u32[]{:S(2)}) collective-permute-start(bf16[512,512]{1,0:T(8,128)(2,1)} %get-tuple-element.87.own), channel_id=1, source_target_pairs={{0,3},{1,2},{2,1},{3,0},{4,7},{5,6},{6,5},{7,4},{8,11},{9,10},{10,... | collective-permute-start | bytes 1572872 | tf_op jit(solution)/shard_map/ppermute | solution.py:178
  104.0 40.2 %collective-permute-start.16 = (bf16[512,512]{1,0:T(8,128)(2,1)}, bf16[512,512]{1,0:T(8,128)(2,1)}, u32[]{:S(2)}, u32[]{:S(2)}) collective-permute-start(bf16[512,512]{1,0:T(8,128)(2,1)} %get-tuple-element.87.own), channel_id=1, source_target_pairs={{0,1},{1,0},{2,3},{3,2},{4,5},{5,4},{6,7},{7,6},{8,9},{9,8},{10,11... | collective-permute-start | bytes 1572872 | tf_op jit(solution)/shard_map/ppermute | solution.py:178
  106.9 24.9 %copy-start.7 = (bf16[512,512]{1,0:T(8,128)(2,1)}, bf16[512,512]{1,0:T(8,128)(2,1)S(1)}, u32[]{:S(2)}) copy-start(bf16[512,512]{1,0:T(8,128)(2,1)S(1)} %get-tuple-element.60.kept) | copy-start | bytes 1572868
  106.9 24.9 %copy-start.11 = (bf16[256,512]{1,0:T(8,128)(2,1)}, bf16[256,512]{1,0:T(8,128)(2,1)S(1)}, u32[]{:S(2)}) copy-start(bf16[256,512]{1,0:T(8,128)(2,1)S(1)} %get-tuple-element.64) | copy-start | bytes 786436
  106.9 43.4 %collective-permute-start.12 = (bf16[512,512]{1,0:T(8,128)(2,1)}, bf16[512,512]{1,0:T(8,128)(2,1)}, u32[]{:S(2)}, u32[]{:S(2)}) collective-permute-start(bf16[512,512]{1,0:T(8,128)(2,1)} %get-tuple-element.61), channel_id=1, source_target_pairs={{0,1},{1,0},{2,3},{3,2},{4,5},{5,4},{6,7},{7,6},{8,9},{9,8},{10,11... | collective-permute-start | bytes 1572872 | tf_op jit(solution)/shard_map/ppermute | solution.py:178
  108.3 22.4 %collective-permute-start.6 = (bf16[256,512]{1,0:T(8,128)(2,1)S(1)}, bf16[256,512]{1,0:T(8,128)(2,1)S(1)}, u32[]{:S(2)}, u32[]{:S(2)}) collective-permute-start(bf16[256,512]{1,0:T(8,128)(2,1)S(1)} %add_convert_fusion.5), channel_id=1, source_target_pairs={{0,1},{1,0},{2,3},{3,2},{4,5},{5,4},{6,7},{7,6},{8,9},{9,8},{10,11... | collective-permute-start | bytes 786440 | tf_op jit(solution)/shard_map/ppermute | solution.py:178
  108.5 45.2 %collective-permute-start.13 = (bf16[512,512]{1,0:T(8,128)(2,1)}, bf16[512,512]{1,0:T(8,128)(2,1)}, u32[]{:S(2)}, u32[]{:S(2)}) collective-permute-start(bf16[512,512]{1,0:T(8,128)(2,1)} %get-tuple-element.62), channel_id=1, source_target_pairs={{0,3},{1,2},{2,1},{3,0},{4,7},{5,6},{6,5},{7,4},{8,11},{9,10},{10,... | collective-permute-start | bytes 1572872 | tf_op jit(solution)/shard_map/ppermute | solution.py:178
  131.7 32.0 %all-to-all-start.1 = ((bf16[64,8,512]{2,1,0:T(8,128)(2,1)}), bf16[64,8,512]{2,1,0:T(8,128)(2,1)}, u32[]{:S(2)}, u32[]{:S(2)}) async-start(bf16[64,8,512]{2,1,0:T(8,128)(2,1)} %bitcast.24), calls=%async_computation.1 | async-start | bytes 1048576 | tf_op jit(solution)/shard_map/all_to_all | solution.py:175
  144.0 11.2 %collective-permute-start.18 = (bf16[256,512]{1,0:T(8,128)(2,1)S(1)}, bf16[256,512]{1,0:T(8,128)(2,1)S(1)}, u32[]{:S(2)}, u32[]{:S(2)}) collective-permute-start(bf16[256,512]{1,0:T(8,128)(2,1)S(1)} %slice.86), channel_id=1, source_target_pairs={{0,1},{1,0},{2,3},{3,2},{4,5},{5,4},{6,7},{7,6},{8,9},{9,8},{10,11... | collective-permute-start | bytes 786440 | tf_op jit(solution)/shard_map/ppermute | solution.py:178
  145.1 10.1 %collective-permute-start.19 = (bf16[256,512]{1,0:T(8,128)(2,1)S(1)}, bf16[256,512]{1,0:T(8,128)(2,1)S(1)}, u32[]{:S(2)}, u32[]{:S(2)}) collective-permute-start(bf16[256,512]{1,0:T(8,128)(2,1)S(1)} %slice.87), channel_id=1, source_target_pairs={{0,3},{1,2},{2,1},{3,0},{4,7},{5,6},{6,5},{7,4},{8,11},{9,10},{10,... | collective-permute-start | bytes 786440 | tf_op jit(solution)/shard_map/ppermute | solution.py:178
  151.4 8.2 %collective-permute-start.15 = (bf16[256,512]{1,0:T(8,128)(2,1)S(1)}, bf16[256,512]{1,0:T(8,128)(2,1)S(1)}, u32[]{:S(2)}, u32[]{:S(2)}) collective-permute-start(bf16[256,512]{1,0:T(8,128)(2,1)S(1)} %add_convert_fusion.2), channel_id=1, source_target_pairs={{0,3},{1,2},{2,1},{3,0},{4,7},{5,6},{6,5},{7,4},{8,11},{9,10},{10,... | collective-permute-start | bytes 786440 | tf_op jit(solution)/shard_map/ppermute | solution.py:178
  154.8 6.8 %collective-permute-start.14 = (bf16[256,512]{1,0:T(8,128)(2,1)S(1)}, bf16[256,512]{1,0:T(8,128)(2,1)S(1)}, u32[]{:S(2)}, u32[]{:S(2)}) collective-permute-start(bf16[256,512]{1,0:T(8,128)(2,1)S(1)} %add_convert_fusion.3), channel_id=1, source_target_pairs={{0,1},{1,0},{2,3},{3,2},{4,5},{5,4},{6,7},{7,6},{8,9},{9,8},{10,11... | collective-permute-start | bytes 786440 | tf_op jit(solution)/shard_map/ppermute | solution.py:178
  158.0 20.0 %collective-permute-start.20 = (bf16[512,512]{1,0:T(8,128)(2,1)}, bf16[512,512]{1,0:T(8,128)(2,1)S(1)}, u32[]{:S(2)}, u32[]{:S(2)}) collective-permute-start(bf16[512,512]{1,0:T(8,128)(2,1)} %get-tuple-element.70), channel_id=1, source_target_pairs={{0,1},{1,0},{2,3},{3,2},{4,5},{5,4},{6,7},{7,6},{8,9},{9,8},{10,11... | collective-permute-start | bytes 1572872 | tf_op jit(solution)/shard_map/ppermute | solution.py:178
  163.7 35.0 %all-to-all-start.3 = ((bf16[64,8,512]{2,1,0:T(8,128)(2,1)}), bf16[64,8,512]{2,1,0:T(8,128)(2,1)S(1)}, u32[]{:S(2)}, u32[]{:S(2)}) async-start(bf16[64,8,512]{2,1,0:T(8,128)(2,1)} %bitcast.28), calls=%async_computation.3 | async-start | bytes 1048576 | tf_op jit(solution)/shard_map/all_to_all | solution.py:175
  177.6 14.3 %collective-permute-start.21 = (bf16[512,512]{1,0:T(8,128)(2,1)S(1)}, bf16[512,512]{1,0:T(8,128)(2,1)S(1)}, u32[]{:S(2)}, u32[]{:S(2)}) collective-permute-start(bf16[512,512]{1,0:T(8,128)(2,1)S(1)} %get-tuple-element.71), channel_id=1, source_target_pairs={{0,3},{1,2},{2,1},{3,0},{4,7},{5,6},{6,5},{7,4},{8,11},{9,10},{10,... | collective-permute-start | bytes 1572872 | tf_op jit(solution)/shard_map/ppermute | solution.py:178
  178.1 19.4 %collective-permute-start.23 = (bf16[256,512]{1,0:T(8,128)(2,1)S(1)}, bf16[256,512]{1,0:T(8,128)(2,1)S(1)}, u32[]{:S(2)}, u32[]{:S(2)}) collective-permute-start(bf16[256,512]{1,0:T(8,128)(2,1)S(1)} %add_convert_fusion), channel_id=1, source_target_pairs={{0,3},{1,2},{2,1},{3,0},{4,7},{5,6},{6,5},{7,4},{8,11},{9,10},{10,... | collective-permute-start | bytes 786440 | tf_op jit(solution)/shard_map/ppermute | solution.py:178
  192.0 5.7 %collective-permute-start.22 = (bf16[256,512]{1,0:T(8,128)(2,1)S(1)}, bf16[256,512]{1,0:T(8,128)(2,1)S(1)}, u32[]{:S(2)}, u32[]{:S(2)}) collective-permute-start(bf16[256,512]{1,0:T(8,128)(2,1)S(1)} %add_convert_fusion.1), channel_id=1, source_target_pairs={{0,1},{1,0},{2,3},{3,2},{4,5},{5,4},{6,7},{7,6},{8,9},{9,8},{10,11... | collective-permute-start | bytes 786440 | tf_op jit(solution)/shard_map/ppermute | solution.py:178
  198.7 30.9 %all-to-all-start.4 = ((bf16[64,8,512]{2,1,0:T(8,128)(2,1)}), bf16[64,8,512]{2,1,0:T(8,128)(2,1)S(1)}, u32[]{:S(2)}, u32[]{:S(2)}) async-start(bf16[64,8,512]{2,1,0:T(8,128)(2,1)} %bitcast.31), calls=%async_computation.4 | async-start | bytes 1048576 | tf_op jit(solution)/shard_map/all_to_all | solution.py:175
  (24 other events, 166.3 us)

commit v3 on v2

--- a/solution.py
+++ b/solution.py
@@ -22,6 +22,50 @@
 
 def dot(a, b):
     return jnp.dot(a, b, preferred_element_type=jnp.float32)
+
+
+def prepare_body(me, tokens, gain, ids, normed_out, rank_out, send_out):
+    tok_count, width = tokens.shape
+    quarter = normed_out.shape[1]
+    groups = rank_out.shape[0]
+    rows = send_out.shape[0]
+    f32, bf16 = jnp.float32, jnp.bfloat16
+    values = tokens[...].astype(f32)
+    scale = lax.rsqrt(jnp.sum(values * values, axis=1, keepdims=True) / width + NORM_EPS)
+    at = pl.ds(pl.multiple_of(me[0] * quarter, quarter), quarter)
+    normed = (tokens[:, at].astype(f32) * scale * gain[:, at]).astype(bf16)
+    normed_out[...] = normed
+    experts = lax.broadcasted_iota(jnp.int32, (groups, tok_count), 0)
+    member = experts == ids[0:1, :]
+    for k in range(1, ids.shape[0]):
+        member = member | (experts == ids[k : k + 1, :])
+    shape = (tok_count, tok_count)
+    earlier = lax.broadcasted_iota(jnp.int32, shape, 0) < lax.broadcasted_iota(jnp.int32, shape, 1)
+    rank = dot(member.astype(f32).astype(bf16), earlier.astype(f32).astype(bf16))
+    rank = jnp.where(member, rank, -1.0)
+    rank_out[...] = rank.astype(jnp.int32)
+    spread = lax.broadcasted_iota(jnp.int32, (rows, groups), 0) // SLOTS
+    spread = (spread == lax.broadcasted_iota(jnp.int32, (rows, groups), 1)).astype(f32).astype(bf16)
+    slot = (lax.broadcasted_iota(jnp.int32, (rows, tok_count), 0) % SLOTS).astype(f32)
+    chosen = (dot(spread, rank.astype(bf16)) == slot).astype(f32).astype(bf16)
+    send_out[...] = dot(chosen, normed).astype(bf16)
+
+
+def prepare_call(me, tokens, gain, ids, quarter, groups):
+    tok_count = tokens.shape[0]
+    vmem = pl.BlockSpec(memory_space=pltpu.VMEM)
+    return pl.pallas_call(
+        prepare_body,
+        out_shape=(
+            jax.ShapeDtypeStruct((tok_count, quarter), jnp.bfloat16),
+            jax.ShapeDtypeStruct((groups, tok_count), jnp.int32),
+            jax.ShapeDtypeStruct((groups * SLOTS, quarter), jnp.bfloat16),
+        ),
+        in_specs=[pl.BlockSpec(memory_space=pltpu.SMEM), vmem, vmem, vmem],
+        compiler_params=pltpu.CompilerParams(vmem_limit_bytes=VMEM_BYTES),
+        interpret=INTERPRET,
+        name="prepare",
+    )(me.reshape(1), tokens, gain.reshape(1, -1), ids)
 
 
 def first_body(own, near_a, near_b, gate_w, up_w, gate_out, up_out):
@@ -119,24 +163,11 @@
     even = [(i, i ^ 1) for i in range(tp_count)]
     odd = [(i, tp_count - 1 - i) for i in range(tp_count)]
 
-    values = tokens.astype(jnp.float32)
-    scale = lax.rsqrt(jnp.mean(values * values, axis=-1, keepdims=True) + NORM_EPS)
-    own_values = lax.dynamic_slice_in_dim(tokens, me * quarter, quarter, 1).astype(jnp.float32)
-    own_gain = lax.dynamic_slice_in_dim(norm_gain, me * quarter, quarter, 0)
-    normed = (own_values * scale * own_gain).astype(bf16)
-
+    normed, rank, first_send = prepare_call(me, tokens, norm_gain, expert_ids.T, quarter, groups)
     experts = jnp.arange(groups, dtype=jnp.int32)[:, None]
     ids = expert_ids.T
     weights = route_weight.T
     named = [ids[k][None, :] == experts for k in range(top_count)]
-    member = named[0]
-    for k in range(1, top_count):
-        member = member | named[k]
-    earlier = (
-        jnp.arange(tok_count, dtype=jnp.int32)[:, None] < jnp.arange(tok_count, dtype=jnp.int32)[None, :]
-    ).astype(bf16)
-    rank = dot(member.astype(bf16), earlier).astype(jnp.int32)
-    rank = jnp.where(member, rank, -1)
     weight = sum(jnp.where(named[k], weights[k][None, :], 0.0) for k in range(top_count))
     weight_high = lax.reduce_precision(weight, 8, 7)
     weight_low = weight - weight_high
@@ -154,7 +185,7 @@
     gate_far, up_far = rows_of(gate_w, (opposite,)), rows_of(up_w, (opposite,))
     down_far, down_near = cols_of(down_w, (opposite,)), cols_of(down_w, (mate_a, mate_b, me))
 
-    tables, sends = [], []
+    tables = []
     for first in range(0, capacity, SLOTS):
         slots = first + jnp.arange(SLOTS, dtype=jnp.int32)
         chosen = rank[:, None, :] == slots[None, :, None]
@@ -163,10 +194,9 @@
             [jnp.where(chosen, p[:, None, :], 0.0).reshape(rows, tok_count).astype(bf16) for p in (weight_high, weight_low)]
         )
 
-    for first, last in ((0, SLOTS), (SLOTS, capacity)):
-        slots = jnp.arange(first, last, dtype=jnp.int32)
-        chosen = (rank[:, None, :] == slots[None, :, None]).reshape(groups * (last - first), tok_count)
-        sends.append(dot(chosen.astype(bf16), normed).astype(bf16))
+    slots = jnp.arange(SLOTS, capacity, dtype=jnp.int32)
+    chosen = (rank[:, None, :] == slots[None, :, None]).reshape(groups * (capacity - SLOTS), tok_count)
+    sends = [first_send, dot(chosen.astype(bf16), normed).astype(bf16)]
 
     combined = jnp.zeros((tok_count, quarter), jnp.float32)
     for chunk, first in enumerate(range(0, capacity, SLOTS)):

time: 232 us -> 231 us (level)
  matrix products: 9.57 us -> 6.17 us
    dot_general x3 -> x1, matrix products: 4.82 us -> 1.42 us  [dot(): return jnp.dot(a, b, preferred_element_type=jnp.float32)]
    unnamed x54 -> x62, local copies, waits for them, and re-layouts: 8.81 us -> 11.4 us
where the time goes in v3:
time: 231 us; the launch traced here: 230 us
  waiting for transfers between devices  92.4 us (40%)
  starting transfers between devices  83 us (36%)
  Pallas kernels  22.2 us (10%)
  local copies, waits for them, and re-layouts  19.8 us (9%)
  matrix products  6.17 us (3%)
  other arithmetic  5.42 us (2%)
    ppermute x24, waiting for transfers between devices, shift(): return lax.ppermute(x, 'tp', even if name[1] == 'r' else odd)  66.3 us
    all_to_all x5, starting transfers between devices, exchange(): return lax.all_to_all(x, 'ep', split_axis=0, concat_axis=0, tiled=True)  57.5 us
    all_to_all x5, waiting for transfers between devices, exchange(): return lax.all_to_all(x, 'ep', split_axis=0, concat_axis=0, tiled=True)  26.2 us
    ppermute x24, starting transfers between devices, shift(): return lax.ppermute(x, 'tp', even if name[1] == 'r' else odd)  25.5 us
    unnamed x62, local copies, waits for them, and re-layouts  11.4 us
    pallas_call x3, Pallas kernels, last_call(): pl.pallas_call(last_body, out_shape=(full, full, small, small, full), com...  8.75 us
    pallas_call x3, Pallas kernels, first_call(): pl.pallas_call(first_body, out_shape=(shape, shape), compiler_params=pltp...  7.87 us
  transfers between devices with their start and end apart: 29, of which 15 were waited for; matrix products, arithmetic and copies ran while one was open for 8% of the time, Pallas kernels for 9%

profile of v3, /device:TPU:1, one launch (start us, length us, event | category | flops | bytes accessed | tf_op | source)
XLA Modules:
  0.0 229.6 jit_solution(11576431931675522430)
XLA Ops:
  4.0 13.3 %all-to-all-start = ((bf16[64,8,512]{2,1,0:T(8,128)(2,1)}), bf16[64,8,512]{2,1,0:T(8,128)(2,1)}, u32[]{:S(2)}, u32[]{:S(2)}) async-start(bf16[64,8,512]{2,1,0:T(8,128)(2,1)} %bitcast.3), calls=%async_computation | async-start | bytes 1048576 | tf_op jit(solution)/shard_map/all_to_all | solution.py:205
  26.3 8.7 %all-to-all-done = bf16[64,8,512]{2,1,0:T(8,128)(2,1)} async-done(((bf16[64,8,512]{2,1,0:T(8,128)(2,1)}), bf16[64,8,512]{2,1,0:T(8,128)(2,1)}, u32[]{:S(2)}, u32[]{:S(2)}) %all-to-all-start) | async-done | bytes 524320 | tf_op jit(solution)/shard_map/all_to_all | solution.py:205
  35.0 5.9 %all-to-all-start.2 = ((bf16[64,16,512]{2,1,0:T(8,128)(2,1)}), bf16[64,16,512]{2,1,0:T(8,128)(2,1)}, u32[]{:S(2)}, u32[]{:S(2)}) async-start(bf16[64,16,512]{2,1,0:T(8,128)(2,1)} %bitcast.118), calls=%async_computation.2 | async-start | bytes 2097152 | tf_op jit(solution)/shard_map/all_to_all | solution.py:205
  40.9 2.6 %collective-permute-start.1 = (bf16[512,512]{1,0:T(8,128)(2,1)}, bf16[512,512]{1,0:T(8,128)(2,1)S(1)}, u32[]{:S(2)}, u32[]{:S(2)}) collective-permute-start(bf16[512,512]{1,0:T(8,128)(2,1)} %bitcast.4.own), channel_id=1, source_target_pairs={{0,3},{1,2},{2,1},{3,0},{4,7},{5,6},{6,5},{7,4},{8,11},{9,10},{10,... | collective-permute-start | bytes 1572872 | tf_op jit(solution)/shard_map/ppermute | solution.py:208
  43.4 12.0 %collective-permute-done.1.near_b = bf16[512,512]{1,0:T(8,128)(2,1)S(1)} collective-permute-done((bf16[512,512]{1,0:T(8,128)(2,1)}, bf16[512,512]{1,0:T(8,128)(2,1)S(1)}, u32[]{:S(2)}, u32[]{:S(2)}) %collective-permute-start.1) | collective-permute-done | bytes 524320 | tf_op jit(solution)/shard_map/ppermute | solution.py:208
  57.2 2.2 collective-permute-start.3
  60.8 2.8 %first.3 = (f32[512,512]{1,0:T(8,128)S(1)}, f32[512,512]{1,0:T(8,128)S(1)}) custom-call(bf16[512,512]{1,0:T(8,128)(2,1)} %bitcast.4.own, bf16[512,512]{1,0:T(8,128)(2,1)S(1)} %collective-permute-done.near_a, bf16[512,512]{1,0:T(8,128)(2,1)S(1)} %collective-permute-done.1.near_b, bf16[1536,512]{1,0:T(8,128)(2,1)S(1)} %pad_maximum_fusion.gate_w, ...), custom_call_target="tpu_custom_call" | custom-call | flops 1610612736 | bytes 8388608 | tf_op jit(solution)/shard_map/first/pallas_call | solution.py:122
  65.7 3.3 %all-to-all-done.2 = bf16[64,16,512]{2,1,0:T(8,128)(2,1)} async-done(((bf16[64,16,512]{2,1,0:T(8,128)(2,1)}), bf16[64,16,512]{2,1,0:T(8,128)(2,1)}, u32[]{:S(2)}, u32[]{:S(2)}) %all-to-all-start.2) | async-done | bytes 1048608 | tf_op jit(solution)/shard_map/all_to_all | solution.py:205
  69.0 2.2 slice_bitcast_fusion
  71.2 2.5 %collective-permute-start.9 = (bf16[512,512]{1,0:T(8,128)(2,1)S(1)}, bf16[512,512]{1,0:T(8,128)(2,1)S(1)}, u32[]{:S(2)}, u32[]{:S(2)}) collective-permute-start(bf16[512,512]{1,0:T(8,128)(2,1)S(1)} %get-tuple-element.94.own), channel_id=1, source_target_pairs={{0,3},{1,2},{2,1},{3,0},{4,7},{5,6},{6,5},{7,4},{8,11},{9,10},{10,... | collective-permute-start | bytes 1572872 | tf_op jit(solution)/shard_map/ppermute | solution.py:208
  76.1 3.1 %last.3 = (bf16[512,512]{1,0:T(8,128)(2,1)S(1)}, bf16[512,512]{1,0:T(8,128)(2,1)S(1)}, bf16[256,512]{1,0:T(8,128)(2,1)S(1)}, bf16[256,512]{1,0:T(8,128)(2,1)S(1)}, bf16[512,512]{1,0:T(8,128)(2,1)S(1)}) custom-call(f32[512,512]{1,0:T(8,128)S(1)} %copy-done.18, f32[512,512]{1,0:T(8,128)S(1)} %copy-done.20, bf16[256,512]{1,0:T(8,128)(2,1)S(1)} %collective-permute-done.2.far_a, ...), custom_call_target="tpu_custom_call" | custom-call | flops 1610612736 | bytes 8388608 | tf_op jit(solution)/shard_map/last/pallas_call | solution.py:139
  79.3 1.5 collective-permute-start.4
  81.0 3.7 %collective-permute-done.9.near_b = bf16[512,512]{1,0:T(8,128)(2,1)S(1)} collective-permute-done((bf16[512,512]{1,0:T(8,128)(2,1)S(1)}, bf16[512,512]{1,0:T(8,128)(2,1)S(1)}, u32[]{:S(2)}, u32[]{:S(2)}) %collective-permute-start.9) | collective-permute-done | bytes 524320 | tf_op jit(solution)/shard_map/ppermute | solution.py:208
  85.7 1.7 collective-permute-start.11
  87.4 9.5 %collective-permute-done.4.got_a = bf16[512,512]{1,0:T(8,128)(2,1)S(1)} collective-permute-done((bf16[512,512]{1,0:T(8,128)(2,1)S(1)}, bf16[512,512]{1,0:T(8,128)(2,1)S(1)}, u32[]{:S(2)}, u32[]{:S(2)}) %collective-permute-start.4) | collective-permute-done | bytes 524320 | tf_op jit(solution)/shard_map/ppermute | solution.py:208
  97.3 2.5 %collective-permute-start.17 = (bf16[512,512]{1,0:T(8,128)(2,1)}, bf16[512,512]{1,0:T(8,128)(2,1)}, u32[]{:S(2)}, u32[]{:S(2)}) collective-permute-start(bf16[512,512]{1,0:T(8,128)(2,1)} %get-tuple-element.93.own), channel_id=1, source_target_pairs={{0,3},{1,2},{2,1},{3,0},{4,7},{5,6},{6,5},{7,4},{8,11},{9,10},{10,... | collective-permute-start | bytes 1572872 | tf_op jit(solution)/shard_map/ppermute | solution.py:208
  99.8 1.8 first.4
  102.6 2.8 %last.4 = (bf16[512,512]{1,0:T(8,128)(2,1)}, bf16[512,512]{1,0:T(8,128)(2,1)}, bf16[256,512]{1,0:T(8,128)(2,1)S(1)}, bf16[256,512]{1,0:T(8,128)(2,1)S(1)}, bf16[512,512]{1,0:T(8,128)(2,1)S(1)}) custom-call(f32[512,512]{1,0:T(8,128)S(1)} %get-tuple-element.64.gate_sum, f32[512,512]{1,0:T(8,128)S(1)} %get-tuple-element.65.up_sum, ...), custom_call_target="tpu_custom_call" | custom-call | flops 1610612736 | bytes 8388608 | tf_op jit(solution)/shard_map/last/pallas_call | solution.py:139
  107.1 2.6 %collective-permute-start.13 = (bf16[512,512]{1,0:T(8,128)(2,1)}, bf16[512,512]{1,0:T(8,128)(2,1)}, u32[]{:S(2)}, u32[]{:S(2)}) collective-permute-start(bf16[512,512]{1,0:T(8,128)(2,1)} %get-tuple-element.68), channel_id=1, source_target_pairs={{0,3},{1,2},{2,1},{3,0},{4,7},{5,6},{6,5},{7,4},{8,11},{9,10},{10,... | collective-permute-start | bytes 1572872 | tf_op jit(solution)/shard_map/ppermute | solution.py:208
  109.7 19.7 %collective-permute-done.6.late_a = bf16[256,512]{1,0:T(8,128)(2,1)S(1)} collective-permute-done((bf16[256,512]{1,0:T(8,128)(2,1)S(1)}, bf16[256,512]{1,0:T(8,128)(2,1)S(1)}, u32[]{:S(2)}, u32[]{:S(2)}) %collective-permute-start.6) | collective-permute-done | bytes 262176 | tf_op jit(solution)/shard_map/ppermute | solution.py:208
  130.3 11.3 %all-to-all-start.1 = ((bf16[64,8,512]{2,1,0:T(8,128)(2,1)}), bf16[64,8,512]{2,1,0:T(8,128)(2,1)}, u32[]{:S(2)}, u32[]{:S(2)}) async-start(bf16[64,8,512]{2,1,0:T(8,128)(2,1)} %bitcast.26), calls=%async_computation.1 | async-start | bytes 1048576 | tf_op jit(solution)/shard_map/all_to_all | solution.py:205
  145.6 3.3 %first.5 = (f32[512,512]{1,0:T(8,128)S(1)}, f32[512,512]{1,0:T(8,128)S(1)}) custom-call(bf16[512,512]{1,0:T(8,128)(2,1)} %get-tuple-element.93.own, bf16[512,512]{1,0:T(8,128)(2,1)} %collective-permute-done.16.near_a, bf16[512,512]{1,0:T(8,128)(2,1)} %collective-permute-done.17.near_b, bf16[1536,512]{1,0:T(8,128)(2,1)S(1)} %pad_maximum_fusion.gate_w, ...), custom_call_target="tpu_custom_call" | custom-call | flops 1610612736 | bytes 8388608 | tf_op jit(solution)/shard_map/first/pallas_call | solution.py:122
  150.0 2.4 %collective-permute-start.15 = (bf16[256,512]{1,0:T(8,128)(2,1)S(1)}, bf16[256,512]{1,0:T(8,128)(2,1)S(1)}, u32[]{:S(2)}, u32[]{:S(2)}) collective-permute-start(bf16[256,512]{1,0:T(8,128)(2,1)S(1)} %add_convert_fusion.2), channel_id=1, source_target_pairs={{0,3},{1,2},{2,1},{3,0},{4,7},{5,6},{6,5},{7,4},{8,11},{9,10},{10,... | collective-permute-start | bytes 786440 | tf_op jit(solution)/shard_map/ppermute | solution.py:208
  153.9 2.8 %last.5 = (bf16[512,512]{1,0:T(8,128)(2,1)}, bf16[512,512]{1,0:T(8,128)(2,1)S(1)}, bf16[256,512]{1,0:T(8,128)(2,1)S(1)}, bf16[256,512]{1,0:T(8,128)(2,1)S(1)}, bf16[512,512]{1,0:T(8,128)(2,1)S(1)}) custom-call(f32[512,512]{1,0:T(8,128)S(1)} %get-tuple-element.73.gate_sum, f32[512,512]{1,0:T(8,128)S(1)} %get-tuple-element.74.up_sum, ...), custom_call_target="tpu_custom_call" | custom-call | flops 1610612736 | bytes 8388608 | tf_op jit(solution)/shard_map/last/pallas_call | solution.py:139
  158.1 2.0 collective-permute-done.14.late_a
  160.1 2.2 total.4
  162.3 13.8 %all-to-all-start.3 = ((bf16[64,8,512]{2,1,0:T(8,128)(2,1)}), bf16[64,8,512]{2,1,0:T(8,128)(2,1)S(1)}, u32[]{:S(2)}, u32[]{:S(2)}) async-start(bf16[64,8,512]{2,1,0:T(8,128)(2,1)} %bitcast.30), calls=%async_computation.3 | async-start | bytes 1048576 | tf_op jit(solution)/shard_map/all_to_all | solution.py:205
  176.7 2.4 %collective-permute-start.23 = (bf16[256,512]{1,0:T(8,128)(2,1)S(1)}, bf16[256,512]{1,0:T(8,128)(2,1)S(1)}, u32[]{:S(2)}, u32[]{:S(2)}) collective-permute-start(bf16[256,512]{1,0:T(8,128)(2,1)S(1)} %add_convert_fusion), channel_id=1, source_target_pairs={{0,3},{1,2},{2,1},{3,0},{4,7},{5,6},{6,5},{7,4},{8,11},{9,10},{10,... | collective-permute-start | bytes 786440 | tf_op jit(solution)/shard_map/ppermute | solution.py:208
  179.1 11.4 %collective-permute-done.21.got_b = bf16[512,512]{1,0:T(8,128)(2,1)S(1)} collective-permute-done((bf16[512,512]{1,0:T(8,128)(2,1)S(1)}, bf16[512,512]{1,0:T(8,128)(2,1)S(1)}, u32[]{:S(2)}, u32[]{:S(2)}) %collective-permute-start.21) | collective-permute-done | bytes 524320 | tf_op jit(solution)/shard_map/ppermute | solution.py:208
  190.7 5.4 %collective-permute-done.23.late_b = bf16[256,512]{1,0:T(8,128)(2,1)S(1)} collective-permute-done((bf16[256,512]{1,0:T(8,128)(2,1)S(1)}, bf16[256,512]{1,0:T(8,128)(2,1)S(1)}, u32[]{:S(2)}, u32[]{:S(2)}) %collective-permute-start.23) | collective-permute-done | bytes 262176 | tf_op jit(solution)/shard_map/ppermute | solution.py:208
  197.3 13.2 %all-to-all-start.4 = ((bf16[64,8,512]{2,1,0:T(8,128)(2,1)}), bf16[64,8,512]{2,1,0:T(8,128)(2,1)S(1)}, u32[]{:S(2)}, u32[]{:S(2)}) async-start(bf16[64,8,512]{2,1,0:T(8,128)(2,1)} %bitcast.33), calls=%async_computation.4 | async-start | bytes 1048576 | tf_op jit(solution)/shard_map/all_to_all | solution.py:205
  214.0 14.2 %all-to-all-done.4 = bf16[64,8,512]{2,1,0:T(8,128)(2,1)S(1)} async-done(((bf16[64,8,512]{2,1,0:T(8,128)(2,1)}), bf16[64,8,512]{2,1,0:T(8,128)(2,1)S(1)}, u32[]{:S(2)}, u32[]{:S(2)}) %all-to-all-start.4) | async-done | bytes 524320 | tf_op jit(solution)/shard_map/all_to_all | solution.py:205
  (139 shorter events, 40.4 us)
Async XLA Ops:
  4.0 30.9 %all-to-all-start = ((bf16[64,8,512]{2,1,0:T(8,128)(2,1)}), bf16[64,8,512]{2,1,0:T(8,128)(2,1)}, u32[]{:S(2)}, u32[]{:S(2)}) async-start(bf16[64,8,512]{2,1,0:T(8,128)(2,1)} %bitcast.3), calls=%async_computation | async-start | bytes 1048576 | tf_op jit(solution)/shard_map/all_to_all | solution.py:205
  35.0 34.0 %all-to-all-start.2 = ((bf16[64,16,512]{2,1,0:T(8,128)(2,1)}), bf16[64,16,512]{2,1,0:T(8,128)(2,1)}, u32[]{:S(2)}, u32[]{:S(2)}) async-start(bf16[64,16,512]{2,1,0:T(8,128)(2,1)} %bitcast.118), calls=%async_computation.2 | async-start | bytes 2097152 | tf_op jit(solution)/shard_map/all_to_all | solution.py:205
  40.9 14.6 %collective-permute-start.1 = (bf16[512,512]{1,0:T(8,128)(2,1)}, bf16[512,512]{1,0:T(8,128)(2,1)S(1)}, u32[]{:S(2)}, u32[]{:S(2)}) collective-permute-start(bf16[512,512]{1,0:T(8,128)(2,1)} %bitcast.4.own), channel_id=1, source_target_pairs={{0,3},{1,2},{2,1},{3,0},{4,7},{5,6},{6,5},{7,4},{8,11},{9,10},{10,... | collective-permute-start | bytes 1572872 | tf_op jit(solution)/shard_map/ppermute | solution.py:208
  43.4 13.0 %collective-permute-start = (bf16[512,512]{1,0:T(8,128)(2,1)}, bf16[512,512]{1,0:T(8,128)(2,1)S(1)}, u32[]{:S(2)}, u32[]{:S(2)}) collective-permute-start(bf16[512,512]{1,0:T(8,128)(2,1)} %bitcast.4.own), channel_id=1, source_target_pairs={{0,1},{1,0},{2,3},{3,2},{4,5},{5,4},{6,7},{7,6},{8,9},{9,8},{10,11... | collective-permute-start | bytes 1572872 | tf_op jit(solution)/shard_map/ppermute | solution.py:208
  56.2 17.5 %collective-permute-start.2 = (bf16[256,512]{1,0:T(8,128)(2,1)}, bf16[256,512]{1,0:T(8,128)(2,1)S(1)}, u32[]{:S(2)}, u32[]{:S(2)}) collective-permute-start(bf16[256,512]{1,0:T(8,128)(2,1)} %slice.76), channel_id=1, source_target_pairs={{0,1},{1,0},{2,3},{3,2},{4,5},{5,4},{6,7},{7,6},{8,9},{9,8},{10,11... | collective-permute-start | bytes 786440 | tf_op jit(solution)/shard_map/ppermute | solution.py:208
  57.2 16.5 %collective-permute-start.3 = (bf16[256,512]{1,0:T(8,128)(2,1)}, bf16[256,512]{1,0:T(8,128)(2,1)}, u32[]{:S(2)}, u32[]{:S(2)}) collective-permute-start(bf16[256,512]{1,0:T(8,128)(2,1)} %slice.77), channel_id=1, source_target_pairs={{0,3},{1,2},{2,1},{3,0},{4,7},{5,6},{6,5},{7,4},{8,11},{9,10},{10,... | collective-permute-start | bytes 786440 | tf_op jit(solution)/shard_map/ppermute | solution.py:208
  71.2 13.5 %collective-permute-start.9 = (bf16[512,512]{1,0:T(8,128)(2,1)S(1)}, bf16[512,512]{1,0:T(8,128)(2,1)S(1)}, u32[]{:S(2)}, u32[]{:S(2)}) collective-permute-start(bf16[512,512]{1,0:T(8,128)(2,1)S(1)} %get-tuple-element.94.own), channel_id=1, source_target_pairs={{0,3},{1,2},{2,1},{3,0},{4,7},{5,6},{6,5},{7,4},{8,11},{9,10},{10,... | collective-permute-start | bytes 1572872 | tf_op jit(solution)/shard_map/ppermute | solution.py:208
  73.6 12.1 %collective-permute-start.8 = (bf16[512,512]{1,0:T(8,128)(2,1)S(1)}, bf16[512,512]{1,0:T(8,128)(2,1)S(1)}, u32[]{:S(2)}, u32[]{:S(2)}) collective-permute-start(bf16[512,512]{1,0:T(8,128)(2,1)S(1)} %get-tuple-element.94.own), channel_id=1, source_target_pairs={{0,1},{1,0},{2,3},{3,2},{4,5},{5,4},{6,7},{7,6},{8,9},{9,8},{10,11... | collective-permute-start | bytes 1572872 | tf_op jit(solution)/shard_map/ppermute | solution.py:208
  76.1 23.6 %copy-start.1 = (bf16[1536,512]{1,0:T(8,128)(2,1)S(1)}, bf16[1536,512]{1,0:T(8,128)(2,1)}, u32[]{:S(2)}) copy-start(bf16[1536,512]{1,0:T(8,128)(2,1)} %pad_maximum_fusion.1.up_w) | copy-start | bytes 4718596
  79.3 17.6 %collective-permute-start.4 = (bf16[512,512]{1,0:T(8,128)(2,1)S(1)}, bf16[512,512]{1,0:T(8,128)(2,1)S(1)}, u32[]{:S(2)}, u32[]{:S(2)}) collective-permute-start(bf16[512,512]{1,0:T(8,128)(2,1)S(1)} %get-tuple-element.57), channel_id=1, source_target_pairs={{0,1},{1,0},{2,3},{3,2},{4,5},{5,4},{6,7},{7,6},{8,9},{9,8},{10,11... | collective-permute-start | bytes 1572872 | tf_op jit(solution)/shard_map/ppermute | solution.py:208
  80.8 26.0 %collective-permute-start.5 = (bf16[512,512]{1,0:T(8,128)(2,1)S(1)}, bf16[512,512]{1,0:T(8,128)(2,1)S(1)}, u32[]{:S(2)}, u32[]{:S(2)}) collective-permute-start(bf16[512,512]{1,0:T(8,128)(2,1)S(1)} %get-tuple-element.58), channel_id=1, source_target_pairs={{0,3},{1,2},{2,1},{3,0},{4,7},{5,6},{6,5},{7,4},{8,11},{9,10},{10,... | collective-permute-start | bytes 1572872 | tf_op jit(solution)/shard_map/ppermute | solution.py:208
  84.7 17.8 %collective-permute-start.10 = (bf16[256,512]{1,0:T(8,128)(2,1)S(1)}, bf16[256,512]{1,0:T(8,128)(2,1)S(1)}, u32[]{:S(2)}, u32[]{:S(2)}) collective-permute-start(bf16[256,512]{1,0:T(8,128)(2,1)S(1)} %slice.81), channel_id=1, source_target_pairs={{0,1},{1,0},{2,3},{3,2},{4,5},{5,4},{6,7},{7,6},{8,9},{9,8},{10,11... | collective-permute-start | bytes 786440 | tf_op jit(solution)/shard_map/ppermute | solution.py:208
  85.7 16.9 %collective-permute-start.11 = (bf16[256,512]{1,0:T(8,128)(2,1)S(1)}, bf16[256,512]{1,0:T(8,128)(2,1)S(1)}, u32[]{:S(2)}, u32[]{:S(2)}) collective-permute-start(bf16[256,512]{1,0:T(8,128)(2,1)S(1)} %slice.82), channel_id=1, source_target_pairs={{0,3},{1,2},{2,1},{3,0},{4,7},{5,6},{6,5},{7,4},{8,11},{9,10},{10,... | collective-permute-start | bytes 786440 | tf_op jit(solution)/shard_map/ppermute | solution.py:208
  97.0 10.1 %collective-permute-start.7 = (bf16[256,512]{1,0:T(8,128)(2,1)S(1)}, bf16[256,512]{1,0:T(8,128)(2,1)S(1)}, u32[]{:S(2)}, u32[]{:S(2)}) collective-permute-start(bf16[256,512]{1,0:T(8,128)(2,1)S(1)} %add_convert_fusion.4), channel_id=1, source_target_pairs={{0,3},{1,2},{2,1},{3,0},{4,7},{5,6},{6,5},{7,4},{8,11},{9,10},{10,... | collective-permute-start | bytes 786440 | tf_op jit(solution)/shard_map/ppermute | solution.py:208
  97.3 44.3 %collective-permute-start.17 = (bf16[512,512]{1,0:T(8,128)(2,1)}, bf16[512,512]{1,0:T(8,128)(2,1)}, u32[]{:S(2)}, u32[]{:S(2)}) collective-permute-start(bf16[512,512]{1,0:T(8,128)(2,1)} %get-tuple-element.93.own), channel_id=1, source_target_pairs={{0,3},{1,2},{2,1},{3,0},{4,7},{5,6},{6,5},{7,4},{8,11},{9,10},{10,... | collective-permute-start | bytes 1572872 | tf_op jit(solution)/shard_map/ppermute | solution.py:208
  102.5 40.2 %collective-permute-start.16 = (bf16[512,512]{1,0:T(8,128)(2,1)}, bf16[512,512]{1,0:T(8,128)(2,1)}, u32[]{:S(2)}, u32[]{:S(2)}) collective-permute-start(bf16[512,512]{1,0:T(8,128)(2,1)} %get-tuple-element.93.own), channel_id=1, source_target_pairs={{0,1},{1,0},{2,3},{3,2},{4,5},{5,4},{6,7},{7,6},{8,9},{9,8},{10,11... | collective-permute-start | bytes 1572872 | tf_op jit(solution)/shard_map/ppermute | solution.py:208
  105.4 24.9 %copy-start.8 = (bf16[512,512]{1,0:T(8,128)(2,1)}, bf16[512,512]{1,0:T(8,128)(2,1)S(1)}, u32[]{:S(2)}) copy-start(bf16[512,512]{1,0:T(8,128)(2,1)S(1)} %get-tuple-element.66.kept) | copy-start | bytes 1572868
  105.4 24.9 %copy-start.12 = (bf16[256,512]{1,0:T(8,128)(2,1)}, bf16[256,512]{1,0:T(8,128)(2,1)S(1)}, u32[]{:S(2)}) copy-start(bf16[256,512]{1,0:T(8,128)(2,1)S(1)} %get-tuple-element.70) | copy-start | bytes 786436
  105.4 43.5 %collective-permute-start.12 = (bf16[512,512]{1,0:T(8,128)(2,1)}, bf16[512,512]{1,0:T(8,128)(2,1)}, u32[]{:S(2)}, u32[]{:S(2)}) collective-permute-start(bf16[512,512]{1,0:T(8,128)(2,1)} %get-tuple-element.67), channel_id=1, source_target_pairs={{0,1},{1,0},{2,3},{3,2},{4,5},{5,4},{6,7},{7,6},{8,9},{9,8},{10,11... | collective-permute-start | bytes 1572872 | tf_op jit(solution)/shard_map/ppermute | solution.py:208
  106.9 22.4 %collective-permute-start.6 = (bf16[256,512]{1,0:T(8,128)(2,1)S(1)}, bf16[256,512]{1,0:T(8,128)(2,1)S(1)}, u32[]{:S(2)}, u32[]{:S(2)}) collective-permute-start(bf16[256,512]{1,0:T(8,128)(2,1)S(1)} %add_convert_fusion.5), channel_id=1, source_target_pairs={{0,1},{1,0},{2,3},{3,2},{4,5},{5,4},{6,7},{7,6},{8,9},{9,8},{10,11... | collective-permute-start | bytes 786440 | tf_op jit(solution)/shard_map/ppermute | solution.py:208
  107.1 45.2 %collective-permute-start.13 = (bf16[512,512]{1,0:T(8,128)(2,1)}, bf16[512,512]{1,0:T(8,128)(2,1)}, u32[]{:S(2)}, u32[]{:S(2)}) collective-permute-start(bf16[512,512]{1,0:T(8,128)(2,1)} %get-tuple-element.68), channel_id=1, source_target_pairs={{0,3},{1,2},{2,1},{3,0},{4,7},{5,6},{6,5},{7,4},{8,11},{9,10},{10,... | collective-permute-start | bytes 1572872 | tf_op jit(solution)/shard_map/ppermute | solution.py:208
  130.3 32.0 %all-to-all-start.1 = ((bf16[64,8,512]{2,1,0:T(8,128)(2,1)}), bf16[64,8,512]{2,1,0:T(8,128)(2,1)}, u32[]{:S(2)}, u32[]{:S(2)}) async-start(bf16[64,8,512]{2,1,0:T(8,128)(2,1)} %bitcast.26), calls=%async_computation.1 | async-start | bytes 1048576 | tf_op jit(solution)/shard_map/all_to_all | solution.py:205
  142.6 11.2 %collective-permute-start.18 = (bf16[256,512]{1,0:T(8,128)(2,1)S(1)}, bf16[256,512]{1,0:T(8,128)(2,1)S(1)}, u32[]{:S(2)}, u32[]{:S(2)}) collective-permute-start(bf16[256,512]{1,0:T(8,128)(2,1)S(1)} %slice.86), channel_id=1, source_target_pairs={{0,1},{1,0},{2,3},{3,2},{4,5},{5,4},{6,7},{7,6},{8,9},{9,8},{10,11... | collective-permute-start | bytes 786440 | tf_op jit(solution)/shard_map/ppermute | solution.py:208
  143.7 10.1 %collective-permute-start.19 = (bf16[256,512]{1,0:T(8,128)(2,1)S(1)}, bf16[256,512]{1,0:T(8,128)(2,1)S(1)}, u32[]{:S(2)}, u32[]{:S(2)}) collective-permute-start(bf16[256,512]{1,0:T(8,128)(2,1)S(1)} %slice.87), channel_id=1, source_target_pairs={{0,3},{1,2},{2,1},{3,0},{4,7},{5,6},{6,5},{7,4},{8,11},{9,10},{10,... | collective-permute-start | bytes 786440 | tf_op jit(solution)/shard_map/ppermute | solution.py:208
  150.0 8.2 %collective-permute-start.15 = (bf16[256,512]{1,0:T(8,128)(2,1)S(1)}, bf16[256,512]{1,0:T(8,128)(2,1)S(1)}, u32[]{:S(2)}, u32[]{:S(2)}) collective-permute-start(bf16[256,512]{1,0:T(8,128)(2,1)S(1)} %add_convert_fusion.2), channel_id=1, source_target_pairs={{0,3},{1,2},{2,1},{3,0},{4,7},{5,6},{6,5},{7,4},{8,11},{9,10},{10,... | collective-permute-start | bytes 786440 | tf_op jit(solution)/shard_map/ppermute | solution.py:208
  153.3 6.8 %collective-permute-start.14 = (bf16[256,512]{1,0:T(8,128)(2,1)S(1)}, bf16[256,512]{1,0:T(8,128)(2,1)S(1)}, u32[]{:S(2)}, u32[]{:S(2)}) collective-permute-start(bf16[256,512]{1,0:T(8,128)(2,1)S(1)} %add_convert_fusion.3), channel_id=1, source_target_pairs={{0,1},{1,0},{2,3},{3,2},{4,5},{5,4},{6,7},{7,6},{8,9},{9,8},{10,11... | collective-permute-start | bytes 786440 | tf_op jit(solution)/shard_map/ppermute | solution.py:208
  156.7 20.0 %collective-permute-start.20 = (bf16[512,512]{1,0:T(8,128)(2,1)}, bf16[512,512]{1,0:T(8,128)(2,1)S(1)}, u32[]{:S(2)}, u32[]{:S(2)}) collective-permute-start(bf16[512,512]{1,0:T(8,128)(2,1)} %get-tuple-element.76), channel_id=1, source_target_pairs={{0,1},{1,0},{2,3},{3,2},{4,5},{5,4},{6,7},{7,6},{8,9},{9,8},{10,11... | collective-permute-start | bytes 1572872 | tf_op jit(solution)/shard_map/ppermute | solution.py:208
  162.3 35.0 %all-to-all-start.3 = ((bf16[64,8,512]{2,1,0:T(8,128)(2,1)}), bf16[64,8,512]{2,1,0:T(8,128)(2,1)S(1)}, u32[]{:S(2)}, u32[]{:S(2)}) async-start(bf16[64,8,512]{2,1,0:T(8,128)(2,1)} %bitcast.30), calls=%async_computation.3 | async-start | bytes 1048576 | tf_op jit(solution)/shard_map/all_to_all | solution.py:205
  176.2 14.3 %collective-permute-start.21 = (bf16[512,512]{1,0:T(8,128)(2,1)S(1)}, bf16[512,512]{1,0:T(8,128)(2,1)S(1)}, u32[]{:S(2)}, u32[]{:S(2)}) collective-permute-start(bf16[512,512]{1,0:T(8,128)(2,1)S(1)} %get-tuple-element.77), channel_id=1, source_target_pairs={{0,3},{1,2},{2,1},{3,0},{4,7},{5,6},{6,5},{7,4},{8,11},{9,10},{10,... | collective-permute-start | bytes 1572872 | tf_op jit(solution)/shard_map/ppermute | solution.py:208
  176.7 19.4 %collective-permute-start.23 = (bf16[256,512]{1,0:T(8,128)(2,1)S(1)}, bf16[256,512]{1,0:T(8,128)(2,1)S(1)}, u32[]{:S(2)}, u32[]{:S(2)}) collective-permute-start(bf16[256,512]{1,0:T(8,128)(2,1)S(1)} %add_convert_fusion), channel_id=1, source_target_pairs={{0,3},{1,2},{2,1},{3,0},{4,7},{5,6},{6,5},{7,4},{8,11},{9,10},{10,... | collective-permute-start | bytes 786440 | tf_op jit(solution)/shard_map/ppermute | solution.py:208
  190.6 5.7 %collective-permute-start.22 = (bf16[256,512]{1,0:T(8,128)(2,1)S(1)}, bf16[256,512]{1,0:T(8,128)(2,1)S(1)}, u32[]{:S(2)}, u32[]{:S(2)}) collective-permute-start(bf16[256,512]{1,0:T(8,128)(2,1)S(1)} %add_convert_fusion.1), channel_id=1, source_target_pairs={{0,1},{1,0},{2,3},{3,2},{4,5},{5,4},{6,7},{7,6},{8,9},{9,8},{10,11... | collective-permute-start | bytes 786440 | tf_op jit(solution)/shard_map/ppermute | solution.py:208
  197.3 30.9 %all-to-all-start.4 = ((bf16[64,8,512]{2,1,0:T(8,128)(2,1)}), bf16[64,8,512]{2,1,0:T(8,128)(2,1)S(1)}, u32[]{:S(2)}, u32[]{:S(2)}) async-start(bf16[64,8,512]{2,1,0:T(8,128)(2,1)} %bitcast.33), calls=%async_computation.4 | async-start | bytes 1048576 | tf_op jit(solution)/shard_map/all_to_all | solution.py:205
  (28 other events, 184.2 us)

commit v4 on v3

--- a/solution.py
+++ b/solution.py
@@ -53,7 +53,8 @@
 
 def prepare_call(me, tokens, gain, ids, quarter, groups):
     tok_count = tokens.shape[0]
-    vmem = pl.BlockSpec(memory_space=pltpu.VMEM)
+    if not INTERPRET:
+        tokens, gain, ids = (pltpu.with_memory_space_constraint(x, pltpu.HBM) for x in (tokens, gain.reshape(1, -1), ids))
     return pl.pallas_call(
         prepare_body,
         out_shape=(
@@ -61,7 +62,7 @@
             jax.ShapeDtypeStruct((groups, tok_count), jnp.int32),
             jax.ShapeDtypeStruct((groups * SLOTS, quarter), jnp.bfloat16),
         ),
-        in_specs=[pl.BlockSpec(memory_space=pltpu.SMEM), vmem, vmem, vmem],
+        in_specs=[pl.BlockSpec(memory_space=pltpu.SMEM), pl.BlockSpec(), pl.BlockSpec(), pl.BlockSpec()],
         compiler_params=pltpu.CompilerParams(vmem_limit_bytes=VMEM_BYTES),
         interpret=INTERPRET,
         name="prepare",
@@ -134,11 +135,13 @@
 def last_call(gate_sum, up_sum, far_a, far_b, gate_w, up_w, down_far, down_near):
     rows, hidden = gate_sum.shape
     half, quarter = far_a.shape
-    small = jax.ShapeDtypeStruct((half, quarter), jnp.bfloat16)
+    shape_of = jax.ShapeDtypeStruct if INTERPRET else pltpu.HBM
+    small = shape_of((half, quarter), jnp.bfloat16)
+    kept = shape_of((rows, quarter), jnp.bfloat16)
     full = jax.ShapeDtypeStruct((rows, quarter), jnp.bfloat16)
     return pl.pallas_call(
         last_body,
-        out_shape=(full, full, small, small, full),
+        out_shape=(full, full, small, small, kept),
         compiler_params=pltpu.CompilerParams(vmem_limit_bytes=VMEM_BYTES),
         cost_estimate=pl.CostEstimate(
             flops=12 * rows * quarter * hidden, bytes_accessed=8 << 20, transcendentals=rows * hidden

time: 231 us -> 229 us (level)
  waiting for transfers between devices: 92.4 us -> 89.8 us
  Pallas kernels: 22.2 us -> 24.8 us
  local copies, waits for them, and re-layouts: 19.8 us -> 17.2 us
    ppermute x24, waiting for transfers between devices: 66.3 us -> 63.6 us  [shift(): return lax.ppermute(x, 'tp', even if name[1] == 'r' else odd)]
    unnamed x62 -> x64, local copies, waits for them, and re-layouts: 11.4 us -> 8.77 us
  transfers between devices with their start and end apart: 29 -> 29, of which waited for: 15 -> 13; matrix products, arithmetic and copies ran while one was open for 8% -> 9% of each run, Pallas kernels for 9% -> 10%
where the time goes in v4:
time: 229 us; the launch traced here: 228 us
  waiting for transfers between devices  89.8 us (39%)
  starting transfers between devices  83.5 us (36%)
  Pallas kernels  24.8 us (11%)
  local copies, waits for them, and re-layouts  17.2 us (8%)
  other arithmetic  6.38 us (3%)
  matrix products  6.16 us (3%)
    ppermute x24, waiting for transfers between devices, shift(): return lax.ppermute(x, 'tp', even if name[1] == 'r' else odd)  63.6 us
    all_to_all x5, starting transfers between devices, exchange(): return lax.all_to_all(x, 'ep', split_axis=0, concat_axis=0, tiled=True)  58.4 us
    all_to_all x5, waiting for transfers between devices, exchange(): return lax.all_to_all(x, 'ep', split_axis=0, concat_axis=0, tiled=True)  26.2 us
    ppermute x24, starting transfers between devices, shift(): return lax.ppermute(x, 'tp', even if name[1] == 'r' else odd)  25.2 us
    pallas_call x3, Pallas kernels, last_call(): pl.pallas_call(last_body, out_shape=(full, full, small, small, kept), com...  9.88 us
    unnamed x64, local copies, waits for them, and re-layouts  8.77 us
    pallas_call x3, Pallas kernels, first_call(): pl.pallas_call(first_body, out_shape=(shape, shape), compiler_params=pltp...  7.88 us
  transfers between devices with their start and end apart: 29, of which 13 were waited for; matrix products, arithmetic and copies ran while one was open for 9% of the time, Pallas kernels for 10%

profile of v4, /device:TPU:1, one launch (start us, length us, event | category | flops | bytes accessed | tf_op | source)
XLA Modules:
  0.0 228.4 jit_solution(2431438151275048910)
XLA Ops:
  0.0 2.7 %prepare.1 = (bf16[256,512]{1,0:T(8,128)(2,1)S(1)}, s32[64,256]{1,0:T(8,128)S(1)}, bf16[512,512]{1,0:T(8,128)(2,1)}) custom-call(s32[1]{0:T(128)} %bitcast.me, bf16[256,2048]{1,0:T(8,128)(2,1)} %tokens.1, f32[1,2048]{1,0:T(1,128)} %bitcast.116, s32[2,256]{1,0:T(2,128)} %bitcast.117), custom_call_target="tpu_custom_call" | custom-call | tf_op jit(solution)/shard_map/prepare/pallas_call | solution.py:58
  2.7 13.3 %all-to-all-start = ((bf16[64,8,512]{2,1,0:T(8,128)(2,1)}), bf16[64,8,512]{2,1,0:T(8,128)(2,1)}, u32[]{:S(2)}, u32[]{:S(2)}) async-start(bf16[64,8,512]{2,1,0:T(8,128)(2,1)} %bitcast.3), calls=%async_computation | async-start | bytes 1048576 | tf_op jit(solution)/shard_map/all_to_all | solution.py:208
  25.0 8.6 %all-to-all-done = bf16[64,8,512]{2,1,0:T(8,128)(2,1)} async-done(((bf16[64,8,512]{2,1,0:T(8,128)(2,1)}), bf16[64,8,512]{2,1,0:T(8,128)(2,1)}, u32[]{:S(2)}, u32[]{:S(2)}) %all-to-all-start) | async-done | bytes 524320 | tf_op jit(solution)/shard_map/all_to_all | solution.py:208
  33.6 5.9 %all-to-all-start.2 = ((bf16[64,16,512]{2,1,0:T(8,128)(2,1)}), bf16[64,16,512]{2,1,0:T(8,128)(2,1)}, u32[]{:S(2)}, u32[]{:S(2)}) async-start(bf16[64,16,512]{2,1,0:T(8,128)(2,1)} %bitcast.115), calls=%async_computation.2 | async-start | bytes 2097152 | tf_op jit(solution)/shard_map/all_to_all | solution.py:208
  39.5 2.6 %collective-permute-start.1 = (bf16[512,512]{1,0:T(8,128)(2,1)}, bf16[512,512]{1,0:T(8,128)(2,1)S(1)}, u32[]{:S(2)}, u32[]{:S(2)}) collective-permute-start(bf16[512,512]{1,0:T(8,128)(2,1)} %bitcast.4.own), channel_id=1, source_target_pairs={{0,3},{1,2},{2,1},{3,0},{4,7},{5,6},{6,5},{7,4},{8,11},{9,10},{10,... | collective-permute-start | bytes 1572872 | tf_op jit(solution)/shard_map/ppermute | solution.py:211
  42.1 12.0 %collective-permute-done.1.near_b = bf16[512,512]{1,0:T(8,128)(2,1)S(1)} collective-permute-done((bf16[512,512]{1,0:T(8,128)(2,1)}, bf16[512,512]{1,0:T(8,128)(2,1)S(1)}, u32[]{:S(2)}, u32[]{:S(2)}) %collective-permute-start.1) | collective-permute-done | bytes 524320 | tf_op jit(solution)/shard_map/ppermute | solution.py:211
  55.8 2.2 collective-permute-start.3
  59.5 2.8 %first.3 = (f32[512,512]{1,0:T(8,128)S(1)}, f32[512,512]{1,0:T(8,128)S(1)}) custom-call(bf16[512,512]{1,0:T(8,128)(2,1)} %bitcast.4.own, bf16[512,512]{1,0:T(8,128)(2,1)S(1)} %collective-permute-done.near_a, bf16[512,512]{1,0:T(8,128)(2,1)S(1)} %collective-permute-done.1.near_b, bf16[1536,512]{1,0:T(8,128)(2,1)S(1)} %pad_maximum_fusion.gate_w, ...), custom_call_target="tpu_custom_call" | custom-call | flops 1610612736 | bytes 8388608 | tf_op jit(solution)/shard_map/first/pallas_call | solution.py:123
  64.3 3.3 %all-to-all-done.2 = bf16[64,16,512]{2,1,0:T(8,128)(2,1)} async-done(((bf16[64,16,512]{2,1,0:T(8,128)(2,1)}), bf16[64,16,512]{2,1,0:T(8,128)(2,1)}, u32[]{:S(2)}, u32[]{:S(2)}) %all-to-all-start.2) | async-done | bytes 1048608 | tf_op jit(solution)/shard_map/all_to_all | solution.py:208
  67.6 2.2 slice_bitcast_fusion
  69.8 2.5 %collective-permute-start.9 = (bf16[512,512]{1,0:T(8,128)(2,1)S(1)}, bf16[512,512]{1,0:T(8,128)(2,1)S(1)}, u32[]{:S(2)}, u32[]{:S(2)}) collective-permute-start(bf16[512,512]{1,0:T(8,128)(2,1)S(1)} %get-tuple-element.94.own), channel_id=1, source_target_pairs={{0,3},{1,2},{2,1},{3,0},{4,7},{5,6},{6,5},{7,4},{8,11},{9,10},{10,... | collective-permute-start | bytes 1572872 | tf_op jit(solution)/shard_map/ppermute | solution.py:211
  74.8 4.0 %last.3 = (bf16[512,512]{1,0:T(8,128)(2,1)S(1)}, bf16[512,512]{1,0:T(8,128)(2,1)S(1)}, bf16[256,512]{1,0:T(8,128)(2,1)}, bf16[256,512]{1,0:T(8,128)(2,1)}, bf16[512,512]{1,0:T(8,128)(2,1)}) custom-call(f32[512,512]{1,0:T(8,128)S(1)} %copy-done.13, f32[512,512]{1,0:T(8,128)S(1)} %copy-done.15, bf16[256,512]{1,0:T(8,128)(2,1)S(1)} %collective-permute-done.2.far_a, ...), custom_call_target="tpu_custom_call" | custom-call | flops 1610612736 | bytes 8388608 | tf_op jit(solution)/shard_map/last/pallas_call | solution.py:142
  80.4 2.9 %collective-permute-done.9.near_b = bf16[512,512]{1,0:T(8,128)(2,1)S(1)} collective-permute-done((bf16[512,512]{1,0:T(8,128)(2,1)S(1)}, bf16[512,512]{1,0:T(8,128)(2,1)S(1)}, u32[]{:S(2)}, u32[]{:S(2)}) %collective-permute-start.9) | collective-permute-done | bytes 524320 | tf_op jit(solution)/shard_map/ppermute | solution.py:211
  84.3 1.7 collective-permute-start.11
  86.1 9.5 %collective-permute-done.4.got_a = bf16[512,512]{1,0:T(8,128)(2,1)S(1)} collective-permute-done((bf16[512,512]{1,0:T(8,128)(2,1)S(1)}, bf16[512,512]{1,0:T(8,128)(2,1)S(1)}, u32[]{:S(2)}, u32[]{:S(2)}) %collective-permute-start.4) | collective-permute-done | bytes 524320 | tf_op jit(solution)/shard_map/ppermute | solution.py:211
  96.9 2.5 %collective-permute-start.17 = (bf16[512,512]{1,0:T(8,128)(2,1)}, bf16[512,512]{1,0:T(8,128)(2,1)}, u32[]{:S(2)}, u32[]{:S(2)}) collective-permute-start(bf16[512,512]{1,0:T(8,128)(2,1)} %get-tuple-element.93.own), channel_id=1, source_target_pairs={{0,3},{1,2},{2,1},{3,0},{4,7},{5,6},{6,5},{7,4},{8,11},{9,10},{10,... | collective-permute-start | bytes 1572872 | tf_op jit(solution)/shard_map/ppermute | solution.py:211
  99.3 1.8 first.4
  101.3 3.0 %last.4 = (bf16[512,512]{1,0:T(8,128)(2,1)}, bf16[512,512]{1,0:T(8,128)(2,1)}, bf16[256,512]{1,0:T(8,128)(2,1)}, bf16[256,512]{1,0:T(8,128)(2,1)}, bf16[512,512]{1,0:T(8,128)(2,1)}) custom-call(f32[512,512]{1,0:T(8,128)S(1)} %get-tuple-element.64.gate_sum, f32[512,512]{1,0:T(8,128)S(1)} %get-tuple-element.65.up_sum, ...), custom_call_target="tpu_custom_call" | custom-call | flops 1610612736 | bytes 8388608 | tf_op jit(solution)/shard_map/last/pallas_call | solution.py:142
  105.9 2.4 %collective-permute-start.13 = (bf16[512,512]{1,0:T(8,128)(2,1)}, bf16[512,512]{1,0:T(8,128)(2,1)}, u32[]{:S(2)}, u32[]{:S(2)}) collective-permute-start(bf16[512,512]{1,0:T(8,128)(2,1)} %get-tuple-element.68), channel_id=1, source_target_pairs={{0,3},{1,2},{2,1},{3,0},{4,7},{5,6},{6,5},{7,4},{8,11},{9,10},{10,... | collective-permute-start | bytes 1572872 | tf_op jit(solution)/shard_map/ppermute | solution.py:211
  108.3 18.9 %collective-permute-done.6.late_a = bf16[256,512]{1,0:T(8,128)(2,1)S(1)} collective-permute-done((bf16[256,512]{1,0:T(8,128)(2,1)S(1)}, bf16[256,512]{1,0:T(8,128)(2,1)S(1)}, u32[]{:S(2)}, u32[]{:S(2)}) %collective-permute-start.6) | collective-permute-done | bytes 262176 | tf_op jit(solution)/shard_map/ppermute | solution.py:211
  128.2 12.2 %all-to-all-start.1 = ((bf16[64,8,512]{2,1,0:T(8,128)(2,1)}), bf16[64,8,512]{2,1,0:T(8,128)(2,1)}, u32[]{:S(2)}, u32[]{:S(2)}) async-start(bf16[64,8,512]{2,1,0:T(8,128)(2,1)} %bitcast.26), calls=%async_computation.1 | async-start | bytes 1048576 | tf_op jit(solution)/shard_map/all_to_all | solution.py:208
  144.3 3.3 %first.5 = (f32[512,512]{1,0:T(8,128)S(1)}, f32[512,512]{1,0:T(8,128)S(1)}) custom-call(bf16[512,512]{1,0:T(8,128)(2,1)} %get-tuple-element.93.own, bf16[512,512]{1,0:T(8,128)(2,1)} %collective-permute-done.16.near_a, bf16[512,512]{1,0:T(8,128)(2,1)} %collective-permute-done.17.near_b, bf16[1536,512]{1,0:T(8,128)(2,1)S(1)} %pad_maximum_fusion.gate_w, ...), custom_call_target="tpu_custom_call" | custom-call | flops 1610612736 | bytes 8388608 | tf_op jit(solution)/shard_map/first/pallas_call | solution.py:123
  148.6 2.4 %collective-permute-start.15 = (bf16[256,512]{1,0:T(8,128)(2,1)S(1)}, bf16[256,512]{1,0:T(8,128)(2,1)S(1)}, u32[]{:S(2)}, u32[]{:S(2)}) collective-permute-start(bf16[256,512]{1,0:T(8,128)(2,1)S(1)} %add_convert_fusion.2), channel_id=1, source_target_pairs={{0,3},{1,2},{2,1},{3,0},{4,7},{5,6},{6,5},{7,4},{8,11},{9,10},{10,... | collective-permute-start | bytes 786440 | tf_op jit(solution)/shard_map/ppermute | solution.py:211
  152.6 2.9 %last.5 = (bf16[512,512]{1,0:T(8,128)(2,1)S(1)}, bf16[512,512]{1,0:T(8,128)(2,1)S(1)}, bf16[256,512]{1,0:T(8,128)(2,1)}, bf16[256,512]{1,0:T(8,128)(2,1)}, bf16[512,512]{1,0:T(8,128)(2,1)}) custom-call(f32[512,512]{1,0:T(8,128)S(1)} %get-tuple-element.73.gate_sum, f32[512,512]{1,0:T(8,128)S(1)} %get-tuple-element.74.up_sum, ...), custom_call_target="tpu_custom_call" | custom-call | flops 1610612736 | bytes 8388608 | tf_op jit(solution)/shard_map/last/pallas_call | solution.py:142
  156.8 2.0 collective-permute-done.14.late_a
  158.9 2.3 total.4
  161.1 13.8 %all-to-all-start.3 = ((bf16[64,8,512]{2,1,0:T(8,128)(2,1)}), bf16[64,8,512]{2,1,0:T(8,128)(2,1)S(1)}, u32[]{:S(2)}, u32[]{:S(2)}) async-start(bf16[64,8,512]{2,1,0:T(8,128)(2,1)} %bitcast.30), calls=%async_computation.3 | async-start | bytes 1048576 | tf_op jit(solution)/shard_map/all_to_all | solution.py:208
  175.5 2.4 %collective-permute-start.23 = (bf16[256,512]{1,0:T(8,128)(2,1)S(1)}, bf16[256,512]{1,0:T(8,128)(2,1)S(1)}, u32[]{:S(2)}, u32[]{:S(2)}) collective-permute-start(bf16[256,512]{1,0:T(8,128)(2,1)S(1)} %add_convert_fusion), channel_id=1, source_target_pairs={{0,3},{1,2},{2,1},{3,0},{4,7},{5,6},{6,5},{7,4},{8,11},{9,10},{10,... | collective-permute-start | bytes 786440 | tf_op jit(solution)/shard_map/ppermute | solution.py:211
  177.9 11.4 %collective-permute-done.21.got_b = bf16[512,512]{1,0:T(8,128)(2,1)S(1)} collective-permute-done((bf16[512,512]{1,0:T(8,128)(2,1)S(1)}, bf16[512,512]{1,0:T(8,128)(2,1)S(1)}, u32[]{:S(2)}, u32[]{:S(2)}) %collective-permute-start.21) | collective-permute-done | bytes 524320 | tf_op jit(solution)/shard_map/ppermute | solution.py:211
  189.4 5.4 %collective-permute-done.23.late_b = bf16[256,512]{1,0:T(8,128)(2,1)S(1)} collective-permute-done((bf16[256,512]{1,0:T(8,128)(2,1)S(1)}, bf16[256,512]{1,0:T(8,128)(2,1)S(1)}, u32[]{:S(2)}, u32[]{:S(2)}) %collective-permute-start.23) | collective-permute-done | bytes 262176 | tf_op jit(solution)/shard_map/ppermute | solution.py:211
  196.1 13.2 %all-to-all-start.4 = ((bf16[64,8,512]{2,1,0:T(8,128)(2,1)}), bf16[64,8,512]{2,1,0:T(8,128)(2,1)S(1)}, u32[]{:S(2)}, u32[]{:S(2)}) async-start(bf16[64,8,512]{2,1,0:T(8,128)(2,1)} %bitcast.33), calls=%async_computation.4 | async-start | bytes 1048576 | tf_op jit(solution)/shard_map/all_to_all | solution.py:208
  212.8 14.2 %all-to-all-done.4 = bf16[64,8,512]{2,1,0:T(8,128)(2,1)S(1)} async-done(((bf16[64,8,512]{2,1,0:T(8,128)(2,1)}), bf16[64,8,512]{2,1,0:T(8,128)(2,1)S(1)}, u32[]{:S(2)}, u32[]{:S(2)}) %all-to-all-start.4) | async-done | bytes 524320 | tf_op jit(solution)/shard_map/all_to_all | solution.py:208
  (141 shorter events, 37.6 us)
Async XLA Ops:
  2.7 30.9 %all-to-all-start = ((bf16[64,8,512]{2,1,0:T(8,128)(2,1)}), bf16[64,8,512]{2,1,0:T(8,128)(2,1)}, u32[]{:S(2)}, u32[]{:S(2)}) async-start(bf16[64,8,512]{2,1,0:T(8,128)(2,1)} %bitcast.3), calls=%async_computation | async-start | bytes 1048576 | tf_op jit(solution)/shard_map/all_to_all | solution.py:208
  33.6 34.0 %all-to-all-start.2 = ((bf16[64,16,512]{2,1,0:T(8,128)(2,1)}), bf16[64,16,512]{2,1,0:T(8,128)(2,1)}, u32[]{:S(2)}, u32[]{:S(2)}) async-start(bf16[64,16,512]{2,1,0:T(8,128)(2,1)} %bitcast.115), calls=%async_computation.2 | async-start | bytes 2097152 | tf_op jit(solution)/shard_map/all_to_all | solution.py:208
  39.5 14.6 %collective-permute-start.1 = (bf16[512,512]{1,0:T(8,128)(2,1)}, bf16[512,512]{1,0:T(8,128)(2,1)S(1)}, u32[]{:S(2)}, u32[]{:S(2)}) collective-permute-start(bf16[512,512]{1,0:T(8,128)(2,1)} %bitcast.4.own), channel_id=1, source_target_pairs={{0,3},{1,2},{2,1},{3,0},{4,7},{5,6},{6,5},{7,4},{8,11},{9,10},{10,... | collective-permute-start | bytes 1572872 | tf_op jit(solution)/shard_map/ppermute | solution.py:211
  42.1 13.0 %collective-permute-start = (bf16[512,512]{1,0:T(8,128)(2,1)}, bf16[512,512]{1,0:T(8,128)(2,1)S(1)}, u32[]{:S(2)}, u32[]{:S(2)}) collective-permute-start(bf16[512,512]{1,0:T(8,128)(2,1)} %bitcast.4.own), channel_id=1, source_target_pairs={{0,1},{1,0},{2,3},{3,2},{4,5},{5,4},{6,7},{7,6},{8,9},{9,8},{10,11... | collective-permute-start | bytes 1572872 | tf_op jit(solution)/shard_map/ppermute | solution.py:211
  54.8 17.5 %collective-permute-start.2 = (bf16[256,512]{1,0:T(8,128)(2,1)}, bf16[256,512]{1,0:T(8,128)(2,1)S(1)}, u32[]{:S(2)}, u32[]{:S(2)}) collective-permute-start(bf16[256,512]{1,0:T(8,128)(2,1)} %slice.76), channel_id=1, source_target_pairs={{0,1},{1,0},{2,3},{3,2},{4,5},{5,4},{6,7},{7,6},{8,9},{9,8},{10,11... | collective-permute-start | bytes 786440 | tf_op jit(solution)/shard_map/ppermute | solution.py:211
  55.8 16.5 %collective-permute-start.3 = (bf16[256,512]{1,0:T(8,128)(2,1)}, bf16[256,512]{1,0:T(8,128)(2,1)}, u32[]{:S(2)}, u32[]{:S(2)}) collective-permute-start(bf16[256,512]{1,0:T(8,128)(2,1)} %slice.77), channel_id=1, source_target_pairs={{0,3},{1,2},{2,1},{3,0},{4,7},{5,6},{6,5},{7,4},{8,11},{9,10},{10,... | collective-permute-start | bytes 786440 | tf_op jit(solution)/shard_map/ppermute | solution.py:211
  69.8 13.5 %collective-permute-start.9 = (bf16[512,512]{1,0:T(8,128)(2,1)S(1)}, bf16[512,512]{1,0:T(8,128)(2,1)S(1)}, u32[]{:S(2)}, u32[]{:S(2)}) collective-permute-start(bf16[512,512]{1,0:T(8,128)(2,1)S(1)} %get-tuple-element.94.own), channel_id=1, source_target_pairs={{0,3},{1,2},{2,1},{3,0},{4,7},{5,6},{6,5},{7,4},{8,11},{9,10},{10,... | collective-permute-start | bytes 1572872 | tf_op jit(solution)/shard_map/ppermute | solution.py:211
  72.3 12.1 %collective-permute-start.8 = (bf16[512,512]{1,0:T(8,128)(2,1)S(1)}, bf16[512,512]{1,0:T(8,128)(2,1)S(1)}, u32[]{:S(2)}, u32[]{:S(2)}) collective-permute-start(bf16[512,512]{1,0:T(8,128)(2,1)S(1)} %get-tuple-element.94.own), channel_id=1, source_target_pairs={{0,1},{1,0},{2,3},{3,2},{4,5},{5,4},{6,7},{7,6},{8,9},{9,8},{10,11... | collective-permute-start | bytes 1572872 | tf_op jit(solution)/shard_map/ppermute | solution.py:211
  78.7 16.8 %collective-permute-start.4 = (bf16[512,512]{1,0:T(8,128)(2,1)S(1)}, bf16[512,512]{1,0:T(8,128)(2,1)S(1)}, u32[]{:S(2)}, u32[]{:S(2)}) collective-permute-start(bf16[512,512]{1,0:T(8,128)(2,1)S(1)} %get-tuple-element.57), channel_id=1, source_target_pairs={{0,1},{1,0},{2,3},{3,2},{4,5},{5,4},{6,7},{7,6},{8,9},{9,8},{10,11... | collective-permute-start | bytes 1572872 | tf_op jit(solution)/shard_map/ppermute | solution.py:211
  80.2 25.5 %collective-permute-start.5 = (bf16[512,512]{1,0:T(8,128)(2,1)S(1)}, bf16[512,512]{1,0:T(8,128)(2,1)S(1)}, u32[]{:S(2)}, u32[]{:S(2)}) collective-permute-start(bf16[512,512]{1,0:T(8,128)(2,1)S(1)} %get-tuple-element.58), channel_id=1, source_target_pairs={{0,3},{1,2},{2,1},{3,0},{4,7},{5,6},{6,5},{7,4},{8,11},{9,10},{10,... | collective-permute-start | bytes 1572872 | tf_op jit(solution)/shard_map/ppermute | solution.py:211
  83.4 17.8 %collective-permute-start.10 = (bf16[256,512]{1,0:T(8,128)(2,1)S(1)}, bf16[256,512]{1,0:T(8,128)(2,1)S(1)}, u32[]{:S(2)}, u32[]{:S(2)}) collective-permute-start(bf16[256,512]{1,0:T(8,128)(2,1)S(1)} %slice.81), channel_id=1, source_target_pairs={{0,1},{1,0},{2,3},{3,2},{4,5},{5,4},{6,7},{7,6},{8,9},{9,8},{10,11... | collective-permute-start | bytes 786440 | tf_op jit(solution)/shard_map/ppermute | solution.py:211
  84.3 16.9 %collective-permute-start.11 = (bf16[256,512]{1,0:T(8,128)(2,1)S(1)}, bf16[256,512]{1,0:T(8,128)(2,1)S(1)}, u32[]{:S(2)}, u32[]{:S(2)}) collective-permute-start(bf16[256,512]{1,0:T(8,128)(2,1)S(1)} %slice.82), channel_id=1, source_target_pairs={{0,3},{1,2},{2,1},{3,0},{4,7},{5,6},{6,5},{7,4},{8,11},{9,10},{10,... | collective-permute-start | bytes 786440 | tf_op jit(solution)/shard_map/ppermute | solution.py:211
  96.6 9.3 %collective-permute-start.7 = (bf16[256,512]{1,0:T(8,128)(2,1)S(1)}, bf16[256,512]{1,0:T(8,128)(2,1)S(1)}, u32[]{:S(2)}, u32[]{:S(2)}) collective-permute-start(bf16[256,512]{1,0:T(8,128)(2,1)S(1)} %add_convert_fusion.4), channel_id=1, source_target_pairs={{0,3},{1,2},{2,1},{3,0},{4,7},{5,6},{6,5},{7,4},{8,11},{9,10},{10,... | collective-permute-start | bytes 786440 | tf_op jit(solution)/shard_map/ppermute | solution.py:211
  96.9 43.5 %collective-permute-start.17 = (bf16[512,512]{1,0:T(8,128)(2,1)}, bf16[512,512]{1,0:T(8,128)(2,1)}, u32[]{:S(2)}, u32[]{:S(2)}) collective-permute-start(bf16[512,512]{1,0:T(8,128)(2,1)} %get-tuple-element.93.own), channel_id=1, source_target_pairs={{0,3},{1,2},{2,1},{3,0},{4,7},{5,6},{6,5},{7,4},{8,11},{9,10},{10,... | collective-permute-start | bytes 1572872 | tf_op jit(solution)/shard_map/ppermute | solution.py:211
  101.2 40.3 %collective-permute-start.16 = (bf16[512,512]{1,0:T(8,128)(2,1)}, bf16[512,512]{1,0:T(8,128)(2,1)}, u32[]{:S(2)}, u32[]{:S(2)}) collective-permute-start(bf16[512,512]{1,0:T(8,128)(2,1)} %get-tuple-element.93.own), channel_id=1, source_target_pairs={{0,1},{1,0},{2,3},{3,2},{4,5},{5,4},{6,7},{7,6},{8,9},{9,8},{10,11... | collective-permute-start | bytes 1572872 | tf_op jit(solution)/shard_map/ppermute | solution.py:211
  101.3 25.9 %copy-start.8 = (bf16[512,512]{1,0:T(8,128)(2,1)S(1)}, bf16[512,512]{1,0:T(8,128)(2,1)}, u32[]{:S(2)}) copy-start(bf16[512,512]{1,0:T(8,128)(2,1)} %get-tuple-element.56.kept) | copy-start | bytes 1572868
  104.3 43.3 %collective-permute-start.12 = (bf16[512,512]{1,0:T(8,128)(2,1)}, bf16[512,512]{1,0:T(8,128)(2,1)}, u32[]{:S(2)}, u32[]{:S(2)}) collective-permute-start(bf16[512,512]{1,0:T(8,128)(2,1)} %get-tuple-element.67), channel_id=1, source_target_pairs={{0,1},{1,0},{2,3},{3,2},{4,5},{5,4},{6,7},{7,6},{8,9},{9,8},{10,11... | collective-permute-start | bytes 1572872 | tf_op jit(solution)/shard_map/ppermute | solution.py:211
  105.8 21.4 %collective-permute-start.6 = (bf16[256,512]{1,0:T(8,128)(2,1)S(1)}, bf16[256,512]{1,0:T(8,128)(2,1)S(1)}, u32[]{:S(2)}, u32[]{:S(2)}) collective-permute-start(bf16[256,512]{1,0:T(8,128)(2,1)S(1)} %add_convert_fusion.5), channel_id=1, source_target_pairs={{0,1},{1,0},{2,3},{3,2},{4,5},{5,4},{6,7},{7,6},{8,9},{9,8},{10,11... | collective-permute-start | bytes 786440 | tf_op jit(solution)/shard_map/ppermute | solution.py:211
  105.9 45.1 %collective-permute-start.13 = (bf16[512,512]{1,0:T(8,128)(2,1)}, bf16[512,512]{1,0:T(8,128)(2,1)}, u32[]{:S(2)}, u32[]{:S(2)}) collective-permute-start(bf16[512,512]{1,0:T(8,128)(2,1)} %get-tuple-element.68), channel_id=1, source_target_pairs={{0,3},{1,2},{2,1},{3,0},{4,7},{5,6},{6,5},{7,4},{8,11},{9,10},{10,... | collective-permute-start | bytes 1572872 | tf_op jit(solution)/shard_map/ppermute | solution.py:211
  128.2 33.0 %all-to-all-start.1 = ((bf16[64,8,512]{2,1,0:T(8,128)(2,1)}), bf16[64,8,512]{2,1,0:T(8,128)(2,1)}, u32[]{:S(2)}, u32[]{:S(2)}) async-start(bf16[64,8,512]{2,1,0:T(8,128)(2,1)} %bitcast.26), calls=%async_computation.1 | async-start | bytes 1048576 | tf_op jit(solution)/shard_map/all_to_all | solution.py:208
  141.3 11.3 %collective-permute-start.18 = (bf16[256,512]{1,0:T(8,128)(2,1)S(1)}, bf16[256,512]{1,0:T(8,128)(2,1)S(1)}, u32[]{:S(2)}, u32[]{:S(2)}) collective-permute-start(bf16[256,512]{1,0:T(8,128)(2,1)S(1)} %slice.86), channel_id=1, source_target_pairs={{0,1},{1,0},{2,3},{3,2},{4,5},{5,4},{6,7},{7,6},{8,9},{9,8},{10,11... | collective-permute-start | bytes 786440 | tf_op jit(solution)/shard_map/ppermute | solution.py:211
  142.4 10.2 %collective-permute-start.19 = (bf16[256,512]{1,0:T(8,128)(2,1)S(1)}, bf16[256,512]{1,0:T(8,128)(2,1)S(1)}, u32[]{:S(2)}, u32[]{:S(2)}) collective-permute-start(bf16[256,512]{1,0:T(8,128)(2,1)S(1)} %slice.87), channel_id=1, source_target_pairs={{0,3},{1,2},{2,1},{3,0},{4,7},{5,6},{6,5},{7,4},{8,11},{9,10},{10,... | collective-permute-start | bytes 786440 | tf_op jit(solution)/shard_map/ppermute | solution.py:211
  148.6 8.2 %collective-permute-start.15 = (bf16[256,512]{1,0:T(8,128)(2,1)S(1)}, bf16[256,512]{1,0:T(8,128)(2,1)S(1)}, u32[]{:S(2)}, u32[]{:S(2)}) collective-permute-start(bf16[256,512]{1,0:T(8,128)(2,1)S(1)} %add_convert_fusion.2), channel_id=1, source_target_pairs={{0,3},{1,2},{2,1},{3,0},{4,7},{5,6},{6,5},{7,4},{8,11},{9,10},{10,... | collective-permute-start | bytes 786440 | tf_op jit(solution)/shard_map/ppermute | solution.py:211
  152.1 6.8 %collective-permute-start.14 = (bf16[256,512]{1,0:T(8,128)(2,1)S(1)}, bf16[256,512]{1,0:T(8,128)(2,1)S(1)}, u32[]{:S(2)}, u32[]{:S(2)}) collective-permute-start(bf16[256,512]{1,0:T(8,128)(2,1)S(1)} %add_convert_fusion.3), channel_id=1, source_target_pairs={{0,1},{1,0},{2,3},{3,2},{4,5},{5,4},{6,7},{7,6},{8,9},{9,8},{10,11... | collective-permute-start | bytes 786440 | tf_op jit(solution)/shard_map/ppermute | solution.py:211
  155.5 19.9 %collective-permute-start.20 = (bf16[512,512]{1,0:T(8,128)(2,1)S(1)}, bf16[512,512]{1,0:T(8,128)(2,1)S(1)}, u32[]{:S(2)}, u32[]{:S(2)}) collective-permute-start(bf16[512,512]{1,0:T(8,128)(2,1)S(1)} %get-tuple-element.76), channel_id=1, source_target_pairs={{0,1},{1,0},{2,3},{3,2},{4,5},{5,4},{6,7},{7,6},{8,9},{9,8},{10,11... | collective-permute-start | bytes 1572872 | tf_op jit(solution)/shard_map/ppermute | solution.py:211
  158.9 30.4 %copy-start.28 = (bf16[256,512]{1,0:T(8,128)(2,1)S(1)}, bf16[256,512]{1,0:T(8,128)(2,1)}, u32[]{:S(2)}) copy-start(bf16[256,512]{1,0:T(8,128)(2,1)} %get-tuple-element.78) | copy-start | bytes 786436
  158.9 36.2 %copy-start.9 = (bf16[512,512]{1,0:T(8,128)(2,1)S(1)}, bf16[512,512]{1,0:T(8,128)(2,1)}, u32[]{:S(2)}) copy-start(bf16[512,512]{1,0:T(8,128)(2,1)} %get-tuple-element.75.kept) | copy-start | bytes 1572868
  161.1 35.0 %all-to-all-start.3 = ((bf16[64,8,512]{2,1,0:T(8,128)(2,1)}), bf16[64,8,512]{2,1,0:T(8,128)(2,1)S(1)}, u32[]{:S(2)}, u32[]{:S(2)}) async-start(bf16[64,8,512]{2,1,0:T(8,128)(2,1)} %bitcast.30), calls=%async_computation.3 | async-start | bytes 1048576 | tf_op jit(solution)/shard_map/all_to_all | solution.py:208
  174.9 14.3 %collective-permute-start.21 = (bf16[512,512]{1,0:T(8,128)(2,1)S(1)}, bf16[512,512]{1,0:T(8,128)(2,1)S(1)}, u32[]{:S(2)}, u32[]{:S(2)}) collective-permute-start(bf16[512,512]{1,0:T(8,128)(2,1)S(1)} %get-tuple-element.77), channel_id=1, source_target_pairs={{0,3},{1,2},{2,1},{3,0},{4,7},{5,6},{6,5},{7,4},{8,11},{9,10},{10,... | collective-permute-start | bytes 1572872 | tf_op jit(solution)/shard_map/ppermute | solution.py:211
  175.5 19.4 %collective-permute-start.23 = (bf16[256,512]{1,0:T(8,128)(2,1)S(1)}, bf16[256,512]{1,0:T(8,128)(2,1)S(1)}, u32[]{:S(2)}, u32[]{:S(2)}) collective-permute-start(bf16[256,512]{1,0:T(8,128)(2,1)S(1)} %add_convert_fusion), channel_id=1, source_target_pairs={{0,3},{1,2},{2,1},{3,0},{4,7},{5,6},{6,5},{7,4},{8,11},{9,10},{10,... | collective-permute-start | bytes 786440 | tf_op jit(solution)/shard_map/ppermute | solution.py:211
  189.3 5.7 %collective-permute-start.22 = (bf16[256,512]{1,0:T(8,128)(2,1)S(1)}, bf16[256,512]{1,0:T(8,128)(2,1)S(1)}, u32[]{:S(2)}, u32[]{:S(2)}) collective-permute-start(bf16[256,512]{1,0:T(8,128)(2,1)S(1)} %add_convert_fusion.1), channel_id=1, source_target_pairs={{0,1},{1,0},{2,3},{3,2},{4,5},{5,4},{6,7},{7,6},{8,9},{9,8},{10,11... | collective-permute-start | bytes 786440 | tf_op jit(solution)/shard_map/ppermute | solution.py:211
  196.1 30.9 %all-to-all-start.4 = ((bf16[64,8,512]{2,1,0:T(8,128)(2,1)}), bf16[64,8,512]{2,1,0:T(8,128)(2,1)S(1)}, u32[]{:S(2)}, u32[]{:S(2)}) async-start(bf16[64,8,512]{2,1,0:T(8,128)(2,1)} %bitcast.33), calls=%async_computation.4 | async-start | bytes 1048576 | tf_op jit(solution)/shard_map/all_to_all | solution.py:208
  (29 other events, 234.7 us)

commit v5 on v4

--- a/solution.py
+++ b/solution.py
@@ -100,15 +100,21 @@
 def total_body(kept, got_a, got_b, late_a, late_b, out):
     half = late_a.shape[0]
     f32 = jnp.float32
-    top = kept[:half, :].astype(f32) + got_a[half:, :].astype(f32) + late_b[...].astype(f32)
+    top = kept[:half, :].astype(f32) + got_a[...].astype(f32) + late_b[...].astype(f32)
     out[:half, :] = top.astype(jnp.bfloat16)
-    bottom = kept[half:, :].astype(f32) + late_a[...].astype(f32) + got_b[half:, :].astype(f32)
+    bottom = kept[half:, :].astype(f32) + late_a[...].astype(f32) + got_b[...].astype(f32)
     out[half:, :] = bottom.astype(jnp.bfloat16)
 
 
 def total_call(kept, got_a, got_b, late_a, late_b):
+    whole = pl.BlockSpec(kept.shape, lambda i: (0, 0))
+    first = pl.BlockSpec(late_a.shape, lambda i: (0, 0))
+    second = pl.BlockSpec(late_a.shape, lambda i: (1, 0))
     return pl.pallas_call(
         total_body,
+        grid=(1,),
+        in_specs=[whole, second, second, first, first],
+        out_specs=whole,
         out_shape=jax.ShapeDtypeStruct(kept.shape, kept.dtype),
         compiler_params=pltpu.CompilerParams(vmem_limit_bytes=8 << 20),
         cost_estimate=pl.CostEstimate(flops=1 << 20, bytes_accessed=3 << 20, transcendentals=0),

time: 229 us -> 229 us (level)
  no operation moved by 1% of the time
where the time goes in v5:
time: 229 us; the launch traced here: 228 us
  waiting for transfers between devices  89.8 us (39%)
  starting transfers between devices  83.5 us (36%)
  Pallas kernels  24.6 us (11%)
  local copies, waits for them, and re-layouts  17.2 us (8%)
  other arithmetic  6.38 us (3%)
  matrix products  6.17 us (3%)
    ppermute x24, waiting for transfers between devices, shift(): return lax.ppermute(x, 'tp', even if name[1] == 'r' else odd)  63.6 us
    all_to_all x5, starting transfers between devices, exchange(): return lax.all_to_all(x, 'ep', split_axis=0, concat_axis=0, tiled=True)  58.4 us
    all_to_all x5, waiting for transfers between devices, exchange(): return lax.all_to_all(x, 'ep', split_axis=0, concat_axis=0, tiled=True)  26.2 us
    ppermute x24, starting transfers between devices, shift(): return lax.ppermute(x, 'tp', even if name[1] == 'r' else odd)  25.2 us
    pallas_call x3, Pallas kernels, last_call(): pl.pallas_call(last_body, out_shape=(full, full, small, small, kept), com...  9.88 us
    unnamed x64, local copies, waits for them, and re-layouts  8.77 us
    pallas_call x3, Pallas kernels, first_call(): pl.pallas_call(first_body, out_shape=(shape, shape), compiler_params=pltp...  7.88 us
  transfers between devices with their start and end apart: 29, of which 13 were waited for; matrix products, arithmetic and copies ran while one was open for 9% of the time, Pallas kernels for 10%

profile of v5, /device:TPU:1, one launch (start us, length us, event | category | flops | bytes accessed | tf_op | source)
XLA Modules:
  0.0 228.2 jit_solution(16913780782178864755)
XLA Ops:
  0.0 2.7 %prepare.1 = (bf16[256,512]{1,0:T(8,128)(2,1)S(1)}, s32[64,256]{1,0:T(8,128)S(1)}, bf16[512,512]{1,0:T(8,128)(2,1)}) custom-call(s32[1]{0:T(128)} %bitcast.me, bf16[256,2048]{1,0:T(8,128)(2,1)} %tokens.1, f32[1,2048]{1,0:T(1,128)} %bitcast.116, s32[2,256]{1,0:T(2,128)} %bitcast.117), custom_call_target="tpu_custom_call" | custom-call | tf_op jit(solution)/shard_map/prepare/pallas_call | solution.py:58
  2.7 13.3 %all-to-all-start = ((bf16[64,8,512]{2,1,0:T(8,128)(2,1)}), bf16[64,8,512]{2,1,0:T(8,128)(2,1)}, u32[]{:S(2)}, u32[]{:S(2)}) async-start(bf16[64,8,512]{2,1,0:T(8,128)(2,1)} %bitcast.3), calls=%async_computation | async-start | bytes 1048576 | tf_op jit(solution)/shard_map/all_to_all | solution.py:214
  25.0 8.6 %all-to-all-done = bf16[64,8,512]{2,1,0:T(8,128)(2,1)} async-done(((bf16[64,8,512]{2,1,0:T(8,128)(2,1)}), bf16[64,8,512]{2,1,0:T(8,128)(2,1)}, u32[]{:S(2)}, u32[]{:S(2)}) %all-to-all-start) | async-done | bytes 524320 | tf_op jit(solution)/shard_map/all_to_all | solution.py:214
  33.6 5.9 %all-to-all-start.2 = ((bf16[64,16,512]{2,1,0:T(8,128)(2,1)}), bf16[64,16,512]{2,1,0:T(8,128)(2,1)}, u32[]{:S(2)}, u32[]{:S(2)}) async-start(bf16[64,16,512]{2,1,0:T(8,128)(2,1)} %bitcast.115), calls=%async_computation.2 | async-start | bytes 2097152 | tf_op jit(solution)/shard_map/all_to_all | solution.py:214
  39.5 2.6 %collective-permute-start.1 = (bf16[512,512]{1,0:T(8,128)(2,1)}, bf16[512,512]{1,0:T(8,128)(2,1)S(1)}, u32[]{:S(2)}, u32[]{:S(2)}) collective-permute-start(bf16[512,512]{1,0:T(8,128)(2,1)} %bitcast.4.own), channel_id=1, source_target_pairs={{0,3},{1,2},{2,1},{3,0},{4,7},{5,6},{6,5},{7,4},{8,11},{9,10},{10,... | collective-permute-start | bytes 1572872 | tf_op jit(solution)/shard_map/ppermute | solution.py:217
  42.1 12.0 %collective-permute-done.1.near_b = bf16[512,512]{1,0:T(8,128)(2,1)S(1)} collective-permute-done((bf16[512,512]{1,0:T(8,128)(2,1)}, bf16[512,512]{1,0:T(8,128)(2,1)S(1)}, u32[]{:S(2)}, u32[]{:S(2)}) %collective-permute-start.1) | collective-permute-done | bytes 524320 | tf_op jit(solution)/shard_map/ppermute | solution.py:217
  55.8 2.2 collective-permute-start.3
  59.5 2.8 %first.3 = (f32[512,512]{1,0:T(8,128)S(1)}, f32[512,512]{1,0:T(8,128)S(1)}) custom-call(bf16[512,512]{1,0:T(8,128)(2,1)} %bitcast.4.own, bf16[512,512]{1,0:T(8,128)(2,1)S(1)} %collective-permute-done.near_a, bf16[512,512]{1,0:T(8,128)(2,1)S(1)} %collective-permute-done.1.near_b, bf16[1536,512]{1,0:T(8,128)(2,1)S(1)} %pad_maximum_fusion.gate_w, ...), custom_call_target="tpu_custom_call" | custom-call | flops 1610612736 | bytes 8388608 | tf_op jit(solution)/shard_map/first/pallas_call | solution.py:129
  64.3 3.3 %all-to-all-done.2 = bf16[64,16,512]{2,1,0:T(8,128)(2,1)} async-done(((bf16[64,16,512]{2,1,0:T(8,128)(2,1)}), bf16[64,16,512]{2,1,0:T(8,128)(2,1)}, u32[]{:S(2)}, u32[]{:S(2)}) %all-to-all-start.2) | async-done | bytes 1048608 | tf_op jit(solution)/shard_map/all_to_all | solution.py:214
  67.6 2.2 slice_bitcast_fusion
  69.8 2.5 %collective-permute-start.9 = (bf16[512,512]{1,0:T(8,128)(2,1)S(1)}, bf16[512,512]{1,0:T(8,128)(2,1)S(1)}, u32[]{:S(2)}, u32[]{:S(2)}) collective-permute-start(bf16[512,512]{1,0:T(8,128)(2,1)S(1)} %get-tuple-element.94.own), channel_id=1, source_target_pairs={{0,3},{1,2},{2,1},{3,0},{4,7},{5,6},{6,5},{7,4},{8,11},{9,10},{10,... | collective-permute-start | bytes 1572872 | tf_op jit(solution)/shard_map/ppermute | solution.py:217
  74.8 4.0 %last.3 = (bf16[512,512]{1,0:T(8,128)(2,1)S(1)}, bf16[512,512]{1,0:T(8,128)(2,1)S(1)}, bf16[256,512]{1,0:T(8,128)(2,1)}, bf16[256,512]{1,0:T(8,128)(2,1)}, bf16[512,512]{1,0:T(8,128)(2,1)}) custom-call(f32[512,512]{1,0:T(8,128)S(1)} %copy-done.13, f32[512,512]{1,0:T(8,128)S(1)} %copy-done.15, bf16[256,512]{1,0:T(8,128)(2,1)S(1)} %collective-permute-done.2.far_a, ...), custom_call_target="tpu_custom_call" | custom-call | flops 1610612736 | bytes 8388608 | tf_op jit(solution)/shard_map/last/pallas_call | solution.py:148
  80.4 2.9 %collective-permute-done.9.near_b = bf16[512,512]{1,0:T(8,128)(2,1)S(1)} collective-permute-done((bf16[512,512]{1,0:T(8,128)(2,1)S(1)}, bf16[512,512]{1,0:T(8,128)(2,1)S(1)}, u32[]{:S(2)}, u32[]{:S(2)}) %collective-permute-start.9) | collective-permute-done | bytes 524320 | tf_op jit(solution)/shard_map/ppermute | solution.py:217
  84.3 1.7 collective-permute-start.11
  86.1 9.5 %collective-permute-done.4.got_a = bf16[512,512]{1,0:T(8,128)(2,1)S(1)} collective-permute-done((bf16[512,512]{1,0:T(8,128)(2,1)S(1)}, bf16[512,512]{1,0:T(8,128)(2,1)S(1)}, u32[]{:S(2)}, u32[]{:S(2)}) %collective-permute-start.4) | collective-permute-done | bytes 524320 | tf_op jit(solution)/shard_map/ppermute | solution.py:217
  96.9 2.5 %collective-permute-start.17 = (bf16[512,512]{1,0:T(8,128)(2,1)}, bf16[512,512]{1,0:T(8,128)(2,1)}, u32[]{:S(2)}, u32[]{:S(2)}) collective-permute-start(bf16[512,512]{1,0:T(8,128)(2,1)} %get-tuple-element.93.own), channel_id=1, source_target_pairs={{0,3},{1,2},{2,1},{3,0},{4,7},{5,6},{6,5},{7,4},{8,11},{9,10},{10,... | collective-permute-start | bytes 1572872 | tf_op jit(solution)/shard_map/ppermute | solution.py:217
  99.3 1.8 first.4
  101.3 3.0 %last.4 = (bf16[512,512]{1,0:T(8,128)(2,1)}, bf16[512,512]{1,0:T(8,128)(2,1)}, bf16[256,512]{1,0:T(8,128)(2,1)}, bf16[256,512]{1,0:T(8,128)(2,1)}, bf16[512,512]{1,0:T(8,128)(2,1)}) custom-call(f32[512,512]{1,0:T(8,128)S(1)} %get-tuple-element.64.gate_sum, f32[512,512]{1,0:T(8,128)S(1)} %get-tuple-element.65.up_sum, ...), custom_call_target="tpu_custom_call" | custom-call | flops 1610612736 | bytes 8388608 | tf_op jit(solution)/shard_map/last/pallas_call | solution.py:148
  105.9 2.4 %collective-permute-start.13 = (bf16[512,512]{1,0:T(8,128)(2,1)}, bf16[512,512]{1,0:T(8,128)(2,1)}, u32[]{:S(2)}, u32[]{:S(2)}) collective-permute-start(bf16[512,512]{1,0:T(8,128)(2,1)} %get-tuple-element.68), channel_id=1, source_target_pairs={{0,3},{1,2},{2,1},{3,0},{4,7},{5,6},{6,5},{7,4},{8,11},{9,10},{10,... | collective-permute-start | bytes 1572872 | tf_op jit(solution)/shard_map/ppermute | solution.py:217
  108.3 18.9 %collective-permute-done.6.late_a = bf16[256,512]{1,0:T(8,128)(2,1)S(1)} collective-permute-done((bf16[256,512]{1,0:T(8,128)(2,1)S(1)}, bf16[256,512]{1,0:T(8,128)(2,1)S(1)}, u32[]{:S(2)}, u32[]{:S(2)}) %collective-permute-start.6) | collective-permute-done | bytes 262176 | tf_op jit(solution)/shard_map/ppermute | solution.py:217
  128.2 12.2 %all-to-all-start.1 = ((bf16[64,8,512]{2,1,0:T(8,128)(2,1)}), bf16[64,8,512]{2,1,0:T(8,128)(2,1)}, u32[]{:S(2)}, u32[]{:S(2)}) async-start(bf16[64,8,512]{2,1,0:T(8,128)(2,1)} %bitcast.26), calls=%async_computation.1 | async-start | bytes 1048576 | tf_op jit(solution)/shard_map/all_to_all | solution.py:214
  144.3 3.3 %first.5 = (f32[512,512]{1,0:T(8,128)S(1)}, f32[512,512]{1,0:T(8,128)S(1)}) custom-call(bf16[512,512]{1,0:T(8,128)(2,1)} %get-tuple-element.93.own, bf16[512,512]{1,0:T(8,128)(2,1)} %collective-permute-done.16.near_a, bf16[512,512]{1,0:T(8,128)(2,1)} %collective-permute-done.17.near_b, bf16[1536,512]{1,0:T(8,128)(2,1)S(1)} %pad_maximum_fusion.gate_w, ...), custom_call_target="tpu_custom_call" | custom-call | flops 1610612736 | bytes 8388608 | tf_op jit(solution)/shard_map/first/pallas_call | solution.py:129
  148.6 2.4 %collective-permute-start.15 = (bf16[256,512]{1,0:T(8,128)(2,1)S(1)}, bf16[256,512]{1,0:T(8,128)(2,1)S(1)}, u32[]{:S(2)}, u32[]{:S(2)}) collective-permute-start(bf16[256,512]{1,0:T(8,128)(2,1)S(1)} %add_convert_fusion.2), channel_id=1, source_target_pairs={{0,3},{1,2},{2,1},{3,0},{4,7},{5,6},{6,5},{7,4},{8,11},{9,10},{10,... | collective-permute-start | bytes 786440 | tf_op jit(solution)/shard_map/ppermute | solution.py:217
  152.6 2.9 %last.5 = (bf16[512,512]{1,0:T(8,128)(2,1)S(1)}, bf16[512,512]{1,0:T(8,128)(2,1)S(1)}, bf16[256,512]{1,0:T(8,128)(2,1)}, bf16[256,512]{1,0:T(8,128)(2,1)}, bf16[512,512]{1,0:T(8,128)(2,1)}) custom-call(f32[512,512]{1,0:T(8,128)S(1)} %get-tuple-element.73.gate_sum, f32[512,512]{1,0:T(8,128)S(1)} %get-tuple-element.74.up_sum, ...), custom_call_target="tpu_custom_call" | custom-call | flops 1610612736 | bytes 8388608 | tf_op jit(solution)/shard_map/last/pallas_call | solution.py:148
  156.8 2.0 collective-permute-done.14.late_a
  158.9 2.1 total.4
  161.0 13.8 %all-to-all-start.3 = ((bf16[64,8,512]{2,1,0:T(8,128)(2,1)}), bf16[64,8,512]{2,1,0:T(8,128)(2,1)S(1)}, u32[]{:S(2)}, u32[]{:S(2)}) async-start(bf16[64,8,512]{2,1,0:T(8,128)(2,1)} %bitcast.30), calls=%async_computation.3 | async-start | bytes 1048576 | tf_op jit(solution)/shard_map/all_to_all | solution.py:214
  175.3 2.4 %collective-permute-start.23 = (bf16[256,512]{1,0:T(8,128)(2,1)S(1)}, bf16[256,512]{1,0:T(8,128)(2,1)S(1)}, u32[]{:S(2)}, u32[]{:S(2)}) collective-permute-start(bf16[256,512]{1,0:T(8,128)(2,1)S(1)} %add_convert_fusion), channel_id=1, source_target_pairs={{0,3},{1,2},{2,1},{3,0},{4,7},{5,6},{6,5},{7,4},{8,11},{9,10},{10,... | collective-permute-start | bytes 786440 | tf_op jit(solution)/shard_map/ppermute | solution.py:217
  177.7 11.4 %collective-permute-done.21.got_b = bf16[512,512]{1,0:T(8,128)(2,1)S(1)} collective-permute-done((bf16[512,512]{1,0:T(8,128)(2,1)S(1)}, bf16[512,512]{1,0:T(8,128)(2,1)S(1)}, u32[]{:S(2)}, u32[]{:S(2)}) %collective-permute-start.21) | collective-permute-done | bytes 524320 | tf_op jit(solution)/shard_map/ppermute | solution.py:217
  189.3 5.4 %collective-permute-done.23.late_b = bf16[256,512]{1,0:T(8,128)(2,1)S(1)} collective-permute-done((bf16[256,512]{1,0:T(8,128)(2,1)S(1)}, bf16[256,512]{1,0:T(8,128)(2,1)S(1)}, u32[]{:S(2)}, u32[]{:S(2)}) %collective-permute-start.23) | collective-permute-done | bytes 262176 | tf_op jit(solution)/shard_map/ppermute | solution.py:217
  196.0 13.2 %all-to-all-start.4 = ((bf16[64,8,512]{2,1,0:T(8,128)(2,1)}), bf16[64,8,512]{2,1,0:T(8,128)(2,1)S(1)}, u32[]{:S(2)}, u32[]{:S(2)}) async-start(bf16[64,8,512]{2,1,0:T(8,128)(2,1)} %bitcast.33), calls=%async_computation.4 | async-start | bytes 1048576 | tf_op jit(solution)/shard_map/all_to_all | solution.py:214
  212.6 14.2 %all-to-all-done.4 = bf16[64,8,512]{2,1,0:T(8,128)(2,1)S(1)} async-done(((bf16[64,8,512]{2,1,0:T(8,128)(2,1)}), bf16[64,8,512]{2,1,0:T(8,128)(2,1)S(1)}, u32[]{:S(2)}, u32[]{:S(2)}) %all-to-all-start.4) | async-done | bytes 524320 | tf_op jit(solution)/shard_map/all_to_all | solution.py:214
  (141 shorter events, 37.6 us)
Async XLA Ops:
  2.7 30.9 %all-to-all-start = ((bf16[64,8,512]{2,1,0:T(8,128)(2,1)}), bf16[64,8,512]{2,1,0:T(8,128)(2,1)}, u32[]{:S(2)}, u32[]{:S(2)}) async-start(bf16[64,8,512]{2,1,0:T(8,128)(2,1)} %bitcast.3), calls=%async_computation | async-start | bytes 1048576 | tf_op jit(solution)/shard_map/all_to_all | solution.py:214
  33.6 34.0 %all-to-all-start.2 = ((bf16[64,16,512]{2,1,0:T(8,128)(2,1)}), bf16[64,16,512]{2,1,0:T(8,128)(2,1)}, u32[]{:S(2)}, u32[]{:S(2)}) async-start(bf16[64,16,512]{2,1,0:T(8,128)(2,1)} %bitcast.115), calls=%async_computation.2 | async-start | bytes 2097152 | tf_op jit(solution)/shard_map/all_to_all | solution.py:214
  39.5 14.6 %collective-permute-start.1 = (bf16[512,512]{1,0:T(8,128)(2,1)}, bf16[512,512]{1,0:T(8,128)(2,1)S(1)}, u32[]{:S(2)}, u32[]{:S(2)}) collective-permute-start(bf16[512,512]{1,0:T(8,128)(2,1)} %bitcast.4.own), channel_id=1, source_target_pairs={{0,3},{1,2},{2,1},{3,0},{4,7},{5,6},{6,5},{7,4},{8,11},{9,10},{10,... | collective-permute-start | bytes 1572872 | tf_op jit(solution)/shard_map/ppermute | solution.py:217
  42.1 13.0 %collective-permute-start = (bf16[512,512]{1,0:T(8,128)(2,1)}, bf16[512,512]{1,0:T(8,128)(2,1)S(1)}, u32[]{:S(2)}, u32[]{:S(2)}) collective-permute-start(bf16[512,512]{1,0:T(8,128)(2,1)} %bitcast.4.own), channel_id=1, source_target_pairs={{0,1},{1,0},{2,3},{3,2},{4,5},{5,4},{6,7},{7,6},{8,9},{9,8},{10,11... | collective-permute-start | bytes 1572872 | tf_op jit(solution)/shard_map/ppermute | solution.py:217
  54.8 17.5 %collective-permute-start.2 = (bf16[256,512]{1,0:T(8,128)(2,1)}, bf16[256,512]{1,0:T(8,128)(2,1)S(1)}, u32[]{:S(2)}, u32[]{:S(2)}) collective-permute-start(bf16[256,512]{1,0:T(8,128)(2,1)} %slice.76), channel_id=1, source_target_pairs={{0,1},{1,0},{2,3},{3,2},{4,5},{5,4},{6,7},{7,6},{8,9},{9,8},{10,11... | collective-permute-start | bytes 786440 | tf_op jit(solution)/shard_map/ppermute | solution.py:217
  55.8 16.5 %collective-permute-start.3 = (bf16[256,512]{1,0:T(8,128)(2,1)}, bf16[256,512]{1,0:T(8,128)(2,1)}, u32[]{:S(2)}, u32[]{:S(2)}) collective-permute-start(bf16[256,512]{1,0:T(8,128)(2,1)} %slice.77), channel_id=1, source_target_pairs={{0,3},{1,2},{2,1},{3,0},{4,7},{5,6},{6,5},{7,4},{8,11},{9,10},{10,... | collective-permute-start | bytes 786440 | tf_op jit(solution)/shard_map/ppermute | solution.py:217
  69.8 13.5 %collective-permute-start.9 = (bf16[512,512]{1,0:T(8,128)(2,1)S(1)}, bf16[512,512]{1,0:T(8,128)(2,1)S(1)}, u32[]{:S(2)}, u32[]{:S(2)}) collective-permute-start(bf16[512,512]{1,0:T(8,128)(2,1)S(1)} %get-tuple-element.94.own), channel_id=1, source_target_pairs={{0,3},{1,2},{2,1},{3,0},{4,7},{5,6},{6,5},{7,4},{8,11},{9,10},{10,... | collective-permute-start | bytes 1572872 | tf_op jit(solution)/shard_map/ppermute | solution.py:217
  72.3 12.1 %collective-permute-start.8 = (bf16[512,512]{1,0:T(8,128)(2,1)S(1)}, bf16[512,512]{1,0:T(8,128)(2,1)S(1)}, u32[]{:S(2)}, u32[]{:S(2)}) collective-permute-start(bf16[512,512]{1,0:T(8,128)(2,1)S(1)} %get-tuple-element.94.own), channel_id=1, source_target_pairs={{0,1},{1,0},{2,3},{3,2},{4,5},{5,4},{6,7},{7,6},{8,9},{9,8},{10,11... | collective-permute-start | bytes 1572872 | tf_op jit(solution)/shard_map/ppermute | solution.py:217
  78.7 16.8 %collective-permute-start.4 = (bf16[512,512]{1,0:T(8,128)(2,1)S(1)}, bf16[512,512]{1,0:T(8,128)(2,1)S(1)}, u32[]{:S(2)}, u32[]{:S(2)}) collective-permute-start(bf16[512,512]{1,0:T(8,128)(2,1)S(1)} %get-tuple-element.57), channel_id=1, source_target_pairs={{0,1},{1,0},{2,3},{3,2},{4,5},{5,4},{6,7},{7,6},{8,9},{9,8},{10,11... | collective-permute-start | bytes 1572872 | tf_op jit(solution)/shard_map/ppermute | solution.py:217
  80.2 25.5 %collective-permute-start.5 = (bf16[512,512]{1,0:T(8,128)(2,1)S(1)}, bf16[512,512]{1,0:T(8,128)(2,1)S(1)}, u32[]{:S(2)}, u32[]{:S(2)}) collective-permute-start(bf16[512,512]{1,0:T(8,128)(2,1)S(1)} %get-tuple-element.58), channel_id=1, source_target_pairs={{0,3},{1,2},{2,1},{3,0},{4,7},{5,6},{6,5},{7,4},{8,11},{9,10},{10,... | collective-permute-start | bytes 1572872 | tf_op jit(solution)/shard_map/ppermute | solution.py:217
  83.4 17.8 %collective-permute-start.10 = (bf16[256,512]{1,0:T(8,128)(2,1)S(1)}, bf16[256,512]{1,0:T(8,128)(2,1)S(1)}, u32[]{:S(2)}, u32[]{:S(2)}) collective-permute-start(bf16[256,512]{1,0:T(8,128)(2,1)S(1)} %slice.81), channel_id=1, source_target_pairs={{0,1},{1,0},{2,3},{3,2},{4,5},{5,4},{6,7},{7,6},{8,9},{9,8},{10,11... | collective-permute-start | bytes 786440 | tf_op jit(solution)/shard_map/ppermute | solution.py:217
  84.3 16.9 %collective-permute-start.11 = (bf16[256,512]{1,0:T(8,128)(2,1)S(1)}, bf16[256,512]{1,0:T(8,128)(2,1)S(1)}, u32[]{:S(2)}, u32[]{:S(2)}) collective-permute-start(bf16[256,512]{1,0:T(8,128)(2,1)S(1)} %slice.82), channel_id=1, source_target_pairs={{0,3},{1,2},{2,1},{3,0},{4,7},{5,6},{6,5},{7,4},{8,11},{9,10},{10,... | collective-permute-start | bytes 786440 | tf_op jit(solution)/shard_map/ppermute | solution.py:217
  96.6 9.3 %collective-permute-start.7 = (bf16[256,512]{1,0:T(8,128)(2,1)S(1)}, bf16[256,512]{1,0:T(8,128)(2,1)S(1)}, u32[]{:S(2)}, u32[]{:S(2)}) collective-permute-start(bf16[256,512]{1,0:T(8,128)(2,1)S(1)} %add_convert_fusion.4), channel_id=1, source_target_pairs={{0,3},{1,2},{2,1},{3,0},{4,7},{5,6},{6,5},{7,4},{8,11},{9,10},{10,... | collective-permute-start | bytes 786440 | tf_op jit(solution)/shard_map/ppermute | solution.py:217
  96.9 43.5 %collective-permute-start.17 = (bf16[512,512]{1,0:T(8,128)(2,1)}, bf16[512,512]{1,0:T(8,128)(2,1)}, u32[]{:S(2)}, u32[]{:S(2)}) collective-permute-start(bf16[512,512]{1,0:T(8,128)(2,1)} %get-tuple-element.93.own), channel_id=1, source_target_pairs={{0,3},{1,2},{2,1},{3,0},{4,7},{5,6},{6,5},{7,4},{8,11},{9,10},{10,... | collective-permute-start | bytes 1572872 | tf_op jit(solution)/shard_map/ppermute | solution.py:217
  101.2 40.3 %collective-permute-start.16 = (bf16[512,512]{1,0:T(8,128)(2,1)}, bf16[512,512]{1,0:T(8,128)(2,1)}, u32[]{:S(2)}, u32[]{:S(2)}) collective-permute-start(bf16[512,512]{1,0:T(8,128)(2,1)} %get-tuple-element.93.own), channel_id=1, source_target_pairs={{0,1},{1,0},{2,3},{3,2},{4,5},{5,4},{6,7},{7,6},{8,9},{9,8},{10,11... | collective-permute-start | bytes 1572872 | tf_op jit(solution)/shard_map/ppermute | solution.py:217
  101.3 25.9 %copy-start.8 = (bf16[512,512]{1,0:T(8,128)(2,1)S(1)}, bf16[512,512]{1,0:T(8,128)(2,1)}, u32[]{:S(2)}) copy-start(bf16[512,512]{1,0:T(8,128)(2,1)} %get-tuple-element.56.kept) | copy-start | bytes 1572868
  104.3 43.3 %collective-permute-start.12 = (bf16[512,512]{1,0:T(8,128)(2,1)}, bf16[512,512]{1,0:T(8,128)(2,1)}, u32[]{:S(2)}, u32[]{:S(2)}) collective-permute-start(bf16[512,512]{1,0:T(8,128)(2,1)} %get-tuple-element.67), channel_id=1, source_target_pairs={{0,1},{1,0},{2,3},{3,2},{4,5},{5,4},{6,7},{7,6},{8,9},{9,8},{10,11... | collective-permute-start | bytes 1572872 | tf_op jit(solution)/shard_map/ppermute | solution.py:217
  105.8 21.4 %collective-permute-start.6 = (bf16[256,512]{1,0:T(8,128)(2,1)S(1)}, bf16[256,512]{1,0:T(8,128)(2,1)S(1)}, u32[]{:S(2)}, u32[]{:S(2)}) collective-permute-start(bf16[256,512]{1,0:T(8,128)(2,1)S(1)} %add_convert_fusion.5), channel_id=1, source_target_pairs={{0,1},{1,0},{2,3},{3,2},{4,5},{5,4},{6,7},{7,6},{8,9},{9,8},{10,11... | collective-permute-start | bytes 786440 | tf_op jit(solution)/shard_map/ppermute | solution.py:217
  105.9 45.1 %collective-permute-start.13 = (bf16[512,512]{1,0:T(8,128)(2,1)}, bf16[512,512]{1,0:T(8,128)(2,1)}, u32[]{:S(2)}, u32[]{:S(2)}) collective-permute-start(bf16[512,512]{1,0:T(8,128)(2,1)} %get-tuple-element.68), channel_id=1, source_target_pairs={{0,3},{1,2},{2,1},{3,0},{4,7},{5,6},{6,5},{7,4},{8,11},{9,10},{10,... | collective-permute-start | bytes 1572872 | tf_op jit(solution)/shard_map/ppermute | solution.py:217
  128.2 32.8 %all-to-all-start.1 = ((bf16[64,8,512]{2,1,0:T(8,128)(2,1)}), bf16[64,8,512]{2,1,0:T(8,128)(2,1)}, u32[]{:S(2)}, u32[]{:S(2)}) async-start(bf16[64,8,512]{2,1,0:T(8,128)(2,1)} %bitcast.26), calls=%async_computation.1 | async-start | bytes 1048576 | tf_op jit(solution)/shard_map/all_to_all | solution.py:214
  141.3 11.3 %collective-permute-start.18 = (bf16[256,512]{1,0:T(8,128)(2,1)S(1)}, bf16[256,512]{1,0:T(8,128)(2,1)S(1)}, u32[]{:S(2)}, u32[]{:S(2)}) collective-permute-start(bf16[256,512]{1,0:T(8,128)(2,1)S(1)} %slice.86), channel_id=1, source_target_pairs={{0,1},{1,0},{2,3},{3,2},{4,5},{5,4},{6,7},{7,6},{8,9},{9,8},{10,11... | collective-permute-start | bytes 786440 | tf_op jit(solution)/shard_map/ppermute | solution.py:217
  142.4 10.2 %collective-permute-start.19 = (bf16[256,512]{1,0:T(8,128)(2,1)S(1)}, bf16[256,512]{1,0:T(8,128)(2,1)S(1)}, u32[]{:S(2)}, u32[]{:S(2)}) collective-permute-start(bf16[256,512]{1,0:T(8,128)(2,1)S(1)} %slice.87), channel_id=1, source_target_pairs={{0,3},{1,2},{2,1},{3,0},{4,7},{5,6},{6,5},{7,4},{8,11},{9,10},{10,... | collective-permute-start | bytes 786440 | tf_op jit(solution)/shard_map/ppermute | solution.py:217
  148.6 8.2 %collective-permute-start.15 = (bf16[256,512]{1,0:T(8,128)(2,1)S(1)}, bf16[256,512]{1,0:T(8,128)(2,1)S(1)}, u32[]{:S(2)}, u32[]{:S(2)}) collective-permute-start(bf16[256,512]{1,0:T(8,128)(2,1)S(1)} %add_convert_fusion.2), channel_id=1, source_target_pairs={{0,3},{1,2},{2,1},{3,0},{4,7},{5,6},{6,5},{7,4},{8,11},{9,10},{10,... | collective-permute-start | bytes 786440 | tf_op jit(solution)/shard_map/ppermute | solution.py:217
  152.1 6.8 %collective-permute-start.14 = (bf16[256,512]{1,0:T(8,128)(2,1)S(1)}, bf16[256,512]{1,0:T(8,128)(2,1)S(1)}, u32[]{:S(2)}, u32[]{:S(2)}) collective-permute-start(bf16[256,512]{1,0:T(8,128)(2,1)S(1)} %add_convert_fusion.3), channel_id=1, source_target_pairs={{0,1},{1,0},{2,3},{3,2},{4,5},{5,4},{6,7},{7,6},{8,9},{9,8},{10,11... | collective-permute-start | bytes 786440 | tf_op jit(solution)/shard_map/ppermute | solution.py:217
  155.5 19.7 %collective-permute-start.20 = (bf16[512,512]{1,0:T(8,128)(2,1)S(1)}, bf16[512,512]{1,0:T(8,128)(2,1)S(1)}, u32[]{:S(2)}, u32[]{:S(2)}) collective-permute-start(bf16[512,512]{1,0:T(8,128)(2,1)S(1)} %get-tuple-element.76), channel_id=1, source_target_pairs={{0,1},{1,0},{2,3},{3,2},{4,5},{5,4},{6,7},{7,6},{8,9},{9,8},{10,11... | collective-permute-start | bytes 1572872 | tf_op jit(solution)/shard_map/ppermute | solution.py:217
  158.9 30.2 %copy-start.28 = (bf16[256,512]{1,0:T(8,128)(2,1)S(1)}, bf16[256,512]{1,0:T(8,128)(2,1)}, u32[]{:S(2)}) copy-start(bf16[256,512]{1,0:T(8,128)(2,1)} %get-tuple-element.78) | copy-start | bytes 786436
  158.9 36.0 %copy-start.9 = (bf16[512,512]{1,0:T(8,128)(2,1)S(1)}, bf16[512,512]{1,0:T(8,128)(2,1)}, u32[]{:S(2)}) copy-start(bf16[512,512]{1,0:T(8,128)(2,1)} %get-tuple-element.75.kept) | copy-start | bytes 1572868
  161.0 35.0 %all-to-all-start.3 = ((bf16[64,8,512]{2,1,0:T(8,128)(2,1)}), bf16[64,8,512]{2,1,0:T(8,128)(2,1)S(1)}, u32[]{:S(2)}, u32[]{:S(2)}) async-start(bf16[64,8,512]{2,1,0:T(8,128)(2,1)} %bitcast.30), calls=%async_computation.3 | async-start | bytes 1048576 | tf_op jit(solution)/shard_map/all_to_all | solution.py:214
  174.8 14.3 %collective-permute-start.21 = (bf16[512,512]{1,0:T(8,128)(2,1)S(1)}, bf16[512,512]{1,0:T(8,128)(2,1)S(1)}, u32[]{:S(2)}, u32[]{:S(2)}) collective-permute-start(bf16[512,512]{1,0:T(8,128)(2,1)S(1)} %get-tuple-element.77), channel_id=1, source_target_pairs={{0,3},{1,2},{2,1},{3,0},{4,7},{5,6},{6,5},{7,4},{8,11},{9,10},{10,... | collective-permute-start | bytes 1572872 | tf_op jit(solution)/shard_map/ppermute | solution.py:217
  175.3 19.4 %collective-permute-start.23 = (bf16[256,512]{1,0:T(8,128)(2,1)S(1)}, bf16[256,512]{1,0:T(8,128)(2,1)S(1)}, u32[]{:S(2)}, u32[]{:S(2)}) collective-permute-start(bf16[256,512]{1,0:T(8,128)(2,1)S(1)} %add_convert_fusion), channel_id=1, source_target_pairs={{0,3},{1,2},{2,1},{3,0},{4,7},{5,6},{6,5},{7,4},{8,11},{9,10},{10,... | collective-permute-start | bytes 786440 | tf_op jit(solution)/shard_map/ppermute | solution.py:217
  189.2 5.7 %collective-permute-start.22 = (bf16[256,512]{1,0:T(8,128)(2,1)S(1)}, bf16[256,512]{1,0:T(8,128)(2,1)S(1)}, u32[]{:S(2)}, u32[]{:S(2)}) collective-permute-start(bf16[256,512]{1,0:T(8,128)(2,1)S(1)} %add_convert_fusion.1), channel_id=1, source_target_pairs={{0,1},{1,0},{2,3},{3,2},{4,5},{5,4},{6,7},{7,6},{8,9},{9,8},{10,11... | collective-permute-start | bytes 786440 | tf_op jit(solution)/shard_map/ppermute | solution.py:217
  196.0 30.9 %all-to-all-start.4 = ((bf16[64,8,512]{2,1,0:T(8,128)(2,1)}), bf16[64,8,512]{2,1,0:T(8,128)(2,1)S(1)}, u32[]{:S(2)}, u32[]{:S(2)}) async-start(bf16[64,8,512]{2,1,0:T(8,128)(2,1)} %bitcast.33), calls=%async_computation.4 | async-start | bytes 1048576 | tf_op jit(solution)/shard_map/all_to_all | solution.py:214
  (29 other events, 234.5 us)
